TPU v7x, 128 devices: a whole 4x4x4 slice. The times are simulated.
128 devices in a mesh: sp: 16 (over z, y), tp: 8 (over x, core).
Axes of the slice: x: 4, y: 4, z: 4, core: 2. Of those that a mesh axis runs over, the one named last changes fastest.
Arguments:
- arriving_hidden_sum: bfloat16 [16384, 2048], P('sp'), may hold values from -40 to 40
- content_entries_clustered: bfloat16 [16384, 4096], P('sp', 'tp'), may hold values from -6 to 6
- leaving_switch_entries: bfloat16 [16384, 4096], P('sp', 'tp'), may hold values from -6 to 6
- linked_source_target_pairs: bfloat16 [16384, 8, 2, 128], P('sp', 'tp'), may hold values from -1.78125 to 1.78125
- raw_interval_length: bfloat16 [16384, 64], P('sp', 'tp'), may hold values from -5 to 5
- spike_extra_lognoise: float32 [16384, 64], P('sp', 'tp'), may hold values from -0.6 to 0
- content_filter_kernel: bfloat16 [4, 4096], P(None, 'tp'), may hold values from -3 to 3
- coupling_filter_kernel: bfloat16 [4, 8, 2, 128], P(None, 'tp'), may hold values from -3 to 3
- interval_shift_vector: float32 [64], P('tp'), may hold values from -0.5 to 0.5
- fading_speed_exponent: float32 [64], P('tp'), may hold values from -16 to -2.9
- skip_channel_factor: float32 [64], P('tp'), may hold values from 1 to 10
- cluster_rescale_vector: float32 [4096], P('tp'), may hold values from 0.1 to 1.9
- blender_final_tensor: bfloat16 [4096, 2048], P('tp'), may hold values from -0.09375 to 0.09375
- prelayer_rescale_vector: float32 [2048], replicated, may hold values from 0.1 to 1.9
- switching_linear_tensor: bfloat16 [2048, 5632], P('sp', 'tp'), may hold values from -0.125 to 0.125
- widening_linear_tensor: bfloat16 [2048, 5632], P('sp', 'tp'), may hold values from -0.125 to 0.125
- contracting_linear_tensor: bfloat16 [5632, 2048], P('tp', 'sp'), may hold values from -0.078125 to 0.078125
Outputs:
- residual_out: bfloat16 [16384, 2048], P('sp', 'tp')
All inputs are finite; a program needn't handle non-finite values.
Results may differ from a plain program's by a relative error of at most 0.012.
Values may be sent and summed in bfloat16 or wider, within the bound.
No kernel may reach another device: no remote copies, remote signals or barrier semaphores. Data moves between devices by JAX's collectives and lax.ppermute only.
A program may use at most 128 MiB of HBM per device.

v0:
```python
import functools

import jax
import jax.numpy as jnp
from jax import lax
from jax.experimental import pallas as pl
from jax.experimental.pallas import tpu as pltpu
from jax.sharding import Mesh
from jax.sharding import PartitionSpec as P


BF = jnp.bfloat16
F32 = jnp.float32
EPS = 1e-06
T = 1024
BLK = 128
NB = T // BLK
HEADS = 8
CH = 512
ST = 128
PAIR = 128
HALO = 16
LOGROWS = 16
D = 2048
COL = 256
FF = 704
PACK = 2 * FF + FF
FIRST = 512
SECOND = T - FIRST

SP = ("z", "y")

VMEM = pl.BlockSpec(memory_space=pltpu.VMEM)
SMEM = pl.BlockSpec(memory_space=pltpu.SMEM)
ANY = pl.BlockSpec(memory_space=pl.ANY)


def sds(shape, kind):
    return jax.ShapeDtypeStruct(shape, kind)


def params(mib=48):
    return pltpu.CompilerParams(vmem_limit_bytes=mib * 1024 * 1024)


def silu(x):
    return x * jax.nn.sigmoid(x)


def hi_dot(a, b):
    return jnp.dot(a, b, preferred_element_type=F32, precision=lax.Precision.HIGHEST)


def lane_low():
    return lax.broadcasted_iota(jnp.int32, (1, PAIR), 1) < PAIR // 2


def spread(rows, width, pieces):
    parts, rest = [], rows
    for _ in range(pieces):
        part = rest.astype(BF)
        rest = rest - part.astype(F32)
        parts.append(part)
    head = lax.broadcasted_iota(jnp.int32, (HEADS, HEADS * width), 0)
    lane = lax.broadcasted_iota(jnp.int32, (HEADS, HEADS * width), 1)
    ones = ((lane >= head * width) & (lane < (head + 1) * width)).astype(F32).astype(BF)
    return lax.dot_general(
        jnp.concatenate(parts, axis=0), jnp.concatenate([ones] * pieces, axis=0),
        (((0,), (0,)), ((), ())), preferred_element_type=F32,
    )


def block_lanes(b):
    return pl.ds(pl.multiple_of(b * BLK, BLK), BLK)


def conv_rows(ext, taps):
    total = ext[HALO - 3 : HALO - 3 + BLK] * taps[0:1]
    for k in range(1, 4):
        total = total + ext[HALO - 3 + k : HALO - 3 + k + BLK] * taps[k : k + 1]
    return silu(total).astype(BF)


def softplus(x):
    return jnp.maximum(x, 0.0) + jnp.log1p(jnp.exp(-jnp.abs(x)))


def state_body(
    content, pairs, halo, raw, spike, shift, fading, taps_c, taps_p,
    values, maps, cum_out, tot_out, step_out, entering, payload,
    ext_c, ext_p, factors, ends, carry,
):
    ext_c[0:HALO] = halo[:, 0:CH]
    ext_p[0:HALO] = halo[:, CH : CH + 256]
    ext_c[HALO : HALO + T] = content[...]
    ext_p[HALO : HALO + T] = pairs[...]
    carry[...] = jnp.zeros((ST, CH), F32)
    row = lax.broadcasted_iota(jnp.int32, (BLK, BLK), 0)
    col = lax.broadcasted_iota(jnp.int32, (BLK, BLK), 1)
    triu = (row <= col).astype(F32)
    tc = taps_c[...].astype(F32)
    tp = taps_p[...].astype(F32)
    step = softplus(raw[...].astype(F32) + shift[...])
    step_out[...] = step
    log = -jnp.exp(fading[...]) * step + spike[...]
    cum = hi_dot(
        jnp.concatenate([log[:, b * BLK : (b + 1) * BLK] for b in range(NB)], axis=0), triu
    )
    prior = jnp.zeros((HEADS, 1), F32)
    for b in range(NB):
        lanes = slice(b * BLK, (b + 1) * BLK)
        here = cum[b * HEADS : (b + 1) * HEADS]
        end = here[:, BLK - 1 : BLK]
        cum_out[:, lanes] = here
        tot_out[:, lanes] = here + prior
        factors[b] = step[:, lanes] * jnp.exp(end - here)
        ends[b] = jnp.broadcast_to(jnp.exp(end), (HEADS, BLK))
        prior = prior + end

    def block(b, _):
        at = pl.multiple_of(b * BLK, BLK)
        rows = pl.ds(at, BLK)
        wide = pl.ds(at, BLK + HALO)
        v = conv_rows(ext_c[wide, :].astype(F32), tc)
        m = conv_rows(ext_p[wide, :].astype(F32), tp)
        values[rows, :] = v
        maps[rows, :] = m
        scaled = (v.astype(F32) * spread(factors[b], 64, 2)).astype(BF)
        added = lax.dot_general(
            m[:, 0:ST], scaled, (((0,), (0,)), ((), ())), preferred_element_type=F32
        )
        old = carry[...]
        entering[b] = old.astype(BF)
        carry[...] = old * spread(ends[b], 64, 2) + added
        return 0

    lax.fori_loop(0, NB, block, 0, unroll=2)
    payload[0:ST, :] = carry[...].astype(BF)
    total = spread(jnp.broadcast_to(prior, (HEADS, BLK)), 64, 3)[0:8]
    high = total.astype(BF)
    low = (total - high.astype(F32)).astype(BF)
    payload[ST : ST + LOGROWS, :] = jnp.concatenate([high, low], axis=0)


def state_kernel(*args):
    return pl.pallas_call(
        state_body,
        out_shape=(
            sds((T, CH), BF),
            sds((T, 256), BF),
            sds((HEADS, T), F32),
            sds((HEADS, T), F32),
            sds((HEADS, T), F32),
            sds((NB, ST, CH), BF),
            sds((ST + LOGROWS, CH), BF),
        ),
        in_specs=[VMEM] * 9,
        out_specs=(VMEM,) * 7,
        scratch_shapes=[
            pltpu.VMEM((T + HALO, CH), BF),
            pltpu.VMEM((T + HALO, 256), BF),
            pltpu.VMEM((NB, HEADS, BLK), F32),
            pltpu.VMEM((NB, HEADS, BLK), F32),
            pltpu.VMEM((ST, CH), F32),
        ],
        compiler_params=params(16),
        name="state",
    )(*args)


def local_body(values, maps, cum_in, step_in, entering, skip, gate, blend, out, gate_out):
    row = lax.broadcasted_iota(jnp.int32, (BLK, BLK), 0)
    col = lax.broadcasted_iota(jnp.int32, (BLK, BLK), 1)
    causal = col <= row
    low = lane_low()
    gain = spread(jnp.broadcast_to(skip[...], (HEADS, BLK)), 64, 3)

    def block(b, _):
        rows = block_lanes(b)
        v = values[rows, :]
        m = maps[rows, :]
        write, read = m[:, 0:ST], m[:, ST : 2 * ST]
        cum = cum_in[:, rows]
        cum_wide = spread(cum, BLK, 3)
        steps = step_in[:, rows]
        meet = lax.dot_general(
            read, write, (((1,), (1,)), ((), ())), preferred_element_type=F32
        )
        parts = []
        for p in range(HEADS // 2):
            weights = []
            for h in (2 * p, 2 * p + 1):
                gap = cum_wide[:, h * BLK : (h + 1) * BLK] - cum[h : h + 1, :]
                decay = jnp.exp(jnp.where(causal, gap, -jnp.inf))
                weights.append((meet * decay * steps[h : h + 1, :]).astype(BF))
            vp = v[:, p * PAIR : (p + 1) * PAIR]
            none = jnp.zeros_like(vp)
            stacked = jnp.concatenate(
                [jnp.where(low, vp, none), jnp.where(low, none, vp)], axis=0
            )
            parts.append(
                jnp.dot(
                    jnp.concatenate(weights, axis=1), stacked, preferred_element_type=F32
                )
            )
        within = jnp.concatenate(parts, axis=1)
        carried = jnp.dot(read, entering[b], preferred_element_type=F32)
        carried = carried * spread(jnp.exp(cum), 64, 2)
        out[rows, :] = within + carried + v.astype(F32) * gain
        gate_out[rows, :] = silu(gate[rows, :].astype(F32))
        return 0

    lax.fori_loop(0, NB, block, 0)


def local_kernel(*args):
    return pl.pallas_call(
        local_body,
        out_shape=(sds((T, CH), F32), sds((T, CH), F32)),
        in_specs=[VMEM] * 8,
        out_specs=(VMEM,) * 2,
        compiler_params=params(12),
        cost_estimate=pl.CostEstimate(flops=6_000_000_000, transcendentals=0, bytes_accessed=6_000_000),
        name="local",
    )(*args)


def tail_body(content, pairs, out):
    out[:, 0:CH] = content[...]
    out[:, CH : CH + 256] = pairs[...]


def tail_kernel(content, pairs):
    last = T // HALO - 1
    return pl.pallas_call(
        tail_body,
        out_shape=sds((HALO, CH + 256), BF),
        grid=(1,),
        in_specs=[
            pl.BlockSpec((HALO, CH), lambda _: (last, 0)),
            pl.BlockSpec((HALO, 256), lambda _: (last, 0)),
        ],
        out_specs=VMEM,
        compiler_params=params(4),
        name="tail",
    )(content, pairs)


def log_row(ref):
    return ref[ST : ST + 1, :].astype(F32) + ref[ST + 8 : ST + 9, :].astype(F32)


def scan_line(place, refs, state, prefix):
    state[...] = jnp.zeros((ST, CH), F32)
    prefix[...] = jnp.zeros((ST, CH), F32)
    count = len(refs)
    logs = [log_row(r) for r in refs]
    whole = jnp.zeros((1, CH), F32)
    ahead = jnp.zeros((1, CH), F32)
    for j in range(count):
        for d in range(count):

            @pl.when(lax.rem(place - j + count, count) == d)
            def _(d=d):
                if d == 0:
                    prefix[...] = state[...]
                state[...] = state[...] * jnp.exp(logs[d]) + refs[d][0:ST, :].astype(F32)

    for d in range(count):
        whole = whole + logs[d]
        ahead = ahead + jnp.where(place >= d, logs[d], 0.0) if d else ahead
    return whole, ahead


def line_body(place, r0, r1, r2, r3, payload, prefix, ahead_out, state):
    whole, ahead = scan_line(place[0], (r0, r1, r2, r3), state, prefix)
    payload[0:ST, :] = state[...].astype(BF)
    high = whole.astype(BF)
    low = (whole - high.astype(F32)).astype(BF)
    payload[ST : ST + 8, :] = jnp.broadcast_to(high, (8, CH))
    payload[ST + 8 : ST + 16, :] = jnp.broadcast_to(low, (8, CH))
    ahead_out[...] = jnp.broadcast_to(ahead, (8, CH))


def line_kernel(place, received):
    return pl.pallas_call(
        line_body,
        out_shape=(
            sds((ST + LOGROWS, CH), BF),
            sds((ST, CH), F32),
            sds((8, CH), F32),
        ),
        in_specs=[SMEM] + [VMEM] * 4,
        out_specs=(VMEM,) * 3,
        scratch_shapes=[pltpu.VMEM((ST, CH), F32)],
        compiler_params=params(8),
        name="line",
    )(place, *received)


def incoming_body(place, q0, q1, q2, q3, prefix, ahead, incoming, state, prefix_z):
    scan_line(place[0], (q0, q1, q2, q3), state, prefix_z)
    incoming[...] = (prefix_z[...] * jnp.exp(ahead[0:1, :]) + prefix[...]).astype(BF)


def incoming_kernel(place, received, prefix, ahead):
    return pl.pallas_call(
        incoming_body,
        out_shape=sds((ST, CH), BF),
        in_specs=[SMEM] + [VMEM] * 6,
        out_specs=VMEM,
        scratch_shapes=[pltpu.VMEM((ST, CH), F32), pltpu.VMEM((ST, CH), F32)],
        compiler_params=params(8),
        name="incoming",
    )(place, *received, prefix, ahead)


def mix_body(
    start, count, order, incoming, local, maps, tot, gate, gain, blend, send, keep, mixed
):
    rescale = gain[...]

    def block(b, _):
        rows = pl.ds(pl.multiple_of(start + b * BLK, BLK), BLK)
        read = maps[rows, ST : 2 * ST]
        arrived = jnp.dot(read, incoming[...], preferred_element_type=F32)
        mixer = local[rows, :] + arrived * spread(jnp.exp(tot[:, rows]), 64, 2)
        gated = mixer * gate[rows, :]
        scale = lax.rsqrt(jnp.mean(gated * gated, axis=1, keepdims=True) + EPS)
        mixed[pl.ds(pl.multiple_of(b * BLK, BLK), BLK), :] = (gated * scale * rescale).astype(BF)
        return 0

    lax.fori_loop(0, count // BLK, block, 0, unroll=2)
    for half, target in ((1, send), (0, keep)):
        for k in range(4):
            cols = pl.ds(pl.multiple_of(order[half * 4 + k] * COL, COL), COL)
            target[k] = jnp.dot(
                mixed[...], blend[:, cols], preferred_element_type=F32
            ).astype(BF)


def mix_kernel(start, count, order, *args):
    return pl.pallas_call(
        functools.partial(mix_body, start, count),
        out_shape=(sds((4, count, COL), BF), sds((4, count, COL), BF)),
        in_specs=[SMEM] + [VMEM] * 7,
        out_specs=(VMEM,) * 2,
        scratch_shapes=[pltpu.VMEM((count, CH), BF)],
        compiler_params=params(16),
        cost_estimate=pl.CostEstimate(flops=3_000_000_000, transcendentals=0, bytes_accessed=6_000_000),
        name="mix",
    )(order, *args)


def pair_body(keep, got, c0, c1, c2, c3):
    for k, out in enumerate((c0, c1, c2, c3)):
        out[...] = (keep[k].astype(F32) + got[k].astype(F32)).astype(BF)


def pair_kernel(keep, got):
    count = keep.shape[1]
    return pl.pallas_call(
        pair_body,
        out_shape=(sds((count, COL), BF),) * 4,
        in_specs=[VMEM] * 2,
        out_specs=(VMEM,) * 4,
        compiler_params=params(8),
        name="pair",
    )(keep, got)


def total_of(refs):
    total = refs[0][...].astype(F32)
    for r in refs[1:]:
        total = total + r[...].astype(F32)
    return total


def own_body(start, c0, f1, f2, f3, arriving, out):
    count = out.shape[0]
    base = arriving[start : start + count, :].astype(F32)
    out[...] = (base + total_of((c0, f1, f2, f3))).astype(BF)


def own_kernel(start, parts, arriving):
    count = parts[0].shape[0]
    return pl.pallas_call(
        functools.partial(own_body, start),
        out_shape=sds((count, COL), BF),
        in_specs=[VMEM] * 5,
        out_specs=VMEM,
        compiler_params=params(8),
        name="own",
    )(*parts, arriving)


def last_body(own, c0, f1, f2, f3, out):
    out[...] = (own[...].astype(F32) + 0.5 * total_of((c0, f1, f2, f3))).astype(BF)


def last_kernel(own, parts):
    return pl.pallas_call(
        last_body,
        out_shape=sds(own.shape, BF),
        in_specs=[VMEM] * 5,
        out_specs=VMEM,
        compiler_params=params(8),
        name="last",
    )(own, *parts)


def join_body(first, own, c0, f1, f2, f3, out):
    split = first.shape[0]
    out[:split, :] = first[...]
    out[split:, :] = (own[...].astype(F32) + 0.5 * total_of((c0, f1, f2, f3))).astype(BF)


def join_kernel(first, own, parts):
    return pl.pallas_call(
        join_body,
        out_shape=sds((T, COL), BF),
        in_specs=[VMEM] * 6,
        out_specs=VMEM,
        compiler_params=params(8),
        name="join",
    )(first, own, *parts)


NORM_ROWS = 128


def row_scale(pieces):
    total = None
    for x in pieces:
        for at in range(0, x.shape[1], 128):
            part = x[:, at : at + 128]
            total = part * part if total is None else total + part * part
    return lax.rsqrt(jnp.sum(total, axis=1, keepdims=True) * (1.0 / D) + EPS)


def ffn_body(
    order, pack, gain, m0, m1, m2, m3, n0, n1, n2, n3, send, keep, weights, rows_x, hid, sem
):
    copies = [
        pltpu.make_async_copy(pack.at[j], weights.at[:, pl.ds(j * 128, 128)], sem)
        for j in range(16)
    ]
    for copy in copies:
        copy.start()
    refs = (m0, m1, m2, m3, n0, n1, n2, n3)

    def norm(b, _):
        rows = pl.ds(pl.multiple_of(b * NORM_ROWS, NORM_ROWS), NORM_ROWS)
        scale = row_scale([r[rows, :].astype(F32) for r in refs])
        for i, r in enumerate(refs):
            cols = pl.ds(pl.multiple_of(order[i] * COL, COL), COL)
            rows_x[rows, cols] = (r[rows, :].astype(F32) * scale * gain[:, cols]).astype(BF)
        return 0

    lax.fori_loop(0, rows_x.shape[0] // NORM_ROWS, norm, 0)
    for copy in copies:
        copy.wait()
    over_k = (((1,), (1,)), ((), ()))
    gate = lax.dot_general(
        rows_x[...], weights[0:FF, :], over_k, preferred_element_type=F32
    )
    up = lax.dot_general(
        rows_x[...], weights[FF : 2 * FF, :], over_k, preferred_element_type=F32
    )
    hid[...] = (silu(gate) * up).astype(BF)
    for half, target in ((1, send), (0, keep)):

        def project(k, _, half=half, target=target):
            cols = pl.ds(pl.multiple_of(order[half * 4 + k] * COL, COL), COL)
            target[k] = jnp.dot(
                hid[...], weights[2 * FF :, cols], preferred_element_type=F32
            ).astype(BF)
            return 0

        lax.fori_loop(0, 4, project, 0)


def ffn_kernel(order, pack, gain, mine, theirs):
    count = mine[0].shape[0]
    return pl.pallas_call(
        ffn_body,
        out_shape=(sds((4, count, COL), BF), sds((4, count, COL), BF)),
        in_specs=[SMEM, pl.BlockSpec(memory_space=pltpu.HBM)] + [VMEM] * 9,
        out_specs=(VMEM,) * 2,
        scratch_shapes=[
            pltpu.VMEM((PACK, D), BF),
            pltpu.VMEM((count, D), BF),
            pltpu.VMEM((count, FF), BF),
            pltpu.SemaphoreType.DMA,
        ],
        compiler_params=params(24),
        cost_estimate=pl.CostEstimate(flops=9_000_000_000, transcendentals=0, bytes_accessed=12_000_000),
        name="ffn",
    )(order, pack, gain, *mine, *theirs)


def turn(array, axis, distance):
    count = lax.axis_size(axis)
    return lax.ppermute(array, axis, [(i, (i + distance) % count) for i in range(count)])


def swap(array):
    return lax.ppermute(array, "c", [(0, 1), (1, 0)])


def reduce_chips(parts):
    c0, c1, c2, c3 = parts
    return c0, turn(c2, "x", 2), turn(c1, "x", 1), turn(c3, "x", -1)


def gather_chips(own):
    return own, turn(own, "x", -1), turn(own, "x", 2), turn(own, "x", 1)


def shards(
    arriving, content, gate, linked, raw, spike, taps_c, taps_p, shift, fading, skip,
    cluster_gain, blender, norm_gain, w_gate, w_up, w_down,
):
    x, c = lax.axis_index("x"), lax.axis_index("c")
    y, z = lax.axis_index("y"), lax.axis_index("z")
    pairs = linked.reshape(T, 256)
    tail = tail_kernel(content, pairs)
    tail, w_gate, w_up, w_down = lax.optimization_barrier((tail, w_gate, w_up, w_down))
    halo = lax.ppermute(tail, SP, [(i, i + 1) for i in range(15)])
    pack = jnp.concatenate([w_gate.T, w_up.T, w_down], axis=0)
    pack = lax.all_gather(pack, SP, axis=0, tiled=True).reshape(16, PACK, 128)
    values, maps, cum, tot, step, entering, payload = state_kernel(
        content, pairs, halo, raw.T, spike.T, shift.reshape(HEADS, 1),
        fading.reshape(HEADS, 1), taps_c, taps_p.reshape(4, 256),
    )
    line = [payload] + [turn(payload, "y", d) for d in (1, 2, 3)]
    local, opened = local_kernel(
        values, maps, cum, step, entering, skip.reshape(HEADS, 1), gate, blender
    )
    local = pltpu.with_memory_space_constraint(local, pltpu.VMEM)
    opened = pltpu.with_memory_space_constraint(opened, pltpu.VMEM)
    mine_cols = lax.dynamic_slice(arriving, (0, (2 * x + c) * COL), (T, COL))
    payload_z, prefix, ahead = line_kernel(y.reshape(1), line)
    lines = [payload_z] + [turn(payload_z, "z", d) for d in (1, 2, 3)]
    steps = jnp.arange(4, dtype=jnp.int32)
    chips = (x + steps) % 4
    order = jnp.concatenate([chips * 2 + c, chips * 2 + (1 - c)]).astype(jnp.int32)
    incoming = incoming_kernel(z.reshape(1), lines, prefix, ahead)
    gain = norm_gain.reshape(1, D)
    mix_args = (incoming, local, maps, tot, opened, cluster_gain.reshape(1, CH), blender)
    spans = ((0, FIRST), (FIRST, SECOND))
    owns, lasts = [], []
    sent, kept = [], []
    for start, count in spans:
        send, keep = mix_kernel(start, count, order, *mix_args)
        sent.append(swap(send))
        kept.append(keep)
    for i, (start, count) in enumerate(spans):
        parts = pair_kernel(kept[i], sent[i])
        parts = reduce_chips(parts)
        owns.append(own_kernel(start, parts, mine_cols))
    pack = pltpu.with_memory_space_constraint(pack, pltpu.HBM)
    for i, (start, count) in enumerate(spans):
        mine = gather_chips(owns[i])
        theirs = tuple(swap(piece) for piece in mine)
        send, keep = ffn_kernel(order, pack, gain, mine, theirs)
        got = swap(send)
        parts = pair_kernel(keep, got)
        lasts.append(reduce_chips(parts))
    return join_kernel(last_kernel(owns[0], lasts[0]), owns[1], lasts[1])


def solution(mesh):
    torus = Mesh(mesh.devices.reshape(4, 4, 4, 2), ("z", "y", "x", "c"))
    tp = ("x", "c")
    return jax.shard_map(
        shards,
        mesh=torus,
        in_specs=(
            P(SP, None), P(SP, tp), P(SP, tp), P(SP, tp, None, None), P(SP, tp), P(SP, tp),
            P(None, tp), P(None, tp, None, None), P(tp), P(tp), P(tp), P(tp), P(tp, None),
            P(), P(SP, tp), P(SP, tp), P(tp, SP),
        ),
        out_specs=P(SP, tp),
        check_vma=False,
    )
```

profile of v0, /device:TPU:0, one launch (start us, length us, event | category | flops | bytes accessed | tf_op | source)
XLA Modules:
  0.0 174.6 jit_solution(18380843537627855039)
XLA Ops:
  11.1 3.6 %collective-permute-start = (bf16[16,768]{1,0:T(8,128)(2,1)S(1)}, bf16[16,768]{1,0:T(8,128)(2,1)S(1)}, u32[]{:S(2)}, u32[]{:S(2)}) collective-permute-start(bf16[16,768]{1,0:T(8,128)(2,1)S(1)} %tail.1), channel_id=1, source_target_pairs={{0,8},{8,16},{16,24},{24,32},{32,40},{40,48},{48,56},{56,64},{64,7... | collective-permute-start | bytes 73736 | tf_op jit(solution)/shard_map/ppermute | solution.py:529
  16.2 5.3 %state.1 = (bf16[1024,512]{1,0:T(8,128)(2,1)S(1)}, bf16[1024,256]{1,0:T(8,128)(2,1)S(1)}, f32[8,1024]{1,0:T(8,128)S(1)}, f32[8,1024]{1,0:T(8,128)S(1)}, f32[8,10...) custom-call(bf16[1024,512]{1,0:T(8,128)(2,1)S(1)} %copy-done.1, ...), custom_call_target="tpu_custom_call" | custom-call | tf_op jit(solution)/shard_map/state/pallas_call | solution.py:146
  23.5 2.3 %collective-permute-start.1 = (bf16[144,512]{1,0:T(8,128)(2,1)S(1)}, bf16[144,512]{1,0:T(8,128)(2,1)S(1)}, u32[]{:S(2)}, u32[]{:S(2)}) collective-permute-start(bf16[144,512]{1,0:T(8,128)(2,1)S(1)} %get-tuple-element.46.r0), channel_id=1, source_target_pairs={{0,8},{8,16},{16,24},{24,0},{1,9},{9,17},{17,25},{25,1},{2,10},{10... | collective-permute-start | bytes 442376 | tf_op jit(solution)/shard_map/ppermute | solution.py:504
  25.8 2.9 %collective-permute-start.2 = (bf16[144,512]{1,0:T(8,128)(2,1)S(1)}, bf16[144,512]{1,0:T(8,128)(2,1)S(1)}, u32[]{:S(2)}, u32[]{:S(2)}) collective-permute-start(bf16[144,512]{1,0:T(8,128)(2,1)S(1)} %get-tuple-element.46.r0), channel_id=1, source_target_pairs={{0,16},{8,24},{16,0},{24,8},{1,17},{9,25},{17,1},{25,9},{2,18},{10... | collective-permute-start | bytes 442376 | tf_op jit(solution)/shard_map/ppermute | solution.py:504
  30.3 3.6 %collective-permute-done.1.r1 = bf16[144,512]{1,0:T(8,128)(2,1)S(1)} collective-permute-done((bf16[144,512]{1,0:T(8,128)(2,1)S(1)}, bf16[144,512]{1,0:T(8,128)(2,1)S(1)}, u32[]{:S(2)}, u32[]{:S(2)}) %collective-permute-start.1) | collective-permute-done | bytes 147488 | tf_op jit(solution)/shard_map/ppermute | solution.py:504
  33.9 8.2 %collective-permute-done.2.r2 = bf16[144,512]{1,0:T(8,128)(2,1)S(1)} collective-permute-done((bf16[144,512]{1,0:T(8,128)(2,1)S(1)}, bf16[144,512]{1,0:T(8,128)(2,1)S(1)}, u32[]{:S(2)}, u32[]{:S(2)}) %collective-permute-start.2) | collective-permute-done | bytes 147488 | tf_op jit(solution)/shard_map/ppermute | solution.py:504
  44.4 3.3 %collective-permute-start.5 = (bf16[144,512]{1,0:T(8,128)(2,1)S(1)}, bf16[144,512]{1,0:T(8,128)(2,1)S(1)}, u32[]{:S(2)}, u32[]{:S(2)}) collective-permute-start(bf16[144,512]{1,0:T(8,128)(2,1)S(1)} %get-tuple-element.47.q0), channel_id=1, source_target_pairs={{0,64},{32,96},{64,0},{96,32},{1,65},{33,97},{65,1},{97,33},{2,66}... | collective-permute-start | bytes 442376 | tf_op jit(solution)/shard_map/ppermute | solution.py:504
  53.2 4.6 %local.1 = (f32[1024,512]{1,0:T(8,128)S(1)}, f32[1024,512]{1,0:T(8,128)S(1)}) custom-call(bf16[1024,512]{1,0:T(8,128)(2,1)S(1)} %copy-done.9, bf16[1024,256]{1,0:T(8,128)(2,1)S(1)} %get-tuple-element.51.maps, f32[8,1024]{1,0:T(8,128)S(1)} %get-tuple-element.52.cum_in, f32[8,1024]{1,0:T(8,128)S(1)} %get-tuple-element.53.step_in, ...), custom_call_target="tpu_custom_call" | custom-call | flops 6000000000 | bytes 6000000 | tf_op jit(solution)/shard_map/local/pallas_call | solution.py:217
  58.2 2.6 %mix.3 = (bf16[4,512,256]{2,1,0:T(8,128)(2,1)S(1)}, bf16[4,512,256]{2,1,0:T(8,128)(2,1)S(1)}) custom-call(s32[8]{0:T(128)S(1)} %pad_add_fusion.order, bf16[128,512]{1,0:T(8,128)(2,1)S(1)} %incoming.1, f32[1024,512]{1,0:T(8,128)S(1)} %get-tuple-element.55.local, bf16[1024,256]{1,0:T(8,128)(2,1)S(1)} %get-tuple-element.51.maps, ...), custom_call_target="tpu_custom_call" | custom-call | flops 3000000000 | bytes 6000000 | tf_op jit(solution)/shard_map/mix/pallas_call | solution.py:343
  60.9 2.6 %mix.2 = (bf16[4,512,256]{2,1,0:T(8,128)(2,1)S(1)}, bf16[4,512,256]{2,1,0:T(8,128)(2,1)S(1)}) custom-call(s32[8]{0:T(128)S(1)} %pad_add_fusion.order, bf16[128,512]{1,0:T(8,128)(2,1)S(1)} %incoming.1, f32[1024,512]{1,0:T(8,128)S(1)} %get-tuple-element.55.local, bf16[1024,256]{1,0:T(8,128)(2,1)S(1)} %get-tuple-element.51.maps, ...), custom_call_target="tpu_custom_call" | custom-call | flops 3000000000 | bytes 6000000 | tf_op jit(solution)/shard_map/mix/pallas_call | solution.py:343
  64.4 3.1 %collective-permute-start.23 = (bf16[512,256]{1,0:T(8,128)(2,1)S(1)}, bf16[512,256]{1,0:T(8,128)(2,1)S(1)}, u32[]{:S(2)}, u32[]{:S(2)}) collective-permute-start(bf16[512,256]{1,0:T(8,128)(2,1)S(1)} %get-tuple-element.76), channel_id=1, source_target_pairs={{0,4},{2,6},{4,0},{6,2},{1,5},{3,7},{5,1},{7,3},{8,12},{10,14},{12... | collective-permute-start | bytes 786440 | tf_op jit(solution)/shard_map/ppermute | solution.py:504
  68.0 2.7 %collective-permute-start.25 = (bf16[512,256]{1,0:T(8,128)(2,1)S(1)}, bf16[512,256]{1,0:T(8,128)(2,1)S(1)}, u32[]{:S(2)}, u32[]{:S(2)}) collective-permute-start(bf16[512,256]{1,0:T(8,128)(2,1)S(1)} %get-tuple-element.78), channel_id=1, source_target_pairs={{0,6},{2,0},{4,2},{6,4},{1,7},{3,1},{5,3},{7,5},{8,14},{10,8},{12,... | collective-permute-start | bytes 786440 | tf_op jit(solution)/shard_map/ppermute | solution.py:504
  72.5 2.7 %collective-permute-done.23.f1 = bf16[512,256]{1,0:T(8,128)(2,1)S(1)} collective-permute-done((bf16[512,256]{1,0:T(8,128)(2,1)S(1)}, bf16[512,256]{1,0:T(8,128)(2,1)S(1)}, u32[]{:S(2)}, u32[]{:S(2)}) %collective-permute-start.23) | collective-permute-done | bytes 262176 | tf_op jit(solution)/shard_map/ppermute | solution.py:504
  77.8 3.1 %collective-permute-done.24.f2 = bf16[512,256]{1,0:T(8,128)(2,1)S(1)} collective-permute-done((bf16[512,256]{1,0:T(8,128)(2,1)S(1)}, bf16[512,256]{1,0:T(8,128)(2,1)S(1)}, u32[]{:S(2)}, u32[]{:S(2)}) %collective-permute-start.24) | collective-permute-done | bytes 262176 | tf_op jit(solution)/shard_map/ppermute | solution.py:504
  86.5 5.4 %collective-permute-done.9.f2 = bf16[512,256]{1,0:T(8,128)(2,1)S(1)} collective-permute-done((bf16[512,256]{1,0:T(8,128)(2,1)S(1)}, bf16[512,256]{1,0:T(8,128)(2,1)S(1)}, u32[]{:S(2)}, u32[]{:S(2)}) %collective-permute-start.9) | collective-permute-done | bytes 262176 | tf_op jit(solution)/shard_map/ppermute | solution.py:504
  92.1 3.0 %collective-permute-start.11 = (bf16[512,256]{1,0:T(8,128)(2,1)S(1)}, bf16[512,256]{1,0:T(8,128)(2,1)S(1)}, u32[]{:S(2)}, u32[]{:S(2)}) collective-permute-start(bf16[512,256]{1,0:T(8,128)(2,1)S(1)} %own.2.m0), channel_id=1, source_target_pairs={{0,6},{2,0},{4,2},{6,4},{1,7},{3,1},{5,3},{7,5},{8,14},{10,8},{12,... | collective-permute-start | bytes 786440 | tf_op jit(solution)/shard_map/ppermute | solution.py:504
  99.2 9.8 %collective-permute-done.11.m1 = bf16[512,256]{1,0:T(8,128)(2,1)S(1)} collective-permute-done((bf16[512,256]{1,0:T(8,128)(2,1)S(1)}, bf16[512,256]{1,0:T(8,128)(2,1)S(1)}, u32[]{:S(2)}, u32[]{:S(2)}) %collective-permute-start.11) | collective-permute-done | bytes 262176 | tf_op jit(solution)/shard_map/ppermute | solution.py:504
  109.6 4.3 %collective-permute-done.28.m3 = bf16[512,256]{1,0:T(8,128)(2,1)S(1)} collective-permute-done((bf16[512,256]{1,0:T(8,128)(2,1)S(1)}, bf16[512,256]{1,0:T(8,128)(2,1)S(1)}, u32[]{:S(2)}, u32[]{:S(2)}) %collective-permute-start.28) | collective-permute-done | bytes 262176 | tf_op jit(solution)/shard_map/ppermute | solution.py:504
  116.6 10.5 %ffn.2 = (bf16[4,512,256]{2,1,0:T(8,128)(2,1)S(1)}, bf16[4,512,256]{2,1,0:T(8,128)(2,1)S(1)}) custom-call(s32[8]{0:T(128)S(1)} %pad_add_fusion.order, bf16[16,2112,128]{2,1,0:T(8,128)(2,1)} %bitcast.38, f32[1,2048]{1,0:T(1,128)S(1)} %bitcast.27, bf16[512,256]{1,0:T(8,128)(2,1)S(1)} %own.2.m0, bf16[512,256]{1,0:T(8,128)(2,1)S(1)} %collective-permute-done.11.m1, ...), custom_call_target="tpu_custom_call" | custom-call | flops 8999999488 | bytes 12000000 | tf_op jit(solution)/shard_map/ffn/pallas_call | solution.py:485
  127.3 11.0 %ffn.3 = (bf16[4,512,256]{2,1,0:T(8,128)(2,1)S(1)}, bf16[4,512,256]{2,1,0:T(8,128)(2,1)S(1)}) custom-call(s32[8]{0:T(128)S(1)} %pad_add_fusion.order, bf16[16,2112,128]{2,1,0:T(8,128)(2,1)} %bitcast.39, f32[1,2048]{1,0:T(1,128)S(1)} %bitcast.28, bf16[512,256]{1,0:T(8,128)(2,1)S(1)} %own.3.m0, bf16[512,256]{1,0:T(8,128)(2,1)S(1)} %collective-permute-done.26.m1, ...), custom_call_target="tpu_custom_call" | custom-call | flops 8999999488 | bytes 12000000 | tf_op jit(solution)/shard_map/ffn/pallas_call | solution.py:485
  139.3 2.7 %collective-permute-start.19 = (bf16[512,256]{1,0:T(8,128)(2,1)S(1)}, bf16[512,256]{1,0:T(8,128)(2,1)S(1)}, u32[]{:S(2)}, u32[]{:S(2)}) collective-permute-start(bf16[512,256]{1,0:T(8,128)(2,1)S(1)} %get-tuple-element.70), channel_id=1, source_target_pairs={{0,4},{2,6},{4,0},{6,2},{1,5},{3,7},{5,1},{7,3},{8,12},{10,14},{12... | collective-permute-start | bytes 786440 | tf_op jit(solution)/shard_map/ppermute | solution.py:504
  150.2 3.3 %collective-permute-start.36 = (bf16[512,256]{1,0:T(8,128)(2,1)S(1)}, bf16[512,256]{1,0:T(8,128)(2,1)S(1)}, u32[]{:S(2)}, u32[]{:S(2)}) collective-permute-start(bf16[512,256]{1,0:T(8,128)(2,1)S(1)} %get-tuple-element.84), channel_id=1, source_target_pairs={{0,6},{2,0},{4,2},{6,4},{1,7},{3,1},{5,3},{7,5},{8,14},{10,8},{12,... | collective-permute-start | bytes 786440 | tf_op jit(solution)/shard_map/ppermute | solution.py:504
  153.5 7.0 %collective-permute-done.20.f2 = bf16[512,256]{1,0:T(8,128)(2,1)S(1)} collective-permute-done((bf16[512,256]{1,0:T(8,128)(2,1)S(1)}, bf16[512,256]{1,0:T(8,128)(2,1)S(1)}, u32[]{:S(2)}, u32[]{:S(2)}) %collective-permute-start.20) | collective-permute-done | bytes 262176 | tf_op jit(solution)/shard_map/ppermute | solution.py:504
  162.2 3.8 %collective-permute-done.35.f2 = bf16[512,256]{1,0:T(8,128)(2,1)S(1)} collective-permute-done((bf16[512,256]{1,0:T(8,128)(2,1)S(1)}, bf16[512,256]{1,0:T(8,128)(2,1)S(1)}, u32[]{:S(2)}, u32[]{:S(2)}) %collective-permute-start.35) | collective-permute-done | bytes 262176 | tf_op jit(solution)/shard_map/ppermute | solution.py:504
  (119 shorter events, 49.4 us)
Async XLA Ops:
  6.5 109.2 %all-gather.2.cloned.1.call-start = ((), (), s32[]{:S(2)}) async-start(), calls=%async_computation | async-start | bytes 9191424 | tf_op jit(solution)/shard_map/all_gather | solution.py:531
  25.8 16.3 %collective-permute-start.2 = (bf16[144,512]{1,0:T(8,128)(2,1)S(1)}, bf16[144,512]{1,0:T(8,128)(2,1)S(1)}, u32[]{:S(2)}, u32[]{:S(2)}) collective-permute-start(bf16[144,512]{1,0:T(8,128)(2,1)S(1)} %get-tuple-element.46.r0), channel_id=1, source_target_pairs={{0,16},{8,24},{16,0},{24,8},{1,17},{9,25},{17,1},{25,9},{2,18},{10... | collective-permute-start | bytes 442376 | tf_op jit(solution)/shard_map/ppermute | solution.py:504
  28.7 13.4 %collective-permute-start.3 = (bf16[144,512]{1,0:T(8,128)(2,1)S(1)}, bf16[144,512]{1,0:T(8,128)(2,1)S(1)}, u32[]{:S(2)}, u32[]{:S(2)}) collective-permute-start(bf16[144,512]{1,0:T(8,128)(2,1)S(1)} %get-tuple-element.46.r0), channel_id=1, source_target_pairs={{0,24},{8,0},{16,8},{24,16},{1,25},{9,1},{17,9},{25,17},{2,26},{10... | collective-permute-start | bytes 442376 | tf_op jit(solution)/shard_map/ppermute | solution.py:504
  42.4 15.5 %collective-permute-start.4 = (bf16[144,512]{1,0:T(8,128)(2,1)S(1)}, bf16[144,512]{1,0:T(8,128)(2,1)S(1)}, u32[]{:S(2)}, u32[]{:S(2)}) collective-permute-start(bf16[144,512]{1,0:T(8,128)(2,1)S(1)} %get-tuple-element.47.q0), channel_id=1, source_target_pairs={{0,32},{32,64},{64,96},{96,0},{1,33},{33,65},{65,97},{97,1},{2,34}... | collective-permute-start | bytes 442376 | tf_op jit(solution)/shard_map/ppermute | solution.py:504
  44.4 13.4 %collective-permute-start.5 = (bf16[144,512]{1,0:T(8,128)(2,1)S(1)}, bf16[144,512]{1,0:T(8,128)(2,1)S(1)}, u32[]{:S(2)}, u32[]{:S(2)}) collective-permute-start(bf16[144,512]{1,0:T(8,128)(2,1)S(1)} %get-tuple-element.47.q0), channel_id=1, source_target_pairs={{0,64},{32,96},{64,0},{96,32},{1,65},{33,97},{65,1},{97,33},{2,66}... | collective-permute-start | bytes 442376 | tf_op jit(solution)/shard_map/ppermute | solution.py:504
  67.5 13.4 %collective-permute-start.24 = (bf16[512,256]{1,0:T(8,128)(2,1)S(1)}, bf16[512,256]{1,0:T(8,128)(2,1)S(1)}, u32[]{:S(2)}, u32[]{:S(2)}) collective-permute-start(bf16[512,256]{1,0:T(8,128)(2,1)S(1)} %get-tuple-element.77), channel_id=1, source_target_pairs={{0,2},{2,4},{4,6},{6,0},{1,3},{3,5},{5,7},{7,1},{8,10},{10,12},{12... | collective-permute-start | bytes 786440 | tf_op jit(solution)/shard_map/ppermute | solution.py:504
  70.9 15.5 %collective-permute-start.10 = (bf16[512,256]{1,0:T(8,128)(2,1)S(1)}, bf16[512,256]{1,0:T(8,128)(2,1)S(1)}, u32[]{:S(2)}, u32[]{:S(2)}) collective-permute-start(bf16[512,256]{1,0:T(8,128)(2,1)S(1)} %get-tuple-element.63), channel_id=1, source_target_pairs={{0,6},{2,0},{4,2},{6,4},{1,7},{3,1},{5,3},{7,5},{8,14},{10,8},{12,... | collective-permute-start | bytes 786440 | tf_op jit(solution)/shard_map/ppermute | solution.py:504
  71.0 15.5 %collective-permute-start.8 = (bf16[512,256]{1,0:T(8,128)(2,1)S(1)}, bf16[512,256]{1,0:T(8,128)(2,1)S(1)}, u32[]{:S(2)}, u32[]{:S(2)}) collective-permute-start(bf16[512,256]{1,0:T(8,128)(2,1)S(1)} %get-tuple-element.61), channel_id=1, source_target_pairs={{0,4},{2,6},{4,0},{6,2},{1,5},{3,7},{5,1},{7,3},{8,12},{10,14},{12... | collective-permute-start | bytes 786440 | tf_op jit(solution)/shard_map/ppermute | solution.py:504
  75.2 16.7 %collective-permute-start.9 = (bf16[512,256]{1,0:T(8,128)(2,1)S(1)}, bf16[512,256]{1,0:T(8,128)(2,1)S(1)}, u32[]{:S(2)}, u32[]{:S(2)}) collective-permute-start(bf16[512,256]{1,0:T(8,128)(2,1)S(1)} %get-tuple-element.62), channel_id=1, source_target_pairs={{0,2},{2,4},{4,6},{6,0},{1,3},{3,5},{5,7},{7,1},{8,10},{10,12},{12... | collective-permute-start | bytes 786440 | tf_op jit(solution)/shard_map/ppermute | solution.py:504
  81.0 16.7 %collective-permute-start.26 = (bf16[512,256]{1,0:T(8,128)(2,1)S(1)}, bf16[512,256]{1,0:T(8,128)(2,1)S(1)}, u32[]{:S(2)}, u32[]{:S(2)}) collective-permute-start(bf16[512,256]{1,0:T(8,128)(2,1)S(1)} %own.3.m0), channel_id=1, source_target_pairs={{0,6},{2,0},{4,2},{6,4},{1,7},{3,1},{5,3},{7,5},{8,14},{10,8},{12,... | collective-permute-start | bytes 786440 | tf_op jit(solution)/shard_map/ppermute | solution.py:504
  83.1 16.1 %collective-permute-start.27 = (bf16[512,256]{1,0:T(8,128)(2,1)S(1)}, bf16[512,256]{1,0:T(8,128)(2,1)S(1)}, u32[]{:S(2)}, u32[]{:S(2)}) collective-permute-start(bf16[512,256]{1,0:T(8,128)(2,1)S(1)} %own.3.m0), channel_id=1, source_target_pairs={{0,4},{2,6},{4,0},{6,2},{1,5},{3,7},{5,1},{7,3},{8,12},{10,14},{12... | collective-permute-start | bytes 786440 | tf_op jit(solution)/shard_map/ppermute | solution.py:504
  92.1 17.0 %collective-permute-start.11 = (bf16[512,256]{1,0:T(8,128)(2,1)S(1)}, bf16[512,256]{1,0:T(8,128)(2,1)S(1)}, u32[]{:S(2)}, u32[]{:S(2)}) collective-permute-start(bf16[512,256]{1,0:T(8,128)(2,1)S(1)} %own.2.m0), channel_id=1, source_target_pairs={{0,6},{2,0},{4,2},{6,4},{1,7},{3,1},{5,3},{7,5},{8,14},{10,8},{12,... | collective-permute-start | bytes 786440 | tf_op jit(solution)/shard_map/ppermute | solution.py:504
  95.1 14.0 %collective-permute-start.12 = (bf16[512,256]{1,0:T(8,128)(2,1)S(1)}, bf16[512,256]{1,0:T(8,128)(2,1)S(1)}, u32[]{:S(2)}, u32[]{:S(2)}) collective-permute-start(bf16[512,256]{1,0:T(8,128)(2,1)S(1)} %own.2.m0), channel_id=1, source_target_pairs={{0,4},{2,6},{4,0},{6,2},{1,5},{3,7},{5,1},{7,3},{8,12},{10,14},{12... | collective-permute-start | bytes 786440 | tf_op jit(solution)/shard_map/ppermute | solution.py:504
  95.9 13.7 %collective-permute-start.13 = (bf16[512,256]{1,0:T(8,128)(2,1)S(1)}, bf16[512,256]{1,0:T(8,128)(2,1)S(1)}, u32[]{:S(2)}, u32[]{:S(2)}) collective-permute-start(bf16[512,256]{1,0:T(8,128)(2,1)S(1)} %own.2.m0), channel_id=1, source_target_pairs={{0,2},{2,4},{4,6},{6,0},{1,3},{3,5},{5,7},{7,1},{8,10},{10,12},{12... | collective-permute-start | bytes 786440 | tf_op jit(solution)/shard_map/ppermute | solution.py:504
  97.8 16.2 %collective-permute-start.28 = (bf16[512,256]{1,0:T(8,128)(2,1)S(1)}, bf16[512,256]{1,0:T(8,128)(2,1)S(1)}, u32[]{:S(2)}, u32[]{:S(2)}) collective-permute-start(bf16[512,256]{1,0:T(8,128)(2,1)S(1)} %own.3.m0), channel_id=1, source_target_pairs={{0,2},{2,4},{4,6},{6,0},{1,3},{3,5},{5,7},{7,1},{8,10},{10,12},{12... | collective-permute-start | bytes 786440 | tf_op jit(solution)/shard_map/ppermute | solution.py:504
  99.2 14.8 %collective-permute-start.14 = (bf16[512,256]{1,0:T(8,128)(2,1)S(1)}, bf16[512,256]{1,0:T(8,128)(2,1)S(1)}, u32[]{:S(2)}, u32[]{:S(2)}) collective-permute-start(bf16[512,256]{1,0:T(8,128)(2,1)S(1)} %own.2.m0), channel_id=1, source_target_pairs={{0,1},{1,0},{2,3},{3,2},{4,5},{5,4},{6,7},{7,6},{8,9},{9,8},{10,11... | collective-permute-start | bytes 786440 | tf_op jit(solution)/shard_map/ppermute | solution.py:508
  113.9 13.4 %collective-permute-start.29 = (bf16[512,256]{1,0:T(8,128)(2,1)S(1)}, bf16[512,256]{1,0:T(8,128)(2,1)S(1)}, u32[]{:S(2)}, u32[]{:S(2)}) collective-permute-start(bf16[512,256]{1,0:T(8,128)(2,1)S(1)} %own.3.m0), channel_id=1, source_target_pairs={{0,1},{1,0},{2,3},{3,2},{4,5},{5,4},{6,7},{7,6},{8,9},{9,8},{10,11... | collective-permute-start | bytes 786440 | tf_op jit(solution)/shard_map/ppermute | solution.py:508
  114.0 13.4 %collective-permute-start.30 = (bf16[512,256]{1,0:T(8,128)(2,1)S(1)}, bf16[512,256]{1,0:T(8,128)(2,1)S(1)}, u32[]{:S(2)}, u32[]{:S(2)}) collective-permute-start(bf16[512,256]{1,0:T(8,128)(2,1)S(1)} %collective-permute-done.26.m1), channel_id=1, source_target_pairs={{0,1},{1,0},{2,3},{3,2},{4,5},{5,4},{6,7},{7,6},{8,9},{9,8},{10,11... | collective-permute-start | bytes 786440 | tf_op jit(solution)/shard_map/ppermute | solution.py:508
  114.5 12.9 %collective-permute-start.31 = (bf16[512,256]{1,0:T(8,128)(2,1)S(1)}, bf16[512,256]{1,0:T(8,128)(2,1)}, u32[]{:S(2)}, u32[]{:S(2)}) collective-permute-start(bf16[512,256]{1,0:T(8,128)(2,1)S(1)} %collective-permute-done.27.m2), channel_id=1, source_target_pairs={{0,1},{1,0},{2,3},{3,2},{4,5},{5,4},{6,7},{7,6},{8,9},{9,8},{10,11... | collective-permute-start | bytes 786440 | tf_op jit(solution)/shard_map/ppermute | solution.py:508
  142.3 19.9 %collective-permute-start.34 = (bf16[512,256]{1,0:T(8,128)(2,1)S(1)}, bf16[512,256]{1,0:T(8,128)(2,1)S(1)}, u32[]{:S(2)}, u32[]{:S(2)}) collective-permute-start(bf16[512,256]{1,0:T(8,128)(2,1)S(1)} %get-tuple-element.82), channel_id=1, source_target_pairs={{0,4},{2,6},{4,0},{6,2},{1,5},{3,7},{5,1},{7,3},{8,12},{10,14},{12... | collective-permute-start | bytes 786440 | tf_op jit(solution)/shard_map/ppermute | solution.py:504
  144.4 16.2 %collective-permute-start.20 = (bf16[512,256]{1,0:T(8,128)(2,1)S(1)}, bf16[512,256]{1,0:T(8,128)(2,1)S(1)}, u32[]{:S(2)}, u32[]{:S(2)}) collective-permute-start(bf16[512,256]{1,0:T(8,128)(2,1)S(1)} %get-tuple-element.71), channel_id=1, source_target_pairs={{0,2},{2,4},{4,6},{6,0},{1,3},{3,5},{5,7},{7,1},{8,10},{10,12},{12... | collective-permute-start | bytes 786440 | tf_op jit(solution)/shard_map/ppermute | solution.py:504
  145.9 16.1 %collective-permute-start.21 = (bf16[512,256]{1,0:T(8,128)(2,1)S(1)}, bf16[512,256]{1,0:T(8,128)(2,1)S(1)}, u32[]{:S(2)}, u32[]{:S(2)}) collective-permute-start(bf16[512,256]{1,0:T(8,128)(2,1)S(1)} %get-tuple-element.72), channel_id=1, source_target_pairs={{0,6},{2,0},{4,2},{6,4},{1,7},{3,1},{5,3},{7,5},{8,14},{10,8},{12,... | collective-permute-start | bytes 786440 | tf_op jit(solution)/shard_map/ppermute | solution.py:504
  147.6 18.5 %collective-permute-start.35 = (bf16[512,256]{1,0:T(8,128)(2,1)S(1)}, bf16[512,256]{1,0:T(8,128)(2,1)S(1)}, u32[]{:S(2)}, u32[]{:S(2)}) collective-permute-start(bf16[512,256]{1,0:T(8,128)(2,1)S(1)} %get-tuple-element.83), channel_id=1, source_target_pairs={{0,2},{2,4},{4,6},{6,0},{1,3},{3,5},{5,7},{7,1},{8,10},{10,12},{12... | collective-permute-start | bytes 786440 | tf_op jit(solution)/shard_map/ppermute | solution.py:504
  150.2 16.6 %collective-permute-start.36 = (bf16[512,256]{1,0:T(8,128)(2,1)S(1)}, bf16[512,256]{1,0:T(8,128)(2,1)S(1)}, u32[]{:S(2)}, u32[]{:S(2)}) collective-permute-start(bf16[512,256]{1,0:T(8,128)(2,1)S(1)} %get-tuple-element.84), channel_id=1, source_target_pairs={{0,6},{2,0},{4,2},{6,4},{1,7},{3,1},{5,3},{7,5},{8,14},{10,8},{12,... | collective-permute-start | bytes 786440 | tf_op jit(solution)/shard_map/ppermute | solution.py:504
  (34 other events, 289.2 us)
Sparse Core Ops, SparseCore 0:
  11.2 79.3 all-gather.1
where the time goes:
time: 175 us
  waiting for transfers between devices  57.4 us (33%)
  starting transfers between devices  49.9 us (29%)
  Pallas kernels  39.7 us (23%)
  between operations  13.7 us (8%)
  local copies, waits for them, and re-layouts  11.8 us (7%)
  other arithmetic  2.1 us (1%)
    ppermute x24, waiting for transfers between devices, turn(): lax.ppermute(array, axis, [(i, (i + distance) % count) for i in range(cou...  56 us
    ppermute x24, starting transfers between devices, turn(): lax.ppermute(array, axis, [(i, (i + distance) % count) for i in range(cou...  43.1 us
    pallas_call x2, Pallas kernels, ffn_kernel(): pl.pallas_call(ffn_body, out_shape=(sds((4, count, COL), BF), sds((4, cou...  21.5 us
    unnamed x42, local copies, waits for them, and re-layouts  10.5 us
    pallas_call x1, Pallas kernels, state_kernel(): pl.pallas_call(state_body, out_shape=(sds((T, CH), BF), sds((T, 256), BF)...  5.34 us
    pallas_call x2, Pallas kernels, mix_kernel(): pl.pallas_call(functools.partial(mix_body, start, count), out_shape=(sds(...  5.24 us
    pallas_call x1, Pallas kernels, local_kernel(): pl.pallas_call(local_body, out_shape=(sds((T, CH), F32), sds((T, CH), F32...  4.59 us
    ppermute x1, starting transfers between devices, shards(): halo = lax.ppermute(tail, SP, [(i, i + 1) for i in range(15)])  3.59 us
  transfers between devices with their start and end apart: 38, of which 15 were waited for; matrix products, arithmetic and copies ran while one was open for 1% of the time, Pallas kernels for 22%

commit v1 on v0

--- a/solution.py
+++ b/solution.py
@@ -81,28 +81,28 @@
     return silu(total).astype(BF)
 
 
+def column(row):
+    own = lax.broadcasted_iota(jnp.int32, (HEADS, HEADS), 0) == lax.broadcasted_iota(
+        jnp.int32, (HEADS, HEADS), 1
+    )
+    spread_row = jnp.broadcast_to(row, (HEADS, HEADS))
+    return jnp.sum(jnp.where(own, spread_row, 0.0), axis=1, keepdims=True)
+
+
 def softplus(x):
     return jnp.maximum(x, 0.0) + jnp.log1p(jnp.exp(-jnp.abs(x)))
 
 
-def state_body(
-    content, pairs, halo, raw, spike, shift, fading, taps_c, taps_p,
-    values, maps, cum_out, tot_out, step_out, entering, payload,
-    ext_c, ext_p, factors, ends, carry,
+def decay_body(
+    raw, spike, shift, fading, skip, taps_c, taps_p,
+    cum_out, tot_out, step_out, factors, ends, total_out, skip_out, taps_c_out, taps_p_out,
 ):
-    ext_c[0:HALO] = halo[:, 0:CH]
-    ext_p[0:HALO] = halo[:, CH : CH + 256]
-    ext_c[HALO : HALO + T] = content[...]
-    ext_p[HALO : HALO + T] = pairs[...]
-    carry[...] = jnp.zeros((ST, CH), F32)
     row = lax.broadcasted_iota(jnp.int32, (BLK, BLK), 0)
     col = lax.broadcasted_iota(jnp.int32, (BLK, BLK), 1)
     triu = (row <= col).astype(F32)
-    tc = taps_c[...].astype(F32)
-    tp = taps_p[...].astype(F32)
-    step = softplus(raw[...].astype(F32) + shift[...])
+    step = softplus(raw[...].astype(F32) + column(shift[...]))
     step_out[...] = step
-    log = -jnp.exp(fading[...]) * step + spike[...]
+    log = -jnp.exp(column(fading[...])) * step + spike[...]
     cum = hi_dot(
         jnp.concatenate([log[:, b * BLK : (b + 1) * BLK] for b in range(NB)], axis=0), triu
     )
@@ -116,6 +116,48 @@
         factors[b] = step[:, lanes] * jnp.exp(end - here)
         ends[b] = jnp.broadcast_to(jnp.exp(end), (HEADS, BLK))
         prior = prior + end
+    total_out[...] = spread(jnp.broadcast_to(prior, (HEADS, BLK)), 64, 3)[0:8]
+    skip_out[...] = spread(jnp.broadcast_to(column(skip[...]), (HEADS, BLK)), 64, 3)[0:8]
+    taps_c_out[0:4, :] = taps_c[...].astype(F32)
+    wide = taps_p[...].astype(F32)
+    taps_p_out[0:4, 0:ST] = wide[:, 0, :]
+    taps_p_out[0:4, ST : 2 * ST] = wide[:, 1, :]
+
+
+def decay_kernel(*args):
+    return pl.pallas_call(
+        decay_body,
+        out_shape=(
+            sds((HEADS, T), F32),
+            sds((HEADS, T), F32),
+            sds((HEADS, T), F32),
+            sds((NB, HEADS, BLK), F32),
+            sds((NB, HEADS, BLK), F32),
+            sds((8, CH), F32),
+            sds((8, CH), F32),
+            sds((8, CH), F32),
+            sds((8, 256), F32),
+        ),
+        grid=(1,),
+        in_specs=[whole(a.shape) for a in args],
+        out_specs=(VMEM,) * 9,
+        compiler_params=params(8),
+        name="decay",
+    )(*in_hbm(*args))
+
+
+def state_body(
+    content, pairs, halo, factors, ends, total, taps_c, taps_p,
+    values, maps, entering, payload,
+    ext_c, ext_p, carry,
+):
+    ext_c[0:HALO] = halo[:, 0:CH]
+    ext_p[0:HALO] = halo[:, CH : CH + 256]
+    ext_c[HALO : HALO + T] = content[...]
+    ext_p[HALO : HALO + T] = pairs[...]
+    carry[...] = jnp.zeros((ST, CH), F32)
+    tc = taps_c[...]
+    tp = taps_p[...]
 
     def block(b, _):
         at = pl.multiple_of(b * BLK, BLK)
@@ -134,11 +176,10 @@
         carry[...] = old * spread(ends[b], 64, 2) + added
         return 0
 
-    lax.fori_loop(0, NB, block, 0, unroll=2)
+    lax.fori_loop(0, NB, block, 0, unroll=4)
     payload[0:ST, :] = carry[...].astype(BF)
-    total = spread(jnp.broadcast_to(prior, (HEADS, BLK)), 64, 3)[0:8]
-    high = total.astype(BF)
-    low = (total - high.astype(F32)).astype(BF)
+    high = total[...].astype(BF)
+    low = (total[...] - high.astype(F32)).astype(BF)
     payload[ST : ST + LOGROWS, :] = jnp.concatenate([high, low], axis=0)
 
 
@@ -148,22 +189,17 @@
         out_shape=(
             sds((T, CH), BF),
             sds((T, 256), BF),
-            sds((HEADS, T), F32),
-            sds((HEADS, T), F32),
-            sds((HEADS, T), F32),
             sds((NB, ST, CH), BF),
             sds((ST + LOGROWS, CH), BF),
         ),
-        in_specs=[VMEM] * 9,
-        out_specs=(VMEM,) * 7,
+        in_specs=[VMEM] * 8,
+        out_specs=(VMEM,) * 4,
         scratch_shapes=[
             pltpu.VMEM((T + HALO, CH), BF),
             pltpu.VMEM((T + HALO, 256), BF),
-            pltpu.VMEM((NB, HEADS, BLK), F32),
-            pltpu.VMEM((NB, HEADS, BLK), F32),
             pltpu.VMEM((ST, CH), F32),
         ],
-        compiler_params=params(16),
+        compiler_params=params(12),
         name="state",
     )(*args)
 
@@ -173,7 +209,7 @@
     col = lax.broadcasted_iota(jnp.int32, (BLK, BLK), 1)
     causal = col <= row
     low = lane_low()
-    gain = spread(jnp.broadcast_to(skip[...], (HEADS, BLK)), 64, 3)
+    gain = skip[0:1, :]
 
     def block(b, _):
         rows = block_lanes(b)
@@ -238,7 +274,7 @@
         grid=(1,),
         in_specs=[
             pl.BlockSpec((HALO, CH), lambda _: (last, 0)),
-            pl.BlockSpec((HALO, 256), lambda _: (last, 0)),
+            pl.BlockSpec((HALO, 256), lambda _: (0, 0)),
         ],
         out_specs=VMEM,
         compiler_params=params(4),
@@ -316,7 +352,7 @@
 
 
 def mix_body(
-    start, count, order, incoming, local, maps, tot, gate, gain, blend, send, keep, mixed
+    start, count, order, incoming, local, maps, tot, gate, gain, blend, send, mixed
 ):
     rescale = gain[...]
 
@@ -331,22 +367,60 @@
         return 0
 
     lax.fori_loop(0, count // BLK, block, 0, unroll=2)
-    for half, target in ((1, send), (0, keep)):
-        for k in range(4):
-            cols = pl.ds(pl.multiple_of(order[half * 4 + k] * COL, COL), COL)
-            target[k] = jnp.dot(
-                mixed[...], blend[:, cols], preferred_element_type=F32
-            ).astype(BF)
+    project(order, 4, mixed, blend, 0, send)
+
+
+def project(order, first, rows, weights, at, target):
+    height = rows.shape[1]
+    for k in range(4):
+        cols = pl.ds(pl.multiple_of(order[first + k] * COL, COL), COL)
+        target[k] = jnp.dot(
+            rows[...], weights[at : at + height, cols], preferred_element_type=F32
+        ).astype(BF)
+
+
+def cols_body(col, arriving, out):
+    out[...] = arriving[...]
+
+
+def cols_kernel(col, arriving):
+    return pl.pallas_call(
+        cols_body,
+        out_shape=sds((T, COL), BF),
+        grid_spec=pltpu.PrefetchScalarGridSpec(
+            num_scalar_prefetch=1,
+            grid=(1,),
+            in_specs=[pl.BlockSpec((T, COL), lambda _, col: (0, col[0]))],
+            out_specs=VMEM,
+        ),
+        compiler_params=params(4),
+        name="cols",
+    )(col, pltpu.with_memory_space_constraint(arriving, pltpu.HBM))
+
+
+def keep_body(at, order, rows, weights, target):
+    project(order, 0, rows, weights, at, target)
+
+
+def keep_kernel(order, rows, weights, at):
+    return pl.pallas_call(
+        functools.partial(keep_body, at),
+        out_shape=sds((4, rows.shape[0], COL), BF),
+        in_specs=[SMEM, VMEM, VMEM],
+        out_specs=VMEM,
+        compiler_params=params(8),
+        cost_estimate=pl.CostEstimate(flops=1_000_000_000, transcendentals=0, bytes_accessed=6_000_000),
+        name="keep",
+    )(order, rows, weights)
 
 
 def mix_kernel(start, count, order, *args):
     return pl.pallas_call(
         functools.partial(mix_body, start, count),
-        out_shape=(sds((4, count, COL), BF), sds((4, count, COL), BF)),
+        out_shape=(sds((4, count, COL), BF), sds((count, CH), BF)),
         in_specs=[SMEM] + [VMEM] * 7,
         out_specs=(VMEM,) * 2,
-        scratch_shapes=[pltpu.VMEM((count, CH), BF)],
-        compiler_params=params(16),
+        compiler_params=params(8),
         cost_estimate=pl.CostEstimate(flops=3_000_000_000, transcendentals=0, bytes_accessed=6_000_000),
         name="mix",
     )(order, *args)
@@ -438,17 +512,7 @@
     return lax.rsqrt(jnp.sum(total, axis=1, keepdims=True) * (1.0 / D) + EPS)
 
 
-def ffn_body(
-    order, pack, gain, m0, m1, m2, m3, n0, n1, n2, n3, send, keep, weights, rows_x, hid, sem
-):
-    copies = [
-        pltpu.make_async_copy(pack.at[j], weights.at[:, pl.ds(j * 128, 128)], sem)
-        for j in range(16)
-    ]
-    for copy in copies:
-        copy.start()
-    refs = (m0, m1, m2, m3, n0, n1, n2, n3)
-
+def ffn_rows(order, gain, refs, rows_x):
     def norm(b, _):
         rows = pl.ds(pl.multiple_of(b * NORM_ROWS, NORM_ROWS), NORM_ROWS)
         scale = row_scale([r[rows, :].astype(F32) for r in refs])
@@ -458,8 +522,9 @@
         return 0
 
     lax.fori_loop(0, rows_x.shape[0] // NORM_ROWS, norm, 0)
-    for copy in copies:
-        copy.wait()
+
+
+def ffn_hidden(weights, rows_x, hid):
     over_k = (((1,), (1,)), ((), ()))
     gate = lax.dot_general(
         rows_x[...], weights[0:FF, :], over_k, preferred_element_type=F32
@@ -468,35 +533,93 @@
         rows_x[...], weights[FF : 2 * FF, :], over_k, preferred_element_type=F32
     )
     hid[...] = (silu(gate) * up).astype(BF)
-    for half, target in ((1, send), (0, keep)):
-
-        def project(k, _, half=half, target=target):
-            cols = pl.ds(pl.multiple_of(order[half * 4 + k] * COL, COL), COL)
-            target[k] = jnp.dot(
-                hid[...], weights[2 * FF :, cols], preferred_element_type=F32
-            ).astype(BF)
-            return 0
-
-        lax.fori_loop(0, 4, project, 0)
-
-
-def ffn_kernel(order, pack, gain, mine, theirs):
-    count = mine[0].shape[0]
-    return pl.pallas_call(
-        ffn_body,
-        out_shape=(sds((4, count, COL), BF), sds((4, count, COL), BF)),
-        in_specs=[SMEM, pl.BlockSpec(memory_space=pltpu.HBM)] + [VMEM] * 9,
-        out_specs=(VMEM,) * 2,
-        scratch_shapes=[
-            pltpu.VMEM((PACK, D), BF),
-            pltpu.VMEM((count, D), BF),
-            pltpu.VMEM((count, FF), BF),
-            pltpu.SemaphoreType.DMA,
-        ],
-        compiler_params=params(24),
+
+
+def ffn_first_body(
+    order, pack, gain, m0, m1, m2, m3, n0, n1, n2, n3, send, hid, weights, rows_x, sems
+):
+    def copies(part, at, size):
+        return [
+            pltpu.make_async_copy(
+                pack.at[j, pl.ds(at, size), :],
+                weights.at[pl.ds(at, size), pl.ds(j * 128, 128)],
+                sems.at[part],
+            )
+            for j in range(16)
+        ]
+
+    up, down = copies(0, 0, 2 * FF), copies(1, 2 * FF, FF)
+    for copy in up + down:
+        copy.start()
+    ffn_rows(order, gain, (m0, m1, m2, m3, n0, n1, n2, n3), rows_x)
+    for copy in up:
+        copy.wait()
+    ffn_hidden(weights, rows_x, hid)
+    for copy in down:
+        copy.wait()
+    project(order, 4, hid, weights, 2 * FF, send)
+
+
+def ffn_next_body(
+    order, weights, gain, m0, m1, m2, m3, n0, n1, n2, n3, send, hid, rows_x
+):
+    ffn_rows(order, gain, (m0, m1, m2, m3, n0, n1, n2, n3), rows_x)
+    ffn_hidden(weights, rows_x, hid)
+    project(order, 4, hid, weights, 2 * FF, send)
+
+
+def ffn_kernel(order, weights, gain, pieces, first):
+    count = pieces[0].shape[0]
+    shapes = (sds((4, count, COL), BF), sds((count, FF), BF))
+    scratch = [pltpu.VMEM((count, D), BF)]
+    if first:
+        shapes += (sds((PACK, D), BF),)
+        scratch.append(pltpu.SemaphoreType.DMA((2,)))
+        (weights,) = in_hbm(weights)
+    return pl.pallas_call(
+        ffn_first_body if first else ffn_next_body,
+        out_shape=shapes,
+        in_specs=[SMEM, HBM if first else VMEM] + [VMEM] * (len(pieces) + 1),
+        out_specs=(VMEM,) * len(shapes),
+        scratch_shapes=scratch,
+        compiler_params=params(14),
         cost_estimate=pl.CostEstimate(flops=9_000_000_000, transcendentals=0, bytes_accessed=12_000_000),
         name="ffn",
-    )(order, pack, gain, *mine, *theirs)
+    )(order, weights, gain, *pieces)
+
+
+HBM = pl.BlockSpec(memory_space=pltpu.HBM)
+
+
+def pack_body(gate, up, down, out, sem):
+    copies = [
+        pltpu.make_async_copy(part, out.at[pl.ds(i * FF, FF), :], sem)
+        for i, part in enumerate((gate, up, down))
+    ]
+    for copy in copies:
+        copy.start()
+    for copy in copies:
+        copy.wait()
+
+
+def whole(shape):
+    return pl.BlockSpec(shape, lambda _: (0,) * len(shape))
+
+
+def in_hbm(*arrays):
+    return tuple(pltpu.with_memory_space_constraint(a, pltpu.HBM) for a in arrays)
+
+
+def pack_kernel(*parts):
+    return pl.pallas_call(
+        pack_body,
+        out_shape=sds((PACK, 128), BF),
+        in_specs=[HBM] * 3,
+        out_specs=VMEM,
+        scratch_shapes=[pltpu.SemaphoreType.DMA],
+        compiler_params=params(4),
+        name="pack",
+    )(*in_hbm(*parts))
 
 
 def turn(array, axis, distance):
@@ -523,51 +646,65 @@
 ):
     x, c = lax.axis_index("x"), lax.axis_index("c")
     y, z = lax.axis_index("y"), lax.axis_index("z")
+    chips = (x + jnp.arange(4, dtype=jnp.int32)) % 4
+    order = jnp.concatenate([chips * 2 + c, chips * 2 + (1 - c)]).astype(jnp.int32)
+    first_col = (2 * x + c).reshape(1)
+    y, z = y.reshape(1), z.reshape(1)
+    pack = pack_kernel(w_gate.T, w_up.T, w_down)
+    gathered = lax.all_gather(pack, SP, axis=0, tiled=True).reshape(16, PACK, 128)
+    linked_tail = linked[T - HALO :].reshape(HALO, 256)
+    content_tail, linked_tail, pack = lax.optimization_barrier((content, linked_tail, pack))
+    tail = tail_kernel(pltpu.with_memory_space_constraint(content_tail, pltpu.HBM), linked_tail)
+    tail, order, first_col, y, z, linked = lax.optimization_barrier(
+        (tail, order, first_col, y, z, linked)
+    )
     pairs = linked.reshape(T, 256)
-    tail = tail_kernel(content, pairs)
-    tail, w_gate, w_up, w_down = lax.optimization_barrier((tail, w_gate, w_up, w_down))
     halo = lax.ppermute(tail, SP, [(i, i + 1) for i in range(15)])
-    pack = jnp.concatenate([w_gate.T, w_up.T, w_down], axis=0)
-    pack = lax.all_gather(pack, SP, axis=0, tiled=True).reshape(16, PACK, 128)
-    values, maps, cum, tot, step, entering, payload = state_kernel(
-        content, pairs, halo, raw.T, spike.T, shift.reshape(HEADS, 1),
-        fading.reshape(HEADS, 1), taps_c, taps_p.reshape(4, 256),
+    cum, tot, step, factors, ends, total, skip, taps_c, taps_p = decay_kernel(
+        raw.T, spike.T, shift.reshape(1, HEADS), fading.reshape(1, HEADS),
+        skip.reshape(1, HEADS), taps_c, taps_p.reshape(4, 2, ST),
+    )
+    values, maps, entering, payload = state_kernel(
+        content, pairs, halo, factors, ends, total, taps_c, taps_p
     )
     line = [payload] + [turn(payload, "y", d) for d in (1, 2, 3)]
     local, opened = local_kernel(
-        values, maps, cum, step, entering, skip.reshape(HEADS, 1), gate, blender
-    )
-    local = pltpu.with_memory_space_constraint(local, pltpu.VMEM)
-    opened = pltpu.with_memory_space_constraint(opened, pltpu.VMEM)
-    mine_cols = lax.dynamic_slice(arriving, (0, (2 * x + c) * COL), (T, COL))
-    payload_z, prefix, ahead = line_kernel(y.reshape(1), line)
+        values, maps, cum, step, entering, skip, gate, blender
+    )
+    mine_cols = cols_kernel(first_col, arriving)
+    payload_z, prefix, ahead = line_kernel(y, line)
     lines = [payload_z] + [turn(payload_z, "z", d) for d in (1, 2, 3)]
-    steps = jnp.arange(4, dtype=jnp.int32)
-    chips = (x + steps) % 4
-    order = jnp.concatenate([chips * 2 + c, chips * 2 + (1 - c)]).astype(jnp.int32)
-    incoming = incoming_kernel(z.reshape(1), lines, prefix, ahead)
+    incoming = incoming_kernel(z, lines, prefix, ahead)
     gain = norm_gain.reshape(1, D)
     mix_args = (incoming, local, maps, tot, opened, cluster_gain.reshape(1, CH), blender)
-    spans = ((0, FIRST), (FIRST, SECOND))
-    owns, lasts = [], []
-    sent, kept = [], []
-    for start, count in spans:
-        send, keep = mix_kernel(start, count, order, *mix_args)
-        sent.append(swap(send))
-        kept.append(keep)
-    for i, (start, count) in enumerate(spans):
-        parts = pair_kernel(kept[i], sent[i])
-        parts = reduce_chips(parts)
-        owns.append(own_kernel(start, parts, mine_cols))
-    pack = pltpu.with_memory_space_constraint(pack, pltpu.HBM)
-    for i, (start, count) in enumerate(spans):
-        mine = gather_chips(owns[i])
-        theirs = tuple(swap(piece) for piece in mine)
-        send, keep = ffn_kernel(order, pack, gain, mine, theirs)
-        got = swap(send)
-        parts = pair_kernel(keep, got)
-        lasts.append(reduce_chips(parts))
-    return join_kernel(last_kernel(owns[0], lasts[0]), owns[1], lasts[1])
+    (at_a, rows_a), (at_b, rows_b) = (0, FIRST), (FIRST, SECOND)
+    send_a, mixed_a = mix_kernel(at_a, rows_a, order, *mix_args)
+    got_a = swap(send_a)
+    keep_a = keep_kernel(order, mixed_a, blender, 0)
+    parts = pair_kernel(keep_a, got_a)
+    parts = reduce_chips(parts)
+    own_a = own_kernel(at_a, parts, mine_cols)
+    mine_a = gather_chips(own_a)
+    send_b, mixed_b = mix_kernel(at_b, rows_b, order, *mix_args)
+    got_b = swap(send_b)
+    keep_b = keep_kernel(order, mixed_b, blender, 0)
+    parts = pair_kernel(keep_b, got_b)
+    parts = reduce_chips(parts)
+    own_b = own_kernel(at_b, parts, mine_cols)
+    mine_b = gather_chips(own_b)
+    theirs_a = tuple(swap(piece) for piece in mine_a)
+    send, hid, weights = ffn_kernel(order, gathered, gain, (*mine_a, *theirs_a), True)
+    got = swap(send)
+    keep = keep_kernel(order, hid, weights, 2 * FF)
+    parts = pair_kernel(keep, got)
+    last_a = reduce_chips(parts)
+    theirs_b = tuple(swap(piece) for piece in mine_b)
+    send, hid = ffn_kernel(order, weights, gain, (*mine_b, *theirs_b), False)
+    got = swap(send)
+    keep = keep_kernel(order, hid, weights, 2 * FF)
+    parts = pair_kernel(keep, got)
+    last_b = reduce_chips(parts)
+    return join_kernel(last_kernel(own_a, last_a), own_b, last_b)
 
 
 def solution(mesh):

time: 175 us -> 163 us (0.931)
  local copies, waits for them, and re-layouts: 11.8 us -> 3.6 us
  starting transfers between devices: 49.9 us -> 44.7 us
  other arithmetic: 2.1 us -> 0.09 us
    unnamed x42 -> x16, local copies, waits for them, and re-layouts: 10.5 us -> 2.81 us
    ppermute x24, starting transfers between devices: 43.1 us -> 38.3 us  [turn(): lax.ppermute(array, axis, [(i, (i + distance) % count) for i in range(cou...]
    pallas_call x2 -> x9, Pallas kernels: 21.5 us -> 24.4 us  [the longest x2 14.1 us: ffn_kernel(): pl.pallas_call(ffn_first_body if first else ffn_next_body, out_shape=shap...]
    ppermute x24, waiting for transfers between devices: 56 us -> 58.1 us  [turn(): lax.ppermute(array, axis, [(i, (i + distance) % count) for i in range(cou...]
    concatenate x1 -> x0, other arithmetic: 2.02 us -> none  [shards(): pack = jnp.concatenate([w_gate.T, w_up.T, w_down], axis=0)]
  transfers between devices with their start and end apart: 38 -> 38, of which waited for: 15 -> 18; matrix products, arithmetic and copies ran while one was open for 1% -> 1% of each run, Pallas kernels for 22% -> 24%
where the time goes in v1:
time: 163 us; the launch traced here: 162 us
  waiting for transfers between devices  58.8 us (36%)
  starting transfers between devices  44.7 us (27%)
  Pallas kernels  41.2 us (25%)
  between operations  13.7 us (8%)
  local copies, waits for them, and re-layouts  3.6 us (2%)
    ppermute x24, waiting for transfers between devices, turn(): lax.ppermute(array, axis, [(i, (i + distance) % count) for i in range(cou...  58.1 us
    ppermute x24, starting transfers between devices, turn(): lax.ppermute(array, axis, [(i, (i + distance) % count) for i in range(cou...  38.3 us
    pallas_call x2, Pallas kernels, ffn_kernel(): pl.pallas_call(ffn_first_body if first else ffn_next_body, out_shape=shap...  14.1 us
    pallas_call x4, Pallas kernels, keep_kernel(): pl.pallas_call(functools.partial(keep_body, at), out_shape=sds((4, rows.s...  5.6 us
    pallas_call x1, Pallas kernels, state_kernel(): pl.pallas_call(state_body, out_shape=(sds((T, CH), BF), sds((T, 256), BF)...  4.61 us
    pallas_call x1, Pallas kernels, local_kernel(): pl.pallas_call(local_body, out_shape=(sds((T, CH), F32), sds((T, CH), F32...  4.3 us
    pallas_call x2, Pallas kernels, mix_kernel(): pl.pallas_call(functools.partial(mix_body, start, count), out_shape=(sds(...  4.16 us
    ppermute x1, starting transfers between devices, shards(): halo = lax.ppermute(tail, SP, [(i, i + 1) for i in range(15)])  3.58 us
  transfers between devices with their start and end apart: 38, of which 18 were waited for; matrix products, arithmetic and copies ran while one was open for 1% of the time, Pallas kernels for 24%

profile of v1, /device:TPU:0, one launch (start us, length us, event | category | flops | bytes accessed | tf_op | source)
XLA Modules:
  0.0 162.1 jit_solution(10985259941231263498)
XLA Ops:
  10.3 3.6 %collective-permute-start = (bf16[16,768]{1,0:T(8,128)(2,1)S(1)}, bf16[16,768]{1,0:T(8,128)(2,1)S(1)}, u32[]{:S(2)}, u32[]{:S(2)}) collective-permute-start(bf16[16,768]{1,0:T(8,128)(2,1)S(1)} %tail.1), channel_id=1, source_target_pairs={{0,8},{8,16},{16,24},{24,32},{32,40},{40,48},{48,56},{56,64},{64,7... | collective-permute-start | bytes 73736 | tf_op jit(solution)/shard_map/ppermute | solution.py:662
  16.5 4.6 %state.1 = (bf16[1024,512]{1,0:T(8,128)(2,1)S(1)}, bf16[1024,256]{1,0:T(8,128)(2,1)S(1)}, bf16[8,128,512]{2,1,0:T(8,128)(2,1)S(1)}, bf16[144,512]{1,0:T(8,128)(2,1)S(1)}) custom-call(bf16[1024,512]{1,0:T(8,128)(2,1)S(1)} %copy-done, bf16[1024,256]{1,0:T(8,128)(2,1)S(1)} %bitcast.24, bf16[16,768]{1,0:T(8,128)(2,1)S(1)} %collective-permute-done.halo, ...), custom_call_target="tpu_custom_call" | custom-call | tf_op jit(solution)/shard_map/state/pallas_call | solution.py:187
  21.1 3.1 %collective-permute-start.3 = (bf16[144,512]{1,0:T(8,128)(2,1)S(1)}, bf16[144,512]{1,0:T(8,128)(2,1)S(1)}, u32[]{:S(2)}, u32[]{:S(2)}) collective-permute-start(bf16[144,512]{1,0:T(8,128)(2,1)S(1)} %get-tuple-element.68.r0), channel_id=1, source_target_pairs={{0,24},{8,0},{16,8},{24,16},{1,25},{9,1},{17,9},{25,17},{2,26},{10... | collective-permute-start | bytes 442376 | tf_op jit(solution)/shard_map/ppermute | solution.py:627
  25.5 7.5 %collective-permute-done.3.r3 = bf16[144,512]{1,0:T(8,128)(2,1)S(1)} collective-permute-done((bf16[144,512]{1,0:T(8,128)(2,1)S(1)}, bf16[144,512]{1,0:T(8,128)(2,1)S(1)}, u32[]{:S(2)}, u32[]{:S(2)}) %collective-permute-start.3) | collective-permute-done | bytes 147488 | tf_op jit(solution)/shard_map/ppermute | solution.py:627
  33.0 2.5 %collective-permute-done.2.r2 = bf16[144,512]{1,0:T(8,128)(2,1)S(1)} collective-permute-done((bf16[144,512]{1,0:T(8,128)(2,1)S(1)}, bf16[144,512]{1,0:T(8,128)(2,1)S(1)}, u32[]{:S(2)}, u32[]{:S(2)}) %collective-permute-start.2) | collective-permute-done | bytes 147488 | tf_op jit(solution)/shard_map/ppermute | solution.py:627
  35.6 2.4 %collective-permute-done.1.r1 = bf16[144,512]{1,0:T(8,128)(2,1)S(1)} collective-permute-done((bf16[144,512]{1,0:T(8,128)(2,1)S(1)}, bf16[144,512]{1,0:T(8,128)(2,1)S(1)}, u32[]{:S(2)}, u32[]{:S(2)}) %collective-permute-start.1) | collective-permute-done | bytes 147488 | tf_op jit(solution)/shard_map/ppermute | solution.py:627
  38.2 3.7 %collective-permute-start.6 = (bf16[144,512]{1,0:T(8,128)(2,1)S(1)}, bf16[144,512]{1,0:T(8,128)(2,1)S(1)}, u32[]{:S(2)}, u32[]{:S(2)}) collective-permute-start(bf16[144,512]{1,0:T(8,128)(2,1)S(1)} %get-tuple-element.69.q0), channel_id=1, source_target_pairs={{0,96},{32,0},{64,32},{96,64},{1,97},{33,1},{65,33},{97,65},{2,98}... | collective-permute-start | bytes 442376 | tf_op jit(solution)/shard_map/ppermute | solution.py:627
  43.5 4.3 %local.1 = (f32[1024,512]{1,0:T(8,128)S(1)}, f32[1024,512]{1,0:T(8,128)S(1)}) custom-call(bf16[1024,512]{1,0:T(8,128)(2,1)S(1)} %get-tuple-element.72.values, bf16[1024,256]{1,0:T(8,128)(2,1)S(1)} %get-tuple-element.73.maps, f32[8,1024]{1,0:T(8,128)S(1)} %get-tuple-element.74.cum_in, f32[8,1024]{1,0:T(8,128)S(1)} %get-tuple-element.75.step_in, ...), custom_call_target="tpu_custom_call" | custom-call | flops 6000000000 | bytes 6000000 | tf_op jit(solution)/shard_map/local/pallas_call | solution.py:253
  57.8 3.1 %collective-permute-start.23 = (bf16[512,256]{1,0:T(8,128)(2,1)S(1)}, bf16[512,256]{1,0:T(8,128)(2,1)S(1)}, u32[]{:S(2)}, u32[]{:S(2)}) collective-permute-start(bf16[512,256]{1,0:T(8,128)(2,1)S(1)} %get-tuple-element.98), channel_id=1, source_target_pairs={{0,4},{2,6},{4,0},{6,2},{1,5},{3,7},{5,1},{7,3},{8,12},{10,14},{12... | collective-permute-start | bytes 786440 | tf_op jit(solution)/shard_map/ppermute | solution.py:627
  62.9 2.7 %collective-permute-start.25 = (bf16[512,256]{1,0:T(8,128)(2,1)S(1)}, bf16[512,256]{1,0:T(8,128)(2,1)S(1)}, u32[]{:S(2)}, u32[]{:S(2)}) collective-permute-start(bf16[512,256]{1,0:T(8,128)(2,1)S(1)} %get-tuple-element.100), channel_id=1, source_target_pairs={{0,6},{2,0},{4,2},{6,4},{1,7},{3,1},{5,3},{7,5},{8,14},{10,8},{12,... | collective-permute-start | bytes 786440 | tf_op jit(solution)/shard_map/ppermute | solution.py:627
  68.6 2.8 %collective-permute-start.10 = (bf16[512,256]{1,0:T(8,128)(2,1)S(1)}, bf16[512,256]{1,0:T(8,128)(2,1)S(1)}, u32[]{:S(2)}, u32[]{:S(2)}) collective-permute-start(bf16[512,256]{1,0:T(8,128)(2,1)S(1)} %get-tuple-element.86), channel_id=1, source_target_pairs={{0,6},{2,0},{4,2},{6,4},{1,7},{3,1},{5,3},{7,5},{8,14},{10,8},{12,... | collective-permute-start | bytes 786440 | tf_op jit(solution)/shard_map/ppermute | solution.py:627
  72.4 5.8 %collective-permute-done.24.f2 = bf16[512,256]{1,0:T(8,128)(2,1)S(1)} collective-permute-done((bf16[512,256]{1,0:T(8,128)(2,1)S(1)}, bf16[512,256]{1,0:T(8,128)(2,1)S(1)}, u32[]{:S(2)}, u32[]{:S(2)}) %collective-permute-start.24) | collective-permute-done | bytes 262176 | tf_op jit(solution)/shard_map/ppermute | solution.py:627
  78.5 4.7 %collective-permute-start.27 = (bf16[512,256]{1,0:T(8,128)(2,1)S(1)}, bf16[512,256]{1,0:T(8,128)(2,1)S(1)}, u32[]{:S(2)}, u32[]{:S(2)}) collective-permute-start(bf16[512,256]{1,0:T(8,128)(2,1)S(1)} %own.3.m0), channel_id=1, source_target_pairs={{0,4},{2,6},{4,0},{6,2},{1,5},{3,7},{5,1},{7,3},{8,12},{10,14},{12... | collective-permute-start | bytes 786440 | tf_op jit(solution)/shard_map/ppermute | solution.py:627
  87.3 2.6 %collective-permute-start.12 = (bf16[512,256]{1,0:T(8,128)(2,1)S(1)}, bf16[512,256]{1,0:T(8,128)(2,1)S(1)}, u32[]{:S(2)}, u32[]{:S(2)}) collective-permute-start(bf16[512,256]{1,0:T(8,128)(2,1)S(1)} %own.2.m0), channel_id=1, source_target_pairs={{0,4},{2,6},{4,0},{6,2},{1,5},{3,7},{5,1},{7,3},{8,12},{10,14},{12... | collective-permute-start | bytes 786440 | tf_op jit(solution)/shard_map/ppermute | solution.py:627
  90.5 4.5 %collective-permute-done.28.m3 = bf16[512,256]{1,0:T(8,128)(2,1)S(1)} collective-permute-done((bf16[512,256]{1,0:T(8,128)(2,1)S(1)}, bf16[512,256]{1,0:T(8,128)(2,1)S(1)}, u32[]{:S(2)}, u32[]{:S(2)}) %collective-permute-start.28) | collective-permute-done | bytes 262176 | tf_op jit(solution)/shard_map/ppermute | solution.py:627
  96.8 5.4 %collective-permute-done.13.m3 = bf16[512,256]{1,0:T(8,128)(2,1)S(1)} collective-permute-done((bf16[512,256]{1,0:T(8,128)(2,1)S(1)}, bf16[512,256]{1,0:T(8,128)(2,1)S(1)}, u32[]{:S(2)}, u32[]{:S(2)}) %collective-permute-start.13) | collective-permute-done | bytes 262176 | tf_op jit(solution)/shard_map/ppermute | solution.py:627
  102.2 4.8 %collective-permute-done.12.m2 = bf16[512,256]{1,0:T(8,128)(2,1)S(1)} collective-permute-done((bf16[512,256]{1,0:T(8,128)(2,1)S(1)}, bf16[512,256]{1,0:T(8,128)(2,1)S(1)}, u32[]{:S(2)}, u32[]{:S(2)}) %collective-permute-start.12) | collective-permute-done | bytes 262176 | tf_op jit(solution)/shard_map/ppermute | solution.py:627
  110.6 7.7 %ffn.2 = (bf16[4,512,256]{2,1,0:T(8,128)(2,1)S(1)}, bf16[512,704]{1,0:T(8,128)(2,1)S(1)}, bf16[2112,2048]{1,0:T(8,128)(2,1)S(1)}) custom-call(s32[8]{0:T(128)S(1)} %pad_add_fusion.order, bf16[16,2112,128]{2,1,0:T(8,128)(2,1)} %bitcast.40, f32[1,2048]{1,0:T(1,128)S(1)} %bitcast.26, bf16[512,256]{1,0:T(8,128)(2,1)S(1)} %own.2.m0, ...), custom_call_target="tpu_custom_call" | custom-call | flops 8999999488 | bytes 12000000 | tf_op jit(solution)/shard_map/ffn/pallas_call | solution.py:579
  118.8 6.4 %ffn.3 = (bf16[4,512,256]{2,1,0:T(8,128)(2,1)S(1)}, bf16[512,704]{1,0:T(8,128)(2,1)S(1)}) custom-call(s32[8]{0:T(128)S(1)} %pad_add_fusion.order, bf16[2112,2048]{1,0:T(8,128)(2,1)S(1)} %get-tuple-element.89.weights, f32[1,2048]{1,0:T(1,128)S(1)} %bitcast.27, bf16[512,256]{1,0:T(8,128)(2,1)S(1)} %own.3.m0, bf16[512,256]{1,0:T(8,128)(2,1)S(1)} %collective-permute-done.26.m1, ...), custom_call_target="tpu_custom_call" | custom-call | flops 8999999488 | bytes 12000000 | tf_op jit(solution)/shard_map/ffn/pallas_call | solution.py:579
  127.5 3.2 %collective-permute-start.19 = (bf16[512,256]{1,0:T(8,128)(2,1)S(1)}, bf16[512,256]{1,0:T(8,128)(2,1)S(1)}, u32[]{:S(2)}, u32[]{:S(2)}) collective-permute-start(bf16[512,256]{1,0:T(8,128)(2,1)S(1)} %get-tuple-element.92), channel_id=1, source_target_pairs={{0,4},{2,6},{4,0},{6,2},{1,5},{3,7},{5,1},{7,3},{8,12},{10,14},{12... | collective-permute-start | bytes 786440 | tf_op jit(solution)/shard_map/ppermute | solution.py:627
  133.6 2.6 %collective-permute-start.21 = (bf16[512,256]{1,0:T(8,128)(2,1)S(1)}, bf16[512,256]{1,0:T(8,128)(2,1)S(1)}, u32[]{:S(2)}, u32[]{:S(2)}) collective-permute-start(bf16[512,256]{1,0:T(8,128)(2,1)S(1)} %get-tuple-element.94), channel_id=1, source_target_pairs={{0,6},{2,0},{4,2},{6,4},{1,7},{3,1},{5,3},{7,5},{8,14},{10,8},{12,... | collective-permute-start | bytes 786440 | tf_op jit(solution)/shard_map/ppermute | solution.py:627
  136.2 2.1 %collective-permute-done.19.f1 = bf16[512,256]{1,0:T(8,128)(2,1)S(1)} collective-permute-done((bf16[512,256]{1,0:T(8,128)(2,1)S(1)}, bf16[512,256]{1,0:T(8,128)(2,1)S(1)}, u32[]{:S(2)}, u32[]{:S(2)}) %collective-permute-start.19) | collective-permute-done | bytes 262176 | tf_op jit(solution)/shard_map/ppermute | solution.py:627
  140.2 8.5 %collective-permute-done.20.f2 = bf16[512,256]{1,0:T(8,128)(2,1)S(1)} collective-permute-done((bf16[512,256]{1,0:T(8,128)(2,1)S(1)}, bf16[512,256]{1,0:T(8,128)(2,1)S(1)}, u32[]{:S(2)}, u32[]{:S(2)}) %collective-permute-start.20) | collective-permute-done | bytes 262176 | tf_op jit(solution)/shard_map/ppermute | solution.py:627
  148.9 5.3 %collective-permute-done.35.f2 = bf16[512,256]{1,0:T(8,128)(2,1)S(1)} collective-permute-done((bf16[512,256]{1,0:T(8,128)(2,1)S(1)}, bf16[512,256]{1,0:T(8,128)(2,1)S(1)}, u32[]{:S(2)}, u32[]{:S(2)}) %collective-permute-start.35) | collective-permute-done | bytes 262176 | tf_op jit(solution)/shard_map/ppermute | solution.py:627
  (96 shorter events, 44.5 us)
Async XLA Ops:
  6.5 103.1 %all-gather.2.cloned.1.call-start = ((), (), s32[]{:S(2)}) async-start(), calls=%async_computation | async-start | bytes 9191424 | tf_op jit(solution)/shard_map/all_gather | solution.py:654
  21.1 11.9 %collective-permute-start.3 = (bf16[144,512]{1,0:T(8,128)(2,1)S(1)}, bf16[144,512]{1,0:T(8,128)(2,1)S(1)}, u32[]{:S(2)}, u32[]{:S(2)}) collective-permute-start(bf16[144,512]{1,0:T(8,128)(2,1)S(1)} %get-tuple-element.68.r0), channel_id=1, source_target_pairs={{0,24},{8,0},{16,8},{24,16},{1,25},{9,1},{17,9},{25,17},{2,26},{10... | collective-permute-start | bytes 442376 | tf_op jit(solution)/shard_map/ppermute | solution.py:627
  24.2 11.4 %collective-permute-start.2 = (bf16[144,512]{1,0:T(8,128)(2,1)S(1)}, bf16[144,512]{1,0:T(8,128)(2,1)S(1)}, u32[]{:S(2)}, u32[]{:S(2)}) collective-permute-start(bf16[144,512]{1,0:T(8,128)(2,1)S(1)} %get-tuple-element.68.r0), channel_id=1, source_target_pairs={{0,16},{8,24},{16,0},{24,8},{1,17},{9,25},{17,1},{25,9},{2,18},{10... | collective-permute-start | bytes 442376 | tf_op jit(solution)/shard_map/ppermute | solution.py:627
  24.8 13.1 %collective-permute-start.1 = (bf16[144,512]{1,0:T(8,128)(2,1)S(1)}, bf16[144,512]{1,0:T(8,128)(2,1)S(1)}, u32[]{:S(2)}, u32[]{:S(2)}) collective-permute-start(bf16[144,512]{1,0:T(8,128)(2,1)S(1)} %get-tuple-element.68.r0), channel_id=1, source_target_pairs={{0,8},{8,16},{16,24},{24,0},{1,9},{9,17},{17,25},{25,1},{2,10},{10... | collective-permute-start | bytes 442376 | tf_op jit(solution)/shard_map/ppermute | solution.py:627
  62.2 16.0 %collective-permute-start.24 = (bf16[512,256]{1,0:T(8,128)(2,1)S(1)}, bf16[512,256]{1,0:T(8,128)(2,1)S(1)}, u32[]{:S(2)}, u32[]{:S(2)}) collective-permute-start(bf16[512,256]{1,0:T(8,128)(2,1)S(1)} %get-tuple-element.99), channel_id=1, source_target_pairs={{0,2},{2,4},{4,6},{6,0},{1,3},{3,5},{5,7},{7,1},{8,10},{10,12},{12... | collective-permute-start | bytes 786440 | tf_op jit(solution)/shard_map/ppermute | solution.py:627
  62.9 15.4 %collective-permute-start.25 = (bf16[512,256]{1,0:T(8,128)(2,1)S(1)}, bf16[512,256]{1,0:T(8,128)(2,1)S(1)}, u32[]{:S(2)}, u32[]{:S(2)}) collective-permute-start(bf16[512,256]{1,0:T(8,128)(2,1)S(1)} %get-tuple-element.100), channel_id=1, source_target_pairs={{0,6},{2,0},{4,2},{6,4},{1,7},{3,1},{5,3},{7,5},{8,14},{10,8},{12,... | collective-permute-start | bytes 786440 | tf_op jit(solution)/shard_map/ppermute | solution.py:627
  65.8 17.4 %collective-permute-start.8 = (bf16[512,256]{1,0:T(8,128)(2,1)S(1)}, bf16[512,256]{1,0:T(8,128)(2,1)S(1)}, u32[]{:S(2)}, u32[]{:S(2)}) collective-permute-start(bf16[512,256]{1,0:T(8,128)(2,1)S(1)} %get-tuple-element.84), channel_id=1, source_target_pairs={{0,4},{2,6},{4,0},{6,2},{1,5},{3,7},{5,1},{7,3},{8,12},{10,14},{12... | collective-permute-start | bytes 786440 | tf_op jit(solution)/shard_map/ppermute | solution.py:627
  66.0 18.6 %collective-permute-start.9 = (bf16[512,256]{1,0:T(8,128)(2,1)S(1)}, bf16[512,256]{1,0:T(8,128)(2,1)S(1)}, u32[]{:S(2)}, u32[]{:S(2)}) collective-permute-start(bf16[512,256]{1,0:T(8,128)(2,1)S(1)} %get-tuple-element.85), channel_id=1, source_target_pairs={{0,2},{2,4},{4,6},{6,0},{1,3},{3,5},{5,7},{7,1},{8,10},{10,12},{12... | collective-permute-start | bytes 786440 | tf_op jit(solution)/shard_map/ppermute | solution.py:627
  68.6 17.0 %collective-permute-start.10 = (bf16[512,256]{1,0:T(8,128)(2,1)S(1)}, bf16[512,256]{1,0:T(8,128)(2,1)S(1)}, u32[]{:S(2)}, u32[]{:S(2)}) collective-permute-start(bf16[512,256]{1,0:T(8,128)(2,1)S(1)} %get-tuple-element.86), channel_id=1, source_target_pairs={{0,6},{2,0},{4,2},{6,4},{1,7},{3,1},{5,3},{7,5},{8,14},{10,8},{12,... | collective-permute-start | bytes 786440 | tf_op jit(solution)/shard_map/ppermute | solution.py:627
  78.4 16.6 %collective-permute-start.28 = (bf16[512,256]{1,0:T(8,128)(2,1)S(1)}, bf16[512,256]{1,0:T(8,128)(2,1)S(1)}, u32[]{:S(2)}, u32[]{:S(2)}) collective-permute-start(bf16[512,256]{1,0:T(8,128)(2,1)S(1)} %own.3.m0), channel_id=1, source_target_pairs={{0,2},{2,4},{4,6},{6,0},{1,3},{3,5},{5,7},{7,1},{8,10},{10,12},{12... | collective-permute-start | bytes 786440 | tf_op jit(solution)/shard_map/ppermute | solution.py:627
  78.5 18.3 %collective-permute-start.27 = (bf16[512,256]{1,0:T(8,128)(2,1)S(1)}, bf16[512,256]{1,0:T(8,128)(2,1)S(1)}, u32[]{:S(2)}, u32[]{:S(2)}) collective-permute-start(bf16[512,256]{1,0:T(8,128)(2,1)S(1)} %own.3.m0), channel_id=1, source_target_pairs={{0,4},{2,6},{4,0},{6,2},{1,5},{3,7},{5,1},{7,3},{8,12},{10,14},{12... | collective-permute-start | bytes 786440 | tf_op jit(solution)/shard_map/ppermute | solution.py:627
  85.8 16.5 %collective-permute-start.13 = (bf16[512,256]{1,0:T(8,128)(2,1)S(1)}, bf16[512,256]{1,0:T(8,128)(2,1)S(1)}, u32[]{:S(2)}, u32[]{:S(2)}) collective-permute-start(bf16[512,256]{1,0:T(8,128)(2,1)S(1)} %own.2.m0), channel_id=1, source_target_pairs={{0,2},{2,4},{4,6},{6,0},{1,3},{3,5},{5,7},{7,1},{8,10},{10,12},{12... | collective-permute-start | bytes 786440 | tf_op jit(solution)/shard_map/ppermute | solution.py:627
  87.3 19.7 %collective-permute-start.12 = (bf16[512,256]{1,0:T(8,128)(2,1)S(1)}, bf16[512,256]{1,0:T(8,128)(2,1)S(1)}, u32[]{:S(2)}, u32[]{:S(2)}) collective-permute-start(bf16[512,256]{1,0:T(8,128)(2,1)S(1)} %own.2.m0), channel_id=1, source_target_pairs={{0,4},{2,6},{4,0},{6,2},{1,5},{3,7},{5,1},{7,3},{8,12},{10,14},{12... | collective-permute-start | bytes 786440 | tf_op jit(solution)/shard_map/ppermute | solution.py:627
  89.9 17.2 %collective-permute-start.11 = (bf16[512,256]{1,0:T(8,128)(2,1)S(1)}, bf16[512,256]{1,0:T(8,128)(2,1)S(1)}, u32[]{:S(2)}, u32[]{:S(2)}) collective-permute-start(bf16[512,256]{1,0:T(8,128)(2,1)S(1)} %own.2.m0), channel_id=1, source_target_pairs={{0,6},{2,0},{4,2},{6,4},{1,7},{3,1},{5,3},{7,5},{8,14},{10,8},{12,... | collective-permute-start | bytes 786440 | tf_op jit(solution)/shard_map/ppermute | solution.py:627
  95.0 12.5 %collective-permute-start.26 = (bf16[512,256]{1,0:T(8,128)(2,1)S(1)}, bf16[512,256]{1,0:T(8,128)(2,1)S(1)}, u32[]{:S(2)}, u32[]{:S(2)}) collective-permute-start(bf16[512,256]{1,0:T(8,128)(2,1)S(1)} %own.3.m0), channel_id=1, source_target_pairs={{0,6},{2,0},{4,2},{6,4},{1,7},{3,1},{5,3},{7,5},{8,14},{10,8},{12,... | collective-permute-start | bytes 786440 | tf_op jit(solution)/shard_map/ppermute | solution.py:627
  96.8 10.9 %collective-permute-start.14 = (bf16[512,256]{1,0:T(8,128)(2,1)S(1)}, bf16[512,256]{1,0:T(8,128)(2,1)S(1)}, u32[]{:S(2)}, u32[]{:S(2)}) collective-permute-start(bf16[512,256]{1,0:T(8,128)(2,1)S(1)} %own.2.m0), channel_id=1, source_target_pairs={{0,1},{1,0},{2,3},{3,2},{4,5},{5,4},{6,7},{7,6},{8,9},{9,8},{10,11... | collective-permute-start | bytes 786440 | tf_op jit(solution)/shard_map/ppermute | solution.py:631
  107.6 11.2 %collective-permute-start.29 = (bf16[512,256]{1,0:T(8,128)(2,1)S(1)}, bf16[512,256]{1,0:T(8,128)(2,1)S(1)}, u32[]{:S(2)}, u32[]{:S(2)}) collective-permute-start(bf16[512,256]{1,0:T(8,128)(2,1)S(1)} %own.3.m0), channel_id=1, source_target_pairs={{0,1},{1,0},{2,3},{3,2},{4,5},{5,4},{6,7},{7,6},{8,9},{9,8},{10,11... | collective-permute-start | bytes 786440 | tf_op jit(solution)/shard_map/ppermute | solution.py:631
  107.6 11.1 %collective-permute-start.32 = (bf16[512,256]{1,0:T(8,128)(2,1)S(1)}, bf16[512,256]{1,0:T(8,128)(2,1)S(1)}, u32[]{:S(2)}, u32[]{:S(2)}) collective-permute-start(bf16[512,256]{1,0:T(8,128)(2,1)S(1)} %collective-permute-done.28.m3), channel_id=1, source_target_pairs={{0,1},{1,0},{2,3},{3,2},{4,5},{5,4},{6,7},{7,6},{8,9},{9,8},{10,11... | collective-permute-start | bytes 786440 | tf_op jit(solution)/shard_map/ppermute | solution.py:631
  127.5 10.9 %collective-permute-start.19 = (bf16[512,256]{1,0:T(8,128)(2,1)S(1)}, bf16[512,256]{1,0:T(8,128)(2,1)S(1)}, u32[]{:S(2)}, u32[]{:S(2)}) collective-permute-start(bf16[512,256]{1,0:T(8,128)(2,1)S(1)} %get-tuple-element.92), channel_id=1, source_target_pairs={{0,4},{2,6},{4,0},{6,2},{1,5},{3,7},{5,1},{7,3},{8,12},{10,14},{12... | collective-permute-start | bytes 786440 | tf_op jit(solution)/shard_map/ppermute | solution.py:627
  132.5 16.5 %collective-permute-start.34 = (bf16[512,256]{1,0:T(8,128)(2,1)S(1)}, bf16[512,256]{1,0:T(8,128)(2,1)S(1)}, u32[]{:S(2)}, u32[]{:S(2)}) collective-permute-start(bf16[512,256]{1,0:T(8,128)(2,1)S(1)} %get-tuple-element.104), channel_id=1, source_target_pairs={{0,4},{2,6},{4,0},{6,2},{1,5},{3,7},{5,1},{7,3},{8,12},{10,14},{12... | collective-permute-start | bytes 786440 | tf_op jit(solution)/shard_map/ppermute | solution.py:627
  133.0 15.8 %collective-permute-start.20 = (bf16[512,256]{1,0:T(8,128)(2,1)S(1)}, bf16[512,256]{1,0:T(8,128)(2,1)S(1)}, u32[]{:S(2)}, u32[]{:S(2)}) collective-permute-start(bf16[512,256]{1,0:T(8,128)(2,1)S(1)} %get-tuple-element.93), channel_id=1, source_target_pairs={{0,2},{2,4},{4,6},{6,0},{1,3},{3,5},{5,7},{7,1},{8,10},{10,12},{12... | collective-permute-start | bytes 786440 | tf_op jit(solution)/shard_map/ppermute | solution.py:627
  133.6 15.1 %collective-permute-start.21 = (bf16[512,256]{1,0:T(8,128)(2,1)S(1)}, bf16[512,256]{1,0:T(8,128)(2,1)S(1)}, u32[]{:S(2)}, u32[]{:S(2)}) collective-permute-start(bf16[512,256]{1,0:T(8,128)(2,1)S(1)} %get-tuple-element.94), channel_id=1, source_target_pairs={{0,6},{2,0},{4,2},{6,4},{1,7},{3,1},{5,3},{7,5},{8,14},{10,8},{12,... | collective-permute-start | bytes 786440 | tf_op jit(solution)/shard_map/ppermute | solution.py:627
  136.2 18.0 %collective-permute-start.35 = (bf16[512,256]{1,0:T(8,128)(2,1)S(1)}, bf16[512,256]{1,0:T(8,128)(2,1)S(1)}, u32[]{:S(2)}, u32[]{:S(2)}) collective-permute-start(bf16[512,256]{1,0:T(8,128)(2,1)S(1)} %get-tuple-element.105), channel_id=1, source_target_pairs={{0,2},{2,4},{4,6},{6,0},{1,3},{3,5},{5,7},{7,1},{8,10},{10,12},{12... | collective-permute-start | bytes 786440 | tf_op jit(solution)/shard_map/ppermute | solution.py:627
  138.4 15.9 %collective-permute-start.36 = (bf16[512,256]{1,0:T(8,128)(2,1)S(1)}, bf16[512,256]{1,0:T(8,128)(2,1)S(1)}, u32[]{:S(2)}, u32[]{:S(2)}) collective-permute-start(bf16[512,256]{1,0:T(8,128)(2,1)S(1)} %get-tuple-element.106), channel_id=1, source_target_pairs={{0,6},{2,0},{4,2},{6,4},{1,7},{3,1},{5,3},{7,5},{8,14},{10,8},{12,... | collective-permute-start | bytes 786440 | tf_op jit(solution)/shard_map/ppermute | solution.py:627
  (21 other events, 235.5 us)
Sparse Core Ops, SparseCore 0:
  9.5 79.6 all-gather.1

commit v2 on v1

--- a/solution.py
+++ b/solution.py
@@ -32,7 +32,7 @@
 
 VMEM = pl.BlockSpec(memory_space=pltpu.VMEM)
 SMEM = pl.BlockSpec(memory_space=pltpu.SMEM)
-ANY = pl.BlockSpec(memory_space=pl.ANY)
+HBM = pl.BlockSpec(memory_space=pltpu.HBM)
 
 
 def sds(shape, kind):
@@ -89,14 +89,46 @@
     return jnp.sum(jnp.where(own, spread_row, 0.0), axis=1, keepdims=True)
 
 
+def in_hbm(*arrays):
+    return tuple(pltpu.with_memory_space_constraint(a, pltpu.HBM) for a in arrays)
+
+
 def softplus(x):
     return jnp.maximum(x, 0.0) + jnp.log1p(jnp.exp(-jnp.abs(x)))
 
 
-def decay_body(
-    raw, spike, shift, fading, skip, taps_c, taps_p,
-    cum_out, tot_out, step_out, factors, ends, total_out, skip_out, taps_c_out, taps_p_out,
+def head_body(
+    gate, up, down, raw_in, spike_in, shift_in, fading_in, skip_in, taps_c_in, taps_p_in,
+    content_in, pairs_in,
+    pack, tail, cum_out, tot_out, step_out, factors, ends, total_out, skip_out, taps_c_out,
+    taps_p_out,
+    packed, raw, spike, shift, fading, skip, taps_c, taps_p, content, pairs, sems,
 ):
+    weights = [
+        pltpu.make_async_copy(part, packed.at[pl.ds(i * FF, FF), :], sems.at[0])
+        for i, part in enumerate((gate, up, down))
+    ]
+    small = [
+        pltpu.make_async_copy(source, target, sems.at[1])
+        for source, target in (
+            (raw_in, raw), (spike_in, spike), (shift_in, shift), (fading_in, fading),
+            (skip_in, skip), (taps_c_in, taps_c), (taps_p_in, taps_p),
+            (content_in.at[pl.ds(T - HALO, HALO), :], content),
+            (pairs_in.at[pl.ds(T - HALO, HALO)], pairs),
+        )
+    ]
+    for copy in weights + small:
+        copy.start()
+    for copy in weights:
+        copy.wait()
+    out = pltpu.make_async_copy(packed, pack, sems.at[2])
+    out.start()
+    for copy in small:
+        copy.wait()
+    tail[:, 0:CH] = content[...]
+    rows = pairs[...].astype(F32)
+    tail[:, CH : CH + ST] = rows[:, 0, :].astype(BF)
+    tail[:, CH + ST : CH + 2 * ST] = rows[:, 1, :].astype(BF)
     row = lax.broadcasted_iota(jnp.int32, (BLK, BLK), 0)
     col = lax.broadcasted_iota(jnp.int32, (BLK, BLK), 1)
     triu = (row <= col).astype(F32)
@@ -122,12 +154,16 @@
     wide = taps_p[...].astype(F32)
     taps_p_out[0:4, 0:ST] = wide[:, 0, :]
     taps_p_out[0:4, ST : 2 * ST] = wide[:, 1, :]
-
-
-def decay_kernel(*args):
-    return pl.pallas_call(
-        decay_body,
+    out.wait()
+
+
+def head_kernel(*args):
+    small = args[3:10]
+    return pl.pallas_call(
+        head_body,
         out_shape=(
+            sds((PACK, 128), BF),
+            sds((HALO, CH + 256), BF),
             sds((HEADS, T), F32),
             sds((HEADS, T), F32),
             sds((HEADS, T), F32),
@@ -138,11 +174,17 @@
             sds((8, CH), F32),
             sds((8, 256), F32),
         ),
-        grid=(1,),
-        in_specs=[whole(a.shape) for a in args],
-        out_specs=(VMEM,) * 9,
-        compiler_params=params(8),
-        name="decay",
+        in_specs=[HBM] * len(args),
+        out_specs=(HBM,) + (VMEM,) * 10,
+        scratch_shapes=[pltpu.VMEM((PACK, 128), BF)]
+        + [pltpu.VMEM(a.shape, a.dtype) for a in small]
+        + [
+            pltpu.VMEM((HALO, CH), BF),
+            pltpu.VMEM((HALO, 2, ST), BF),
+            pltpu.SemaphoreType.DMA((3,)),
+        ],
+        compiler_params=params(8),
+        name="head",
     )(*in_hbm(*args))
 
 
@@ -261,27 +303,6 @@
     )(*args)
 
 
-def tail_body(content, pairs, out):
-    out[:, 0:CH] = content[...]
-    out[:, CH : CH + 256] = pairs[...]
-
-
-def tail_kernel(content, pairs):
-    last = T // HALO - 1
-    return pl.pallas_call(
-        tail_body,
-        out_shape=sds((HALO, CH + 256), BF),
-        grid=(1,),
-        in_specs=[
-            pl.BlockSpec((HALO, CH), lambda _: (last, 0)),
-            pl.BlockSpec((HALO, 256), lambda _: (0, 0)),
-        ],
-        out_specs=VMEM,
-        compiler_params=params(4),
-        name="tail",
-    )(content, pairs)
-
-
 def log_row(ref):
     return ref[ST : ST + 1, :].astype(F32) + ref[ST + 8 : ST + 9, :].astype(F32)
 
@@ -367,15 +388,14 @@
         return 0
 
     lax.fori_loop(0, count // BLK, block, 0, unroll=2)
-    project(order, 4, mixed, blend, 0, send)
-
-
-def project(order, first, rows, weights, at, target):
-    height = rows.shape[1]
+    project(order, 4, mixed, blend, send)
+
+
+def project(order, first, rows, weights, target):
     for k in range(4):
         cols = pl.ds(pl.multiple_of(order[first + k] * COL, COL), COL)
         target[k] = jnp.dot(
-            rows[...], weights[at : at + height, cols], preferred_element_type=F32
+            rows[...], weights[:, cols], preferred_element_type=F32
         ).astype(BF)
 
 
@@ -395,16 +415,16 @@
         ),
         compiler_params=params(4),
         name="cols",
-    )(col, pltpu.with_memory_space_constraint(arriving, pltpu.HBM))
-
-
-def keep_body(at, order, rows, weights, target):
-    project(order, 0, rows, weights, at, target)
-
-
-def keep_kernel(order, rows, weights, at):
-    return pl.pallas_call(
-        functools.partial(keep_body, at),
+    )(col, *in_hbm(arriving))
+
+
+def keep_body(order, rows, weights, target):
+    project(order, 0, rows, weights, target)
+
+
+def keep_kernel(order, rows, weights):
+    return pl.pallas_call(
+        keep_body,
         out_shape=sds((4, rows.shape[0], COL), BF),
         in_specs=[SMEM, VMEM, VMEM],
         out_specs=VMEM,
@@ -524,48 +544,61 @@
     lax.fori_loop(0, rows_x.shape[0] // NORM_ROWS, norm, 0)
 
 
-def ffn_hidden(weights, rows_x, hid):
+def ffn_hidden(weights, rows_x, hid, at, width):
     over_k = (((1,), (1,)), ((), ()))
-    gate = lax.dot_general(
-        rows_x[...], weights[0:FF, :], over_k, preferred_element_type=F32
-    )
-    up = lax.dot_general(
-        rows_x[...], weights[FF : 2 * FF, :], over_k, preferred_element_type=F32
-    )
-    hid[...] = (silu(gate) * up).astype(BF)
+
+    def columns(at):
+        return jnp.concatenate([weights[j, at : at + width, :] for j in range(16)], axis=1)
+
+    gate = lax.dot_general(rows_x[...], columns(at), over_k, preferred_element_type=F32)
+    up = lax.dot_general(rows_x[...], columns(FF + at), over_k, preferred_element_type=F32)
+    hid[:, at : at + width] = (silu(gate) * up).astype(BF)
+
+
+def project_down(order, first, hid, weights, target):
+    for k in range(4):
+        spot = 2 * order[first + k]
+        both = jnp.concatenate(
+            [weights[spot, 2 * FF :, :], weights[spot + 1, 2 * FF :, :]], axis=1
+        )
+        target[k] = jnp.dot(hid[...], both, preferred_element_type=F32).astype(BF)
 
 
 def ffn_first_body(
     order, pack, gain, m0, m1, m2, m3, n0, n1, n2, n3, send, hid, weights, rows_x, sems
 ):
-    def copies(part, at, size):
+    def copies(sem, *spans):
         return [
             pltpu.make_async_copy(
-                pack.at[j, pl.ds(at, size), :],
-                weights.at[pl.ds(at, size), pl.ds(j * 128, 128)],
-                sems.at[part],
+                pack.at[:, pl.ds(at, size), :], weights.at[:, pl.ds(at, size), :], sems.at[sem]
             )
-            for j in range(16)
+            for at, size in spans
         ]
 
-    up, down = copies(0, 0, 2 * FF), copies(1, 2 * FF, FF)
-    for copy in up + down:
-        copy.start()
+    halves = ((0, 512), (512, FF - 512))
+    parts = [
+        copies(i, (at, width), (FF + at, width)) for i, (at, width) in enumerate(halves)
+    ]
+    parts.append(copies(2, (2 * FF, FF)))
+    for part in parts:
+        for copy in part:
+            copy.start()
     ffn_rows(order, gain, (m0, m1, m2, m3, n0, n1, n2, n3), rows_x)
-    for copy in up:
+    for part, (at, width) in zip(parts, halves):
+        for copy in part:
+            copy.wait()
+        ffn_hidden(weights, rows_x, hid, at, width)
+    for copy in parts[2]:
         copy.wait()
-    ffn_hidden(weights, rows_x, hid)
-    for copy in down:
-        copy.wait()
-    project(order, 4, hid, weights, 2 * FF, send)
+    project_down(order, 4, hid, weights, send)
 
 
 def ffn_next_body(
     order, weights, gain, m0, m1, m2, m3, n0, n1, n2, n3, send, hid, rows_x
 ):
     ffn_rows(order, gain, (m0, m1, m2, m3, n0, n1, n2, n3), rows_x)
-    ffn_hidden(weights, rows_x, hid)
-    project(order, 4, hid, weights, 2 * FF, send)
+    ffn_hidden(weights, rows_x, hid, 0, FF)
+    project_down(order, 4, hid, weights, send)
 
 
 def ffn_kernel(order, weights, gain, pieces, first):
@@ -573,8 +606,8 @@
     shapes = (sds((4, count, COL), BF), sds((count, FF), BF))
     scratch = [pltpu.VMEM((count, D), BF)]
     if first:
-        shapes += (sds((PACK, D), BF),)
-        scratch.append(pltpu.SemaphoreType.DMA((2,)))
+        shapes += (sds((16, PACK, 128), BF),)
+        scratch.append(pltpu.SemaphoreType.DMA((3,)))
         (weights,) = in_hbm(weights)
     return pl.pallas_call(
         ffn_first_body if first else ffn_next_body,
@@ -588,38 +621,20 @@
     )(order, weights, gain, *pieces)
 
 
-HBM = pl.BlockSpec(memory_space=pltpu.HBM)
-
-
-def pack_body(gate, up, down, out, sem):
-    copies = [
-        pltpu.make_async_copy(part, out.at[pl.ds(i * FF, FF), :], sem)
-        for i, part in enumerate((gate, up, down))
-    ]
-    for copy in copies:
-        copy.start()
-    for copy in copies:
-        copy.wait()
-
-
-def whole(shape):
-    return pl.BlockSpec(shape, lambda _: (0,) * len(shape))
-
-
-def in_hbm(*arrays):
-    return tuple(pltpu.with_memory_space_constraint(a, pltpu.HBM) for a in arrays)
-
-
-def pack_kernel(*parts):
-    return pl.pallas_call(
-        pack_body,
-        out_shape=sds((PACK, 128), BF),
-        in_specs=[HBM] * 3,
+def keep_down_body(order, hid, weights, target):
+    project_down(order, 0, hid, weights, target)
+
+
+def keep_down_kernel(order, hid, weights):
+    return pl.pallas_call(
+        keep_down_body,
+        out_shape=sds((4, hid.shape[0], COL), BF),
+        in_specs=[SMEM, VMEM, VMEM],
         out_specs=VMEM,
-        scratch_shapes=[pltpu.SemaphoreType.DMA],
-        compiler_params=params(4),
-        name="pack",
-    )(*in_hbm(*parts))
+        compiler_params=params(8),
+        cost_estimate=pl.CostEstimate(flops=1_000_000_000, transcendentals=0, bytes_accessed=6_000_000),
+        name="keep_down",
+    )(order, hid, weights)
 
 
 def turn(array, axis, distance):
@@ -633,11 +648,13 @@
 
 def reduce_chips(parts):
     c0, c1, c2, c3 = parts
-    return c0, turn(c2, "x", 2), turn(c1, "x", 1), turn(c3, "x", -1)
+    far = turn(c2, "x", 2)
+    return c0, far, turn(c1, "x", 1), turn(c3, "x", -1)
 
 
 def gather_chips(own):
-    return own, turn(own, "x", -1), turn(own, "x", 2), turn(own, "x", 1)
+    far = turn(own, "x", 2)
+    return own, turn(own, "x", -1), far, turn(own, "x", 1)
 
 
 def shards(
@@ -650,20 +667,17 @@
     order = jnp.concatenate([chips * 2 + c, chips * 2 + (1 - c)]).astype(jnp.int32)
     first_col = (2 * x + c).reshape(1)
     y, z = y.reshape(1), z.reshape(1)
-    pack = pack_kernel(w_gate.T, w_up.T, w_down)
+    pack, tail, cum, tot, step, factors, ends, total, skip, taps_c, taps_p = head_kernel(
+        w_gate.T, w_up.T, w_down, raw.T, spike.T, shift.reshape(1, HEADS),
+        fading.reshape(1, HEADS), skip.reshape(1, HEADS), taps_c, taps_p.reshape(4, 2, ST),
+        content, linked.reshape(T, 2, ST),
+    )
+    pack, tail, order, first_col, y, z, linked = lax.optimization_barrier(
+        (pack, tail, order, first_col, y, z, linked)
+    )
     gathered = lax.all_gather(pack, SP, axis=0, tiled=True).reshape(16, PACK, 128)
-    linked_tail = linked[T - HALO :].reshape(HALO, 256)
-    content_tail, linked_tail, pack = lax.optimization_barrier((content, linked_tail, pack))
-    tail = tail_kernel(pltpu.with_memory_space_constraint(content_tail, pltpu.HBM), linked_tail)
-    tail, order, first_col, y, z, linked = lax.optimization_barrier(
-        (tail, order, first_col, y, z, linked)
-    )
     pairs = linked.reshape(T, 256)
     halo = lax.ppermute(tail, SP, [(i, i + 1) for i in range(15)])
-    cum, tot, step, factors, ends, total, skip, taps_c, taps_p = decay_kernel(
-        raw.T, spike.T, shift.reshape(1, HEADS), fading.reshape(1, HEADS),
-        skip.reshape(1, HEADS), taps_c, taps_p.reshape(4, 2, ST),
-    )
     values, maps, entering, payload = state_kernel(
         content, pairs, halo, factors, ends, total, taps_c, taps_p
     )
@@ -680,14 +694,14 @@
     (at_a, rows_a), (at_b, rows_b) = (0, FIRST), (FIRST, SECOND)
     send_a, mixed_a = mix_kernel(at_a, rows_a, order, *mix_args)
     got_a = swap(send_a)
-    keep_a = keep_kernel(order, mixed_a, blender, 0)
+    keep_a = keep_kernel(order, mixed_a, blender)
     parts = pair_kernel(keep_a, got_a)
     parts = reduce_chips(parts)
     own_a = own_kernel(at_a, parts, mine_cols)
     mine_a = gather_chips(own_a)
     send_b, mixed_b = mix_kernel(at_b, rows_b, order, *mix_args)
     got_b = swap(send_b)
-    keep_b = keep_kernel(order, mixed_b, blender, 0)
+    keep_b = keep_kernel(order, mixed_b, blender)
     parts = pair_kernel(keep_b, got_b)
     parts = reduce_chips(parts)
     own_b = own_kernel(at_b, parts, mine_cols)
@@ -695,13 +709,13 @@
     theirs_a = tuple(swap(piece) for piece in mine_a)
     send, hid, weights = ffn_kernel(order, gathered, gain, (*mine_a, *theirs_a), True)
     got = swap(send)
-    keep = keep_kernel(order, hid, weights, 2 * FF)
+    keep = keep_down_kernel(order, hid, weights)
     parts = pair_kernel(keep, got)
     last_a = reduce_chips(parts)
     theirs_b = tuple(swap(piece) for piece in mine_b)
     send, hid = ffn_kernel(order, weights, gain, (*mine_b, *theirs_b), False)
     got = swap(send)
-    keep = keep_kernel(order, hid, weights, 2 * FF)
+    keep = keep_down_kernel(order, hid, weights)
     parts = pair_kernel(keep, got)
     last_b = reduce_chips(parts)
     return join_kernel(last_kernel(own_a, last_a), own_b, last_b)

time: 163 us -> 161 us (0.988)
  Pallas kernels: 41.2 us -> 38.8 us
    pallas_call x7 -> x5, Pallas kernels: 9.86 us -> 7.64 us  [the longest x2 3.05 us: keep_down_kernel(): pl.pallas_call(keep_down_body, out_shape=sds((4, hid.shape[0], COL), BF),...]
    unnamed x16 -> x15, local copies, waits for them, and re-layouts: 2.81 us -> 4.02 us
  transfers between devices with their start and end apart: 38 -> 38, of which waited for: 18 -> 19; matrix products, arithmetic and copies ran while one was open for 1% -> 1% of each run, Pallas kernels for 24% -> 22%
where the time goes in v2:
time: 161 us; the launch traced here: 160 us
  waiting for transfers between devices  57.7 us (36%)
  starting transfers between devices  45.9 us (29%)
  Pallas kernels  38.8 us (24%)
  between operations  13.7 us (9%)
  local copies, waits for them, and re-layouts  4.02 us (2%)
    ppermute x24, waiting for transfers between devices, turn(): lax.ppermute(array, axis, [(i, (i + distance) % count) for i in range(cou...  56.7 us
    ppermute x24, starting transfers between devices, turn(): lax.ppermute(array, axis, [(i, (i + distance) % count) for i in range(cou...  39.5 us
    pallas_call x2, Pallas kernels, ffn_kernel(): pl.pallas_call(ffn_first_body if first else ffn_next_body, out_shape=shap...  13.8 us
    pallas_call x1, Pallas kernels, state_kernel(): pl.pallas_call(state_body, out_shape=(sds((T, CH), BF), sds((T, 256), BF)...  4.63 us
    pallas_call x1, Pallas kernels, local_kernel(): pl.pallas_call(local_body, out_shape=(sds((T, CH), F32), sds((T, CH), F32...  4.41 us
    pallas_call x2, Pallas kernels, mix_kernel(): pl.pallas_call(functools.partial(mix_body, start, count), out_shape=(sds(...  4.19 us
    unnamed x15, local copies, waits for them, and re-layouts  4.02 us
    ppermute x1, starting transfers between devices, shards(): halo = lax.ppermute(tail, SP, [(i, i + 1) for i in range(15)])  3.59 us
  transfers between devices with their start and end apart: 38, of which 19 were waited for; matrix products, arithmetic and copies ran while one was open for 1% of the time, Pallas kernels for 22%

profile of v2, /device:TPU:0, one launch (start us, length us, event | category | flops | bytes accessed | tf_op | source)
XLA Modules:
  0.0 160.2 jit_solution(1450436814077952172)
XLA Ops:
  8.7 3.6 %collective-permute-start = (bf16[16,768]{1,0:T(8,128)(2,1)S(1)}, bf16[16,768]{1,0:T(8,128)(2,1)S(1)}, u32[]{:S(2)}, u32[]{:S(2)}) collective-permute-start(bf16[16,768]{1,0:T(8,128)(2,1)S(1)} %get-tuple-element.63), channel_id=1, source_target_pairs={{0,8},{8,16},{16,24},{24,32},{32,40},{40,48},{48,56},{56,64},{64,7... | collective-permute-start | bytes 73736 | tf_op jit(solution)/shard_map/ppermute | solution.py:680
  13.9 4.6 %state.1 = (bf16[1024,512]{1,0:T(8,128)(2,1)S(1)}, bf16[1024,256]{1,0:T(8,128)(2,1)S(1)}, bf16[8,128,512]{2,1,0:T(8,128)(2,1)S(1)}, bf16[144,512]{1,0:T(8,128)(2,1)S(1)}) custom-call(bf16[1024,512]{1,0:T(8,128)(2,1)S(1)} %copy-done, bf16[1024,256]{1,0:T(8,128)(2,1)S(1)} %bitcast.20, bf16[16,768]{1,0:T(8,128)(2,1)S(1)} %collective-permute-done.halo, ...), custom_call_target="tpu_custom_call" | custom-call | tf_op jit(solution)/shard_map/state/pallas_call | solution.py:229
  18.5 3.8 %collective-permute-start.3 = (bf16[144,512]{1,0:T(8,128)(2,1)S(1)}, bf16[144,512]{1,0:T(8,128)(2,1)S(1)}, u32[]{:S(2)}, u32[]{:S(2)}) collective-permute-start(bf16[144,512]{1,0:T(8,128)(2,1)S(1)} %get-tuple-element.69.r0), channel_id=1, source_target_pairs={{0,24},{8,0},{16,8},{24,16},{1,25},{9,1},{17,9},{25,17},{2,26},{10... | collective-permute-start | bytes 442376 | tf_op jit(solution)/shard_map/ppermute | solution.py:642
  23.9 6.4 %collective-permute-done.3.r3 = bf16[144,512]{1,0:T(8,128)(2,1)S(1)} collective-permute-done((bf16[144,512]{1,0:T(8,128)(2,1)S(1)}, bf16[144,512]{1,0:T(8,128)(2,1)S(1)}, u32[]{:S(2)}, u32[]{:S(2)}) %collective-permute-start.3) | collective-permute-done | bytes 147488 | tf_op jit(solution)/shard_map/ppermute | solution.py:642
  30.3 3.0 %collective-permute-done.2.r2 = bf16[144,512]{1,0:T(8,128)(2,1)S(1)} collective-permute-done((bf16[144,512]{1,0:T(8,128)(2,1)S(1)}, bf16[144,512]{1,0:T(8,128)(2,1)S(1)}, u32[]{:S(2)}, u32[]{:S(2)}) %collective-permute-start.2) | collective-permute-done | bytes 147488 | tf_op jit(solution)/shard_map/ppermute | solution.py:642
  35.3 4.4 %collective-permute-start.6 = (bf16[144,512]{1,0:T(8,128)(2,1)S(1)}, bf16[144,512]{1,0:T(8,128)(2,1)S(1)}, u32[]{:S(2)}, u32[]{:S(2)}) collective-permute-start(bf16[144,512]{1,0:T(8,128)(2,1)S(1)} %get-tuple-element.70.q0), channel_id=1, source_target_pairs={{0,96},{32,0},{64,32},{96,64},{1,97},{33,1},{65,33},{97,65},{2,98}... | collective-permute-start | bytes 442376 | tf_op jit(solution)/shard_map/ppermute | solution.py:642
  42.1 4.4 %local.1 = (f32[1024,512]{1,0:T(8,128)S(1)}, f32[1024,512]{1,0:T(8,128)S(1)}) custom-call(bf16[1024,512]{1,0:T(8,128)(2,1)S(1)} %get-tuple-element.73.values, bf16[1024,256]{1,0:T(8,128)(2,1)S(1)} %get-tuple-element.74.maps, f32[8,1024]{1,0:T(8,128)S(1)} %get-tuple-element.75.cum_in, f32[8,1024]{1,0:T(8,128)S(1)} %get-tuple-element.76.step_in, ...), custom_call_target="tpu_custom_call" | custom-call | flops 6000000000 | bytes 6000000 | tf_op jit(solution)/shard_map/local/pallas_call | solution.py:295
  49.8 2.1 %mix.3 = (bf16[4,512,256]{2,1,0:T(8,128)(2,1)S(1)}, bf16[512,512]{1,0:T(8,128)(2,1)S(1)}) custom-call(s32[8]{0:T(128)S(1)} %pad_add_fusion.order, bf16[128,512]{1,0:T(8,128)(2,1)S(1)} %incoming.1, f32[1024,512]{1,0:T(8,128)S(1)} %get-tuple-element.79.local, bf16[1024,256]{1,0:T(8,128)(2,1)S(1)} %get-tuple-element.74.maps, ...), custom_call_target="tpu_custom_call" | custom-call | flops 3000000000 | bytes 6000000 | tf_op jit(solution)/shard_map/mix/pallas_call | solution.py:438
  56.2 3.1 %collective-permute-start.23 = (bf16[512,256]{1,0:T(8,128)(2,1)S(1)}, bf16[512,256]{1,0:T(8,128)(2,1)S(1)}, u32[]{:S(2)}, u32[]{:S(2)}) collective-permute-start(bf16[512,256]{1,0:T(8,128)(2,1)S(1)} %get-tuple-element.100), channel_id=1, source_target_pairs={{0,4},{2,6},{4,0},{6,2},{1,5},{3,7},{5,1},{7,3},{8,12},{10,14},{12... | collective-permute-start | bytes 786440 | tf_op jit(solution)/shard_map/ppermute | solution.py:642
  61.2 2.7 %collective-permute-start.25 = (bf16[512,256]{1,0:T(8,128)(2,1)S(1)}, bf16[512,256]{1,0:T(8,128)(2,1)S(1)}, u32[]{:S(2)}, u32[]{:S(2)}) collective-permute-start(bf16[512,256]{1,0:T(8,128)(2,1)S(1)} %get-tuple-element.102), channel_id=1, source_target_pairs={{0,6},{2,0},{4,2},{6,4},{1,7},{3,1},{5,3},{7,5},{8,14},{10,8},{12,... | collective-permute-start | bytes 786440 | tf_op jit(solution)/shard_map/ppermute | solution.py:642
  66.9 2.7 %collective-permute-start.10 = (bf16[512,256]{1,0:T(8,128)(2,1)S(1)}, bf16[512,256]{1,0:T(8,128)(2,1)S(1)}, u32[]{:S(2)}, u32[]{:S(2)}) collective-permute-start(bf16[512,256]{1,0:T(8,128)(2,1)S(1)} %get-tuple-element.87), channel_id=1, source_target_pairs={{0,6},{2,0},{4,2},{6,4},{1,7},{3,1},{5,3},{7,5},{8,14},{10,8},{12,... | collective-permute-start | bytes 786440 | tf_op jit(solution)/shard_map/ppermute | solution.py:642
  70.8 5.8 %collective-permute-done.24.f2 = bf16[512,256]{1,0:T(8,128)(2,1)S(1)} collective-permute-done((bf16[512,256]{1,0:T(8,128)(2,1)S(1)}, bf16[512,256]{1,0:T(8,128)(2,1)S(1)}, u32[]{:S(2)}, u32[]{:S(2)}) %collective-permute-start.24) | collective-permute-done | bytes 262176 | tf_op jit(solution)/shard_map/ppermute | solution.py:642
  76.8 4.7 %collective-permute-start.27 = (bf16[512,256]{1,0:T(8,128)(2,1)S(1)}, bf16[512,256]{1,0:T(8,128)(2,1)S(1)}, u32[]{:S(2)}, u32[]{:S(2)}) collective-permute-start(bf16[512,256]{1,0:T(8,128)(2,1)S(1)} %own.3.m0), channel_id=1, source_target_pairs={{0,4},{2,6},{4,0},{6,2},{1,5},{3,7},{5,1},{7,3},{8,12},{10,14},{12... | collective-permute-start | bytes 786440 | tf_op jit(solution)/shard_map/ppermute | solution.py:642
  85.7 2.5 %collective-permute-start.12 = (bf16[512,256]{1,0:T(8,128)(2,1)S(1)}, bf16[512,256]{1,0:T(8,128)(2,1)S(1)}, u32[]{:S(2)}, u32[]{:S(2)}) collective-permute-start(bf16[512,256]{1,0:T(8,128)(2,1)S(1)} %own.2.m0), channel_id=1, source_target_pairs={{0,4},{2,6},{4,0},{6,2},{1,5},{3,7},{5,1},{7,3},{8,12},{10,14},{12... | collective-permute-start | bytes 786440 | tf_op jit(solution)/shard_map/ppermute | solution.py:642
  88.9 4.5 %collective-permute-done.28.m3 = bf16[512,256]{1,0:T(8,128)(2,1)S(1)} collective-permute-done((bf16[512,256]{1,0:T(8,128)(2,1)S(1)}, bf16[512,256]{1,0:T(8,128)(2,1)S(1)}, u32[]{:S(2)}, u32[]{:S(2)}) %collective-permute-start.28) | collective-permute-done | bytes 262176 | tf_op jit(solution)/shard_map/ppermute | solution.py:642
  95.1 5.4 %collective-permute-done.13.m3 = bf16[512,256]{1,0:T(8,128)(2,1)S(1)} collective-permute-done((bf16[512,256]{1,0:T(8,128)(2,1)S(1)}, bf16[512,256]{1,0:T(8,128)(2,1)S(1)}, u32[]{:S(2)}, u32[]{:S(2)}) %collective-permute-start.13) | collective-permute-done | bytes 262176 | tf_op jit(solution)/shard_map/ppermute | solution.py:642
  100.6 4.9 %collective-permute-done.12.m2 = bf16[512,256]{1,0:T(8,128)(2,1)S(1)} collective-permute-done((bf16[512,256]{1,0:T(8,128)(2,1)S(1)}, bf16[512,256]{1,0:T(8,128)(2,1)S(1)}, u32[]{:S(2)}, u32[]{:S(2)}) %collective-permute-start.12) | collective-permute-done | bytes 262176 | tf_op jit(solution)/shard_map/ppermute | solution.py:642
  109.0 7.4 %ffn.2 = (bf16[4,512,256]{2,1,0:T(8,128)(2,1)S(1)}, bf16[512,704]{1,0:T(8,128)(2,1)S(1)}, bf16[16,2112,128]{2,1,0:T(8,128)(2,1)S(1)}) custom-call(s32[8]{0:T(128)S(1)} %pad_add_fusion.order, bf16[16,2112,128]{2,1,0:T(8,128)(2,1)} %bitcast.35, f32[1,2048]{1,0:T(1,128)S(1)} %bitcast.21, bf16[512,256]{1,0:T(8,128)(2,1)S(1)} %own.2.m0, ...), custom_call_target="tpu_custom_call" | custom-call | flops 8999999488 | bytes 12000000 | tf_op jit(solution)/shard_map/ffn/pallas_call | solution.py:612
  116.9 6.4 %ffn.3 = (bf16[4,512,256]{2,1,0:T(8,128)(2,1)S(1)}, bf16[512,704]{1,0:T(8,128)(2,1)S(1)}) custom-call(s32[8]{0:T(128)S(1)} %pad_add_fusion.order, bf16[16,2112,128]{2,1,0:T(8,128)(2,1)S(1)} %get-tuple-element.91.weights, f32[1,2048]{1,0:T(1,128)S(1)} %bitcast.22, bf16[512,256]{1,0:T(8,128)(2,1)S(1)} %own.3.m0, ...), custom_call_target="tpu_custom_call" | custom-call | flops 8999999488 | bytes 12000000 | tf_op jit(solution)/shard_map/ffn/pallas_call | solution.py:612
  125.5 3.1 %collective-permute-start.19 = (bf16[512,256]{1,0:T(8,128)(2,1)S(1)}, bf16[512,256]{1,0:T(8,128)(2,1)S(1)}, u32[]{:S(2)}, u32[]{:S(2)}) collective-permute-start(bf16[512,256]{1,0:T(8,128)(2,1)S(1)} %get-tuple-element.94), channel_id=1, source_target_pairs={{0,4},{2,6},{4,0},{6,2},{1,5},{3,7},{5,1},{7,3},{8,12},{10,14},{12... | collective-permute-start | bytes 786440 | tf_op jit(solution)/shard_map/ppermute | solution.py:642
  131.6 2.6 %collective-permute-start.21 = (bf16[512,256]{1,0:T(8,128)(2,1)S(1)}, bf16[512,256]{1,0:T(8,128)(2,1)S(1)}, u32[]{:S(2)}, u32[]{:S(2)}) collective-permute-start(bf16[512,256]{1,0:T(8,128)(2,1)S(1)} %get-tuple-element.96), channel_id=1, source_target_pairs={{0,6},{2,0},{4,2},{6,4},{1,7},{3,1},{5,3},{7,5},{8,14},{10,8},{12,... | collective-permute-start | bytes 786440 | tf_op jit(solution)/shard_map/ppermute | solution.py:642
  134.3 2.1 %collective-permute-done.19.f1 = bf16[512,256]{1,0:T(8,128)(2,1)S(1)} collective-permute-done((bf16[512,256]{1,0:T(8,128)(2,1)S(1)}, bf16[512,256]{1,0:T(8,128)(2,1)S(1)}, u32[]{:S(2)}, u32[]{:S(2)}) %collective-permute-start.19) | collective-permute-done | bytes 262176 | tf_op jit(solution)/shard_map/ppermute | solution.py:642
  138.2 8.6 %collective-permute-done.20.f2 = bf16[512,256]{1,0:T(8,128)(2,1)S(1)} collective-permute-done((bf16[512,256]{1,0:T(8,128)(2,1)S(1)}, bf16[512,256]{1,0:T(8,128)(2,1)S(1)}, u32[]{:S(2)}, u32[]{:S(2)}) %collective-permute-start.20) | collective-permute-done | bytes 262176 | tf_op jit(solution)/shard_map/ppermute | solution.py:642
  147.0 5.3 %collective-permute-done.35.f2 = bf16[512,256]{1,0:T(8,128)(2,1)S(1)} collective-permute-done((bf16[512,256]{1,0:T(8,128)(2,1)S(1)}, bf16[512,256]{1,0:T(8,128)(2,1)S(1)}, u32[]{:S(2)}, u32[]{:S(2)}) %collective-permute-start.35) | collective-permute-done | bytes 262176 | tf_op jit(solution)/shard_map/ppermute | solution.py:642
  (92 shorter events, 42.0 us)
Async XLA Ops:
  6.5 101.5 %all-gather.2.cloned.1.call-start = ((), (), s32[]{:S(2)}) async-start(), calls=%async_computation | async-start | bytes 9191424 | tf_op jit(solution)/shard_map/all_gather | solution.py:678
  18.5 11.8 %collective-permute-start.3 = (bf16[144,512]{1,0:T(8,128)(2,1)S(1)}, bf16[144,512]{1,0:T(8,128)(2,1)S(1)}, u32[]{:S(2)}, u32[]{:S(2)}) collective-permute-start(bf16[144,512]{1,0:T(8,128)(2,1)S(1)} %get-tuple-element.69.r0), channel_id=1, source_target_pairs={{0,24},{8,0},{16,8},{24,16},{1,25},{9,1},{17,9},{25,17},{2,26},{10... | collective-permute-start | bytes 442376 | tf_op jit(solution)/shard_map/ppermute | solution.py:642
  22.3 11.0 %collective-permute-start.2 = (bf16[144,512]{1,0:T(8,128)(2,1)S(1)}, bf16[144,512]{1,0:T(8,128)(2,1)S(1)}, u32[]{:S(2)}, u32[]{:S(2)}) collective-permute-start(bf16[144,512]{1,0:T(8,128)(2,1)S(1)} %get-tuple-element.69.r0), channel_id=1, source_target_pairs={{0,16},{8,24},{16,0},{24,8},{1,17},{9,25},{17,1},{25,9},{2,18},{10... | collective-permute-start | bytes 442376 | tf_op jit(solution)/shard_map/ppermute | solution.py:642
  22.9 12.1 %collective-permute-start.1 = (bf16[144,512]{1,0:T(8,128)(2,1)S(1)}, bf16[144,512]{1,0:T(8,128)(2,1)S(1)}, u32[]{:S(2)}, u32[]{:S(2)}) collective-permute-start(bf16[144,512]{1,0:T(8,128)(2,1)S(1)} %get-tuple-element.69.r0), channel_id=1, source_target_pairs={{0,8},{8,16},{16,24},{24,0},{1,9},{9,17},{17,25},{25,1},{2,10},{10... | collective-permute-start | bytes 442376 | tf_op jit(solution)/shard_map/ppermute | solution.py:642
  35.3 11.2 %collective-permute-start.6 = (bf16[144,512]{1,0:T(8,128)(2,1)S(1)}, bf16[144,512]{1,0:T(8,128)(2,1)S(1)}, u32[]{:S(2)}, u32[]{:S(2)}) collective-permute-start(bf16[144,512]{1,0:T(8,128)(2,1)S(1)} %get-tuple-element.70.q0), channel_id=1, source_target_pairs={{0,96},{32,0},{64,32},{96,64},{1,97},{33,1},{65,33},{97,65},{2,98}... | collective-permute-start | bytes 442376 | tf_op jit(solution)/shard_map/ppermute | solution.py:642
  60.6 16.0 %collective-permute-start.24 = (bf16[512,256]{1,0:T(8,128)(2,1)S(1)}, bf16[512,256]{1,0:T(8,128)(2,1)S(1)}, u32[]{:S(2)}, u32[]{:S(2)}) collective-permute-start(bf16[512,256]{1,0:T(8,128)(2,1)S(1)} %get-tuple-element.101), channel_id=1, source_target_pairs={{0,2},{2,4},{4,6},{6,0},{1,3},{3,5},{5,7},{7,1},{8,10},{10,12},{12... | collective-permute-start | bytes 786440 | tf_op jit(solution)/shard_map/ppermute | solution.py:642
  61.2 15.4 %collective-permute-start.25 = (bf16[512,256]{1,0:T(8,128)(2,1)S(1)}, bf16[512,256]{1,0:T(8,128)(2,1)S(1)}, u32[]{:S(2)}, u32[]{:S(2)}) collective-permute-start(bf16[512,256]{1,0:T(8,128)(2,1)S(1)} %get-tuple-element.102), channel_id=1, source_target_pairs={{0,6},{2,0},{4,2},{6,4},{1,7},{3,1},{5,3},{7,5},{8,14},{10,8},{12,... | collective-permute-start | bytes 786440 | tf_op jit(solution)/shard_map/ppermute | solution.py:642
  64.1 17.4 %collective-permute-start.8 = (bf16[512,256]{1,0:T(8,128)(2,1)S(1)}, bf16[512,256]{1,0:T(8,128)(2,1)S(1)}, u32[]{:S(2)}, u32[]{:S(2)}) collective-permute-start(bf16[512,256]{1,0:T(8,128)(2,1)S(1)} %get-tuple-element.85), channel_id=1, source_target_pairs={{0,4},{2,6},{4,0},{6,2},{1,5},{3,7},{5,1},{7,3},{8,12},{10,14},{12... | collective-permute-start | bytes 786440 | tf_op jit(solution)/shard_map/ppermute | solution.py:642
  64.4 18.6 %collective-permute-start.9 = (bf16[512,256]{1,0:T(8,128)(2,1)S(1)}, bf16[512,256]{1,0:T(8,128)(2,1)S(1)}, u32[]{:S(2)}, u32[]{:S(2)}) collective-permute-start(bf16[512,256]{1,0:T(8,128)(2,1)S(1)} %get-tuple-element.86), channel_id=1, source_target_pairs={{0,2},{2,4},{4,6},{6,0},{1,3},{3,5},{5,7},{7,1},{8,10},{10,12},{12... | collective-permute-start | bytes 786440 | tf_op jit(solution)/shard_map/ppermute | solution.py:642
  66.9 17.0 %collective-permute-start.10 = (bf16[512,256]{1,0:T(8,128)(2,1)S(1)}, bf16[512,256]{1,0:T(8,128)(2,1)S(1)}, u32[]{:S(2)}, u32[]{:S(2)}) collective-permute-start(bf16[512,256]{1,0:T(8,128)(2,1)S(1)} %get-tuple-element.87), channel_id=1, source_target_pairs={{0,6},{2,0},{4,2},{6,4},{1,7},{3,1},{5,3},{7,5},{8,14},{10,8},{12,... | collective-permute-start | bytes 786440 | tf_op jit(solution)/shard_map/ppermute | solution.py:642
  76.8 16.6 %collective-permute-start.28 = (bf16[512,256]{1,0:T(8,128)(2,1)S(1)}, bf16[512,256]{1,0:T(8,128)(2,1)S(1)}, u32[]{:S(2)}, u32[]{:S(2)}) collective-permute-start(bf16[512,256]{1,0:T(8,128)(2,1)S(1)} %own.3.m0), channel_id=1, source_target_pairs={{0,2},{2,4},{4,6},{6,0},{1,3},{3,5},{5,7},{7,1},{8,10},{10,12},{12... | collective-permute-start | bytes 786440 | tf_op jit(solution)/shard_map/ppermute | solution.py:642
  76.8 18.3 %collective-permute-start.27 = (bf16[512,256]{1,0:T(8,128)(2,1)S(1)}, bf16[512,256]{1,0:T(8,128)(2,1)S(1)}, u32[]{:S(2)}, u32[]{:S(2)}) collective-permute-start(bf16[512,256]{1,0:T(8,128)(2,1)S(1)} %own.3.m0), channel_id=1, source_target_pairs={{0,4},{2,6},{4,0},{6,2},{1,5},{3,7},{5,1},{7,3},{8,12},{10,14},{12... | collective-permute-start | bytes 786440 | tf_op jit(solution)/shard_map/ppermute | solution.py:642
  84.1 16.5 %collective-permute-start.13 = (bf16[512,256]{1,0:T(8,128)(2,1)S(1)}, bf16[512,256]{1,0:T(8,128)(2,1)S(1)}, u32[]{:S(2)}, u32[]{:S(2)}) collective-permute-start(bf16[512,256]{1,0:T(8,128)(2,1)S(1)} %own.2.m0), channel_id=1, source_target_pairs={{0,2},{2,4},{4,6},{6,0},{1,3},{3,5},{5,7},{7,1},{8,10},{10,12},{12... | collective-permute-start | bytes 786440 | tf_op jit(solution)/shard_map/ppermute | solution.py:642
  85.7 19.8 %collective-permute-start.12 = (bf16[512,256]{1,0:T(8,128)(2,1)S(1)}, bf16[512,256]{1,0:T(8,128)(2,1)S(1)}, u32[]{:S(2)}, u32[]{:S(2)}) collective-permute-start(bf16[512,256]{1,0:T(8,128)(2,1)S(1)} %own.2.m0), channel_id=1, source_target_pairs={{0,4},{2,6},{4,0},{6,2},{1,5},{3,7},{5,1},{7,3},{8,12},{10,14},{12... | collective-permute-start | bytes 786440 | tf_op jit(solution)/shard_map/ppermute | solution.py:642
  88.2 17.2 %collective-permute-start.11 = (bf16[512,256]{1,0:T(8,128)(2,1)S(1)}, bf16[512,256]{1,0:T(8,128)(2,1)S(1)}, u32[]{:S(2)}, u32[]{:S(2)}) collective-permute-start(bf16[512,256]{1,0:T(8,128)(2,1)S(1)} %own.2.m0), channel_id=1, source_target_pairs={{0,6},{2,0},{4,2},{6,4},{1,7},{3,1},{5,3},{7,5},{8,14},{10,8},{12,... | collective-permute-start | bytes 786440 | tf_op jit(solution)/shard_map/ppermute | solution.py:642
  93.4 12.5 %collective-permute-start.26 = (bf16[512,256]{1,0:T(8,128)(2,1)S(1)}, bf16[512,256]{1,0:T(8,128)(2,1)S(1)}, u32[]{:S(2)}, u32[]{:S(2)}) collective-permute-start(bf16[512,256]{1,0:T(8,128)(2,1)S(1)} %own.3.m0), channel_id=1, source_target_pairs={{0,6},{2,0},{4,2},{6,4},{1,7},{3,1},{5,3},{7,5},{8,14},{10,8},{12,... | collective-permute-start | bytes 786440 | tf_op jit(solution)/shard_map/ppermute | solution.py:642
  95.1 10.9 %collective-permute-start.14 = (bf16[512,256]{1,0:T(8,128)(2,1)S(1)}, bf16[512,256]{1,0:T(8,128)(2,1)S(1)}, u32[]{:S(2)}, u32[]{:S(2)}) collective-permute-start(bf16[512,256]{1,0:T(8,128)(2,1)S(1)} %own.2.m0), channel_id=1, source_target_pairs={{0,1},{1,0},{2,3},{3,2},{4,5},{5,4},{6,7},{7,6},{8,9},{9,8},{10,11... | collective-permute-start | bytes 786440 | tf_op jit(solution)/shard_map/ppermute | solution.py:646
  105.9 10.9 %collective-permute-start.29 = (bf16[512,256]{1,0:T(8,128)(2,1)S(1)}, bf16[512,256]{1,0:T(8,128)(2,1)S(1)}, u32[]{:S(2)}, u32[]{:S(2)}) collective-permute-start(bf16[512,256]{1,0:T(8,128)(2,1)S(1)} %own.3.m0), channel_id=1, source_target_pairs={{0,1},{1,0},{2,3},{3,2},{4,5},{5,4},{6,7},{7,6},{8,9},{9,8},{10,11... | collective-permute-start | bytes 786440 | tf_op jit(solution)/shard_map/ppermute | solution.py:646
  125.5 10.9 %collective-permute-start.19 = (bf16[512,256]{1,0:T(8,128)(2,1)S(1)}, bf16[512,256]{1,0:T(8,128)(2,1)S(1)}, u32[]{:S(2)}, u32[]{:S(2)}) collective-permute-start(bf16[512,256]{1,0:T(8,128)(2,1)S(1)} %get-tuple-element.94), channel_id=1, source_target_pairs={{0,4},{2,6},{4,0},{6,2},{1,5},{3,7},{5,1},{7,3},{8,12},{10,14},{12... | collective-permute-start | bytes 786440 | tf_op jit(solution)/shard_map/ppermute | solution.py:642
  130.5 16.5 %collective-permute-start.34 = (bf16[512,256]{1,0:T(8,128)(2,1)S(1)}, bf16[512,256]{1,0:T(8,128)(2,1)S(1)}, u32[]{:S(2)}, u32[]{:S(2)}) collective-permute-start(bf16[512,256]{1,0:T(8,128)(2,1)S(1)} %get-tuple-element.106), channel_id=1, source_target_pairs={{0,4},{2,6},{4,0},{6,2},{1,5},{3,7},{5,1},{7,3},{8,12},{10,14},{12... | collective-permute-start | bytes 786440 | tf_op jit(solution)/shard_map/ppermute | solution.py:642
  131.0 15.8 %collective-permute-start.20 = (bf16[512,256]{1,0:T(8,128)(2,1)S(1)}, bf16[512,256]{1,0:T(8,128)(2,1)S(1)}, u32[]{:S(2)}, u32[]{:S(2)}) collective-permute-start(bf16[512,256]{1,0:T(8,128)(2,1)S(1)} %get-tuple-element.95), channel_id=1, source_target_pairs={{0,2},{2,4},{4,6},{6,0},{1,3},{3,5},{5,7},{7,1},{8,10},{10,12},{12... | collective-permute-start | bytes 786440 | tf_op jit(solution)/shard_map/ppermute | solution.py:642
  131.6 15.2 %collective-permute-start.21 = (bf16[512,256]{1,0:T(8,128)(2,1)S(1)}, bf16[512,256]{1,0:T(8,128)(2,1)S(1)}, u32[]{:S(2)}, u32[]{:S(2)}) collective-permute-start(bf16[512,256]{1,0:T(8,128)(2,1)S(1)} %get-tuple-element.96), channel_id=1, source_target_pairs={{0,6},{2,0},{4,2},{6,4},{1,7},{3,1},{5,3},{7,5},{8,14},{10,8},{12,... | collective-permute-start | bytes 786440 | tf_op jit(solution)/shard_map/ppermute | solution.py:642
  134.3 18.1 %collective-permute-start.35 = (bf16[512,256]{1,0:T(8,128)(2,1)S(1)}, bf16[512,256]{1,0:T(8,128)(2,1)S(1)}, u32[]{:S(2)}, u32[]{:S(2)}) collective-permute-start(bf16[512,256]{1,0:T(8,128)(2,1)S(1)} %get-tuple-element.107), channel_id=1, source_target_pairs={{0,2},{2,4},{4,6},{6,0},{1,3},{3,5},{5,7},{7,1},{8,10},{10,12},{12... | collective-permute-start | bytes 786440 | tf_op jit(solution)/shard_map/ppermute | solution.py:642
  136.4 15.9 %collective-permute-start.36 = (bf16[512,256]{1,0:T(8,128)(2,1)S(1)}, bf16[512,256]{1,0:T(8,128)(2,1)S(1)}, u32[]{:S(2)}, u32[]{:S(2)}) collective-permute-start(bf16[512,256]{1,0:T(8,128)(2,1)S(1)} %get-tuple-element.108), channel_id=1, source_target_pairs={{0,6},{2,0},{4,2},{6,4},{1,7},{3,1},{5,3},{7,5},{8,14},{10,8},{12,... | collective-permute-start | bytes 786440 | tf_op jit(solution)/shard_map/ppermute | solution.py:642
  (21 other events, 197.0 us)
Sparse Core Ops, SparseCore 0:
  9.5 81.2 all-gather.1

commit v3 on v2

--- a/solution.py
+++ b/solution.py
@@ -218,7 +218,7 @@
         carry[...] = old * spread(ends[b], 64, 2) + added
         return 0
 
-    lax.fori_loop(0, NB, block, 0, unroll=4)
+    lax.fori_loop(0, NB, block, 0, unroll=8)
     payload[0:ST, :] = carry[...].astype(BF)
     high = total[...].astype(BF)
     low = (total[...] - high.astype(F32)).astype(BF)
@@ -387,7 +387,7 @@
         mixed[pl.ds(pl.multiple_of(b * BLK, BLK), BLK), :] = (gated * scale * rescale).astype(BF)
         return 0
 
-    lax.fori_loop(0, count // BLK, block, 0, unroll=2)
+    lax.fori_loop(0, count // BLK, block, 0, unroll=4)
     project(order, 4, mixed, blend, send)
 
 
@@ -655,6 +655,11 @@
 def gather_chips(own):
     far = turn(own, "x", 2)
     return own, turn(own, "x", -1), far, turn(own, "x", 1)
+
+
+def exchange(payload, axis):
+    far = turn(payload, axis, 2)
+    return [payload, turn(payload, axis, 1), far, turn(payload, axis, 3)]
 
 
 def shards(
@@ -681,13 +686,13 @@
     values, maps, entering, payload = state_kernel(
         content, pairs, halo, factors, ends, total, taps_c, taps_p
     )
-    line = [payload] + [turn(payload, "y", d) for d in (1, 2, 3)]
+    line = exchange(payload, "y")
     local, opened = local_kernel(
         values, maps, cum, step, entering, skip, gate, blender
     )
     mine_cols = cols_kernel(first_col, arriving)
     payload_z, prefix, ahead = line_kernel(y, line)
-    lines = [payload_z] + [turn(payload_z, "z", d) for d in (1, 2, 3)]
+    lines = exchange(payload_z, "z")
     incoming = incoming_kernel(z, lines, prefix, ahead)
     gain = norm_gain.reshape(1, D)
     mix_args = (incoming, local, maps, tot, opened, cluster_gain.reshape(1, CH), blender)

time: 161 us -> 161 us (level)
  no operation moved by 1% of the time
where the time goes in v3:
time: 161 us; the launch traced here: 159 us
  waiting for transfers between devices  58 us (36%)
  starting transfers between devices  45.8 us (28%)
  Pallas kernels  37.8 us (23%)
  between operations  13.6 us (8%)
  local copies, waits for them, and re-layouts  4.02 us (2%)
    ppermute x24, waiting for transfers between devices, turn(): lax.ppermute(array, axis, [(i, (i + distance) % count) for i in range(cou...  56.9 us
    ppermute x24, starting transfers between devices, turn(): lax.ppermute(array, axis, [(i, (i + distance) % count) for i in range(cou...  39.4 us
    pallas_call x2, Pallas kernels, ffn_kernel(): pl.pallas_call(ffn_first_body if first else ffn_next_body, out_shape=shap...  13.8 us
    pallas_call x1, Pallas kernels, local_kernel(): pl.pallas_call(local_body, out_shape=(sds((T, CH), F32), sds((T, CH), F32...  4.39 us
    pallas_call x1, Pallas kernels, state_kernel(): pl.pallas_call(state_body, out_shape=(sds((T, CH), BF), sds((T, 256), BF)...  4.37 us
    unnamed x15, local copies, waits for them, and re-layouts  4.02 us
    ppermute x1, starting transfers between devices, shards(): halo = lax.ppermute(tail, SP, [(i, i + 1) for i in range(15)])  3.59 us
    pallas_call x2, Pallas kernels, mix_kernel(): pl.pallas_call(functools.partial(mix_body, start, count), out_shape=(sds(...  3.49 us
  transfers between devices with their start and end apart: 38, of which 19 were waited for; matrix products, arithmetic and copies ran while one was open for 1% of the time, Pallas kernels for 22%

profile of v3, /device:TPU:0, one launch (start us, length us, event | category | flops | bytes accessed | tf_op | source)
XLA Modules:
  0.0 159.4 jit_solution(1241319813674342382)
XLA Ops:
  6.6 2.1 %head.1 = (bf16[2112,128]{1,0:T(8,128)(2,1)}, bf16[16,768]{1,0:T(8,128)(2,1)S(1)}, f32[8,1024]{1,0:T(8,128)S(1)}, f32[8,1024]{1,0:T(8,128)S(1)}, f32[8,1024]{1,0...) custom-call(bf16[704,128]{1,0:T(8,128)(2,1)} %bitcast.27, ...), custom_call_target="tpu_custom_call" | custom-call | tf_op jit(solution)/shard_map/head/pallas_call | solution.py:162
  8.7 3.6 %collective-permute-start = (bf16[16,768]{1,0:T(8,128)(2,1)S(1)}, bf16[16,768]{1,0:T(8,128)(2,1)S(1)}, u32[]{:S(2)}, u32[]{:S(2)}) collective-permute-start(bf16[16,768]{1,0:T(8,128)(2,1)S(1)} %get-tuple-element.63), channel_id=1, source_target_pairs={{0,8},{8,16},{16,24},{24,32},{32,40},{40,48},{48,56},{56,64},{64,7... | collective-permute-start | bytes 73736 | tf_op jit(solution)/shard_map/ppermute | solution.py:685
  13.9 4.4 %state.1 = (bf16[1024,512]{1,0:T(8,128)(2,1)S(1)}, bf16[1024,256]{1,0:T(8,128)(2,1)S(1)}, bf16[8,128,512]{2,1,0:T(8,128)(2,1)S(1)}, bf16[144,512]{1,0:T(8,128)(2,1)S(1)}) custom-call(bf16[1024,512]{1,0:T(8,128)(2,1)S(1)} %copy-done, bf16[1024,256]{1,0:T(8,128)(2,1)S(1)} %bitcast.20, bf16[16,768]{1,0:T(8,128)(2,1)S(1)} %collective-permute-done.halo, ...), custom_call_target="tpu_custom_call" | custom-call | tf_op jit(solution)/shard_map/state/pallas_call | solution.py:229
  18.2 3.8 %collective-permute-start.3 = (bf16[144,512]{1,0:T(8,128)(2,1)S(1)}, bf16[144,512]{1,0:T(8,128)(2,1)S(1)}, u32[]{:S(2)}, u32[]{:S(2)}) collective-permute-start(bf16[144,512]{1,0:T(8,128)(2,1)S(1)} %get-tuple-element.69.r0), channel_id=1, source_target_pairs={{0,24},{8,0},{16,8},{24,16},{1,25},{9,1},{17,9},{25,17},{2,26},{10... | collective-permute-start | bytes 442376 | tf_op jit(solution)/shard_map/ppermute | solution.py:642
  23.6 6.4 %collective-permute-done.3.r3 = bf16[144,512]{1,0:T(8,128)(2,1)S(1)} collective-permute-done((bf16[144,512]{1,0:T(8,128)(2,1)S(1)}, bf16[144,512]{1,0:T(8,128)(2,1)S(1)}, u32[]{:S(2)}, u32[]{:S(2)}) %collective-permute-start.3) | collective-permute-done | bytes 147488 | tf_op jit(solution)/shard_map/ppermute | solution.py:642
  30.0 2.8 %collective-permute-done.2.r2 = bf16[144,512]{1,0:T(8,128)(2,1)S(1)} collective-permute-done((bf16[144,512]{1,0:T(8,128)(2,1)S(1)}, bf16[144,512]{1,0:T(8,128)(2,1)S(1)}, u32[]{:S(2)}, u32[]{:S(2)}) %collective-permute-start.2) | collective-permute-done | bytes 147488 | tf_op jit(solution)/shard_map/ppermute | solution.py:642
  35.0 4.3 %collective-permute-start.6 = (bf16[144,512]{1,0:T(8,128)(2,1)S(1)}, bf16[144,512]{1,0:T(8,128)(2,1)S(1)}, u32[]{:S(2)}, u32[]{:S(2)}) collective-permute-start(bf16[144,512]{1,0:T(8,128)(2,1)S(1)} %get-tuple-element.70.q0), channel_id=1, source_target_pairs={{0,96},{32,0},{64,32},{96,64},{1,97},{33,1},{65,33},{97,65},{2,98}... | collective-permute-start | bytes 442376 | tf_op jit(solution)/shard_map/ppermute | solution.py:642
  41.7 4.4 %local.1 = (f32[1024,512]{1,0:T(8,128)S(1)}, f32[1024,512]{1,0:T(8,128)S(1)}) custom-call(bf16[1024,512]{1,0:T(8,128)(2,1)S(1)} %get-tuple-element.73.values, bf16[1024,256]{1,0:T(8,128)(2,1)S(1)} %get-tuple-element.74.maps, f32[8,1024]{1,0:T(8,128)S(1)} %get-tuple-element.75.cum_in, f32[8,1024]{1,0:T(8,128)S(1)} %get-tuple-element.76.step_in, ...), custom_call_target="tpu_custom_call" | custom-call | flops 6000000000 | bytes 6000000 | tf_op jit(solution)/shard_map/local/pallas_call | solution.py:295
  55.2 3.3 %collective-permute-start.23 = (bf16[512,256]{1,0:T(8,128)(2,1)S(1)}, bf16[512,256]{1,0:T(8,128)(2,1)S(1)}, u32[]{:S(2)}, u32[]{:S(2)}) collective-permute-start(bf16[512,256]{1,0:T(8,128)(2,1)S(1)} %get-tuple-element.100), channel_id=1, source_target_pairs={{0,4},{2,6},{4,0},{6,2},{1,5},{3,7},{5,1},{7,3},{8,12},{10,14},{12... | collective-permute-start | bytes 786440 | tf_op jit(solution)/shard_map/ppermute | solution.py:642
  60.4 2.7 %collective-permute-start.25 = (bf16[512,256]{1,0:T(8,128)(2,1)S(1)}, bf16[512,256]{1,0:T(8,128)(2,1)S(1)}, u32[]{:S(2)}, u32[]{:S(2)}) collective-permute-start(bf16[512,256]{1,0:T(8,128)(2,1)S(1)} %get-tuple-element.102), channel_id=1, source_target_pairs={{0,6},{2,0},{4,2},{6,4},{1,7},{3,1},{5,3},{7,5},{8,14},{10,8},{12,... | collective-permute-start | bytes 786440 | tf_op jit(solution)/shard_map/ppermute | solution.py:642
  66.2 2.7 %collective-permute-start.10 = (bf16[512,256]{1,0:T(8,128)(2,1)S(1)}, bf16[512,256]{1,0:T(8,128)(2,1)S(1)}, u32[]{:S(2)}, u32[]{:S(2)}) collective-permute-start(bf16[512,256]{1,0:T(8,128)(2,1)S(1)} %get-tuple-element.87), channel_id=1, source_target_pairs={{0,6},{2,0},{4,2},{6,4},{1,7},{3,1},{5,3},{7,5},{8,14},{10,8},{12,... | collective-permute-start | bytes 786440 | tf_op jit(solution)/shard_map/ppermute | solution.py:642
  70.0 5.8 %collective-permute-done.24.f2 = bf16[512,256]{1,0:T(8,128)(2,1)S(1)} collective-permute-done((bf16[512,256]{1,0:T(8,128)(2,1)S(1)}, bf16[512,256]{1,0:T(8,128)(2,1)S(1)}, u32[]{:S(2)}, u32[]{:S(2)}) %collective-permute-start.24) | collective-permute-done | bytes 262176 | tf_op jit(solution)/shard_map/ppermute | solution.py:642
  76.1 4.7 %collective-permute-start.27 = (bf16[512,256]{1,0:T(8,128)(2,1)S(1)}, bf16[512,256]{1,0:T(8,128)(2,1)S(1)}, u32[]{:S(2)}, u32[]{:S(2)}) collective-permute-start(bf16[512,256]{1,0:T(8,128)(2,1)S(1)} %own.3.m0), channel_id=1, source_target_pairs={{0,4},{2,6},{4,0},{6,2},{1,5},{3,7},{5,1},{7,3},{8,12},{10,14},{12... | collective-permute-start | bytes 786440 | tf_op jit(solution)/shard_map/ppermute | solution.py:642
  84.9 2.5 %collective-permute-start.12 = (bf16[512,256]{1,0:T(8,128)(2,1)S(1)}, bf16[512,256]{1,0:T(8,128)(2,1)S(1)}, u32[]{:S(2)}, u32[]{:S(2)}) collective-permute-start(bf16[512,256]{1,0:T(8,128)(2,1)S(1)} %own.2.m0), channel_id=1, source_target_pairs={{0,4},{2,6},{4,0},{6,2},{1,5},{3,7},{5,1},{7,3},{8,12},{10,14},{12... | collective-permute-start | bytes 786440 | tf_op jit(solution)/shard_map/ppermute | solution.py:642
  88.1 4.5 %collective-permute-done.28.m3 = bf16[512,256]{1,0:T(8,128)(2,1)S(1)} collective-permute-done((bf16[512,256]{1,0:T(8,128)(2,1)S(1)}, bf16[512,256]{1,0:T(8,128)(2,1)S(1)}, u32[]{:S(2)}, u32[]{:S(2)}) %collective-permute-start.28) | collective-permute-done | bytes 262176 | tf_op jit(solution)/shard_map/ppermute | solution.py:642
  94.4 5.4 %collective-permute-done.13.m3 = bf16[512,256]{1,0:T(8,128)(2,1)S(1)} collective-permute-done((bf16[512,256]{1,0:T(8,128)(2,1)S(1)}, bf16[512,256]{1,0:T(8,128)(2,1)S(1)}, u32[]{:S(2)}, u32[]{:S(2)}) %collective-permute-start.13) | collective-permute-done | bytes 262176 | tf_op jit(solution)/shard_map/ppermute | solution.py:642
  99.8 4.8 %collective-permute-done.12.m2 = bf16[512,256]{1,0:T(8,128)(2,1)S(1)} collective-permute-done((bf16[512,256]{1,0:T(8,128)(2,1)S(1)}, bf16[512,256]{1,0:T(8,128)(2,1)S(1)}, u32[]{:S(2)}, u32[]{:S(2)}) %collective-permute-start.12) | collective-permute-done | bytes 262176 | tf_op jit(solution)/shard_map/ppermute | solution.py:642
  108.2 7.4 %ffn.2 = (bf16[4,512,256]{2,1,0:T(8,128)(2,1)S(1)}, bf16[512,704]{1,0:T(8,128)(2,1)S(1)}, bf16[16,2112,128]{2,1,0:T(8,128)(2,1)S(1)}) custom-call(s32[8]{0:T(128)S(1)} %pad_add_fusion.order, bf16[16,2112,128]{2,1,0:T(8,128)(2,1)} %bitcast.35, f32[1,2048]{1,0:T(1,128)S(1)} %bitcast.21, bf16[512,256]{1,0:T(8,128)(2,1)S(1)} %own.2.m0, ...), custom_call_target="tpu_custom_call" | custom-call | flops 8999999488 | bytes 12000000 | tf_op jit(solution)/shard_map/ffn/pallas_call | solution.py:612
  116.1 6.4 %ffn.3 = (bf16[4,512,256]{2,1,0:T(8,128)(2,1)S(1)}, bf16[512,704]{1,0:T(8,128)(2,1)S(1)}) custom-call(s32[8]{0:T(128)S(1)} %pad_add_fusion.order, bf16[16,2112,128]{2,1,0:T(8,128)(2,1)S(1)} %get-tuple-element.91.weights, f32[1,2048]{1,0:T(1,128)S(1)} %bitcast.22, bf16[512,256]{1,0:T(8,128)(2,1)S(1)} %own.3.m0, ...), custom_call_target="tpu_custom_call" | custom-call | flops 8999999488 | bytes 12000000 | tf_op jit(solution)/shard_map/ffn/pallas_call | solution.py:612
  124.8 3.1 %collective-permute-start.19 = (bf16[512,256]{1,0:T(8,128)(2,1)S(1)}, bf16[512,256]{1,0:T(8,128)(2,1)S(1)}, u32[]{:S(2)}, u32[]{:S(2)}) collective-permute-start(bf16[512,256]{1,0:T(8,128)(2,1)S(1)} %get-tuple-element.94), channel_id=1, source_target_pairs={{0,4},{2,6},{4,0},{6,2},{1,5},{3,7},{5,1},{7,3},{8,12},{10,14},{12... | collective-permute-start | bytes 786440 | tf_op jit(solution)/shard_map/ppermute | solution.py:642
  130.9 2.6 %collective-permute-start.21 = (bf16[512,256]{1,0:T(8,128)(2,1)S(1)}, bf16[512,256]{1,0:T(8,128)(2,1)S(1)}, u32[]{:S(2)}, u32[]{:S(2)}) collective-permute-start(bf16[512,256]{1,0:T(8,128)(2,1)S(1)} %get-tuple-element.96), channel_id=1, source_target_pairs={{0,6},{2,0},{4,2},{6,4},{1,7},{3,1},{5,3},{7,5},{8,14},{10,8},{12,... | collective-permute-start | bytes 786440 | tf_op jit(solution)/shard_map/ppermute | solution.py:642
  133.5 2.1 %collective-permute-done.19.f1 = bf16[512,256]{1,0:T(8,128)(2,1)S(1)} collective-permute-done((bf16[512,256]{1,0:T(8,128)(2,1)S(1)}, bf16[512,256]{1,0:T(8,128)(2,1)S(1)}, u32[]{:S(2)}, u32[]{:S(2)}) %collective-permute-start.19) | collective-permute-done | bytes 262176 | tf_op jit(solution)/shard_map/ppermute | solution.py:642
  137.4 8.6 %collective-permute-done.20.f2 = bf16[512,256]{1,0:T(8,128)(2,1)S(1)} collective-permute-done((bf16[512,256]{1,0:T(8,128)(2,1)S(1)}, bf16[512,256]{1,0:T(8,128)(2,1)S(1)}, u32[]{:S(2)}, u32[]{:S(2)}) %collective-permute-start.20) | collective-permute-done | bytes 262176 | tf_op jit(solution)/shard_map/ppermute | solution.py:642
  146.2 5.3 %collective-permute-done.35.f2 = bf16[512,256]{1,0:T(8,128)(2,1)S(1)} collective-permute-done((bf16[512,256]{1,0:T(8,128)(2,1)S(1)}, bf16[512,256]{1,0:T(8,128)(2,1)S(1)}, u32[]{:S(2)}, u32[]{:S(2)}) %collective-permute-start.35) | collective-permute-done | bytes 262176 | tf_op jit(solution)/shard_map/ppermute | solution.py:642
  (92 shorter events, 41.8 us)
Async XLA Ops:
  6.5 100.7 %all-gather.2.cloned.1.call-start = ((), (), s32[]{:S(2)}) async-start(), calls=%async_computation | async-start | bytes 9191424 | tf_op jit(solution)/shard_map/all_gather | solution.py:683
  18.2 11.8 %collective-permute-start.3 = (bf16[144,512]{1,0:T(8,128)(2,1)S(1)}, bf16[144,512]{1,0:T(8,128)(2,1)S(1)}, u32[]{:S(2)}, u32[]{:S(2)}) collective-permute-start(bf16[144,512]{1,0:T(8,128)(2,1)S(1)} %get-tuple-element.69.r0), channel_id=1, source_target_pairs={{0,24},{8,0},{16,8},{24,16},{1,25},{9,1},{17,9},{25,17},{2,26},{10... | collective-permute-start | bytes 442376 | tf_op jit(solution)/shard_map/ppermute | solution.py:642
  22.7 12.1 %collective-permute-start.1 = (bf16[144,512]{1,0:T(8,128)(2,1)S(1)}, bf16[144,512]{1,0:T(8,128)(2,1)S(1)}, u32[]{:S(2)}, u32[]{:S(2)}) collective-permute-start(bf16[144,512]{1,0:T(8,128)(2,1)S(1)} %get-tuple-element.69.r0), channel_id=1, source_target_pairs={{0,8},{8,16},{16,24},{24,0},{1,9},{9,17},{17,25},{25,1},{2,10},{10... | collective-permute-start | bytes 442376 | tf_op jit(solution)/shard_map/ppermute | solution.py:642
  35.0 11.1 %collective-permute-start.6 = (bf16[144,512]{1,0:T(8,128)(2,1)S(1)}, bf16[144,512]{1,0:T(8,128)(2,1)S(1)}, u32[]{:S(2)}, u32[]{:S(2)}) collective-permute-start(bf16[144,512]{1,0:T(8,128)(2,1)S(1)} %get-tuple-element.70.q0), channel_id=1, source_target_pairs={{0,96},{32,0},{64,32},{96,64},{1,97},{33,1},{65,33},{97,65},{2,98}... | collective-permute-start | bytes 442376 | tf_op jit(solution)/shard_map/ppermute | solution.py:642
  55.2 10.9 %collective-permute-start.23 = (bf16[512,256]{1,0:T(8,128)(2,1)S(1)}, bf16[512,256]{1,0:T(8,128)(2,1)S(1)}, u32[]{:S(2)}, u32[]{:S(2)}) collective-permute-start(bf16[512,256]{1,0:T(8,128)(2,1)S(1)} %get-tuple-element.100), channel_id=1, source_target_pairs={{0,4},{2,6},{4,0},{6,2},{1,5},{3,7},{5,1},{7,3},{8,12},{10,14},{12... | collective-permute-start | bytes 786440 | tf_op jit(solution)/shard_map/ppermute | solution.py:642
  59.8 16.0 %collective-permute-start.24 = (bf16[512,256]{1,0:T(8,128)(2,1)S(1)}, bf16[512,256]{1,0:T(8,128)(2,1)S(1)}, u32[]{:S(2)}, u32[]{:S(2)}) collective-permute-start(bf16[512,256]{1,0:T(8,128)(2,1)S(1)} %get-tuple-element.101), channel_id=1, source_target_pairs={{0,2},{2,4},{4,6},{6,0},{1,3},{3,5},{5,7},{7,1},{8,10},{10,12},{12... | collective-permute-start | bytes 786440 | tf_op jit(solution)/shard_map/ppermute | solution.py:642
  60.4 15.4 %collective-permute-start.25 = (bf16[512,256]{1,0:T(8,128)(2,1)S(1)}, bf16[512,256]{1,0:T(8,128)(2,1)S(1)}, u32[]{:S(2)}, u32[]{:S(2)}) collective-permute-start(bf16[512,256]{1,0:T(8,128)(2,1)S(1)} %get-tuple-element.102), channel_id=1, source_target_pairs={{0,6},{2,0},{4,2},{6,4},{1,7},{3,1},{5,3},{7,5},{8,14},{10,8},{12,... | collective-permute-start | bytes 786440 | tf_op jit(solution)/shard_map/ppermute | solution.py:642
  63.3 17.4 %collective-permute-start.8 = (bf16[512,256]{1,0:T(8,128)(2,1)S(1)}, bf16[512,256]{1,0:T(8,128)(2,1)S(1)}, u32[]{:S(2)}, u32[]{:S(2)}) collective-permute-start(bf16[512,256]{1,0:T(8,128)(2,1)S(1)} %get-tuple-element.85), channel_id=1, source_target_pairs={{0,4},{2,6},{4,0},{6,2},{1,5},{3,7},{5,1},{7,3},{8,12},{10,14},{12... | collective-permute-start | bytes 786440 | tf_op jit(solution)/shard_map/ppermute | solution.py:642
  63.4 18.8 %collective-permute-start.9 = (bf16[512,256]{1,0:T(8,128)(2,1)S(1)}, bf16[512,256]{1,0:T(8,128)(2,1)S(1)}, u32[]{:S(2)}, u32[]{:S(2)}) collective-permute-start(bf16[512,256]{1,0:T(8,128)(2,1)S(1)} %get-tuple-element.86), channel_id=1, source_target_pairs={{0,2},{2,4},{4,6},{6,0},{1,3},{3,5},{5,7},{7,1},{8,10},{10,12},{12... | collective-permute-start | bytes 786440 | tf_op jit(solution)/shard_map/ppermute | solution.py:642
  66.2 17.0 %collective-permute-start.10 = (bf16[512,256]{1,0:T(8,128)(2,1)S(1)}, bf16[512,256]{1,0:T(8,128)(2,1)S(1)}, u32[]{:S(2)}, u32[]{:S(2)}) collective-permute-start(bf16[512,256]{1,0:T(8,128)(2,1)S(1)} %get-tuple-element.87), channel_id=1, source_target_pairs={{0,6},{2,0},{4,2},{6,4},{1,7},{3,1},{5,3},{7,5},{8,14},{10,8},{12,... | collective-permute-start | bytes 786440 | tf_op jit(solution)/shard_map/ppermute | solution.py:642
  76.0 16.6 %collective-permute-start.28 = (bf16[512,256]{1,0:T(8,128)(2,1)S(1)}, bf16[512,256]{1,0:T(8,128)(2,1)S(1)}, u32[]{:S(2)}, u32[]{:S(2)}) collective-permute-start(bf16[512,256]{1,0:T(8,128)(2,1)S(1)} %own.3.m0), channel_id=1, source_target_pairs={{0,2},{2,4},{4,6},{6,0},{1,3},{3,5},{5,7},{7,1},{8,10},{10,12},{12... | collective-permute-start | bytes 786440 | tf_op jit(solution)/shard_map/ppermute | solution.py:642
  76.1 18.3 %collective-permute-start.27 = (bf16[512,256]{1,0:T(8,128)(2,1)S(1)}, bf16[512,256]{1,0:T(8,128)(2,1)S(1)}, u32[]{:S(2)}, u32[]{:S(2)}) collective-permute-start(bf16[512,256]{1,0:T(8,128)(2,1)S(1)} %own.3.m0), channel_id=1, source_target_pairs={{0,4},{2,6},{4,0},{6,2},{1,5},{3,7},{5,1},{7,3},{8,12},{10,14},{12... | collective-permute-start | bytes 786440 | tf_op jit(solution)/shard_map/ppermute | solution.py:642
  83.3 16.5 %collective-permute-start.13 = (bf16[512,256]{1,0:T(8,128)(2,1)S(1)}, bf16[512,256]{1,0:T(8,128)(2,1)S(1)}, u32[]{:S(2)}, u32[]{:S(2)}) collective-permute-start(bf16[512,256]{1,0:T(8,128)(2,1)S(1)} %own.2.m0), channel_id=1, source_target_pairs={{0,2},{2,4},{4,6},{6,0},{1,3},{3,5},{5,7},{7,1},{8,10},{10,12},{12... | collective-permute-start | bytes 786440 | tf_op jit(solution)/shard_map/ppermute | solution.py:642
  84.9 19.8 %collective-permute-start.12 = (bf16[512,256]{1,0:T(8,128)(2,1)S(1)}, bf16[512,256]{1,0:T(8,128)(2,1)S(1)}, u32[]{:S(2)}, u32[]{:S(2)}) collective-permute-start(bf16[512,256]{1,0:T(8,128)(2,1)S(1)} %own.2.m0), channel_id=1, source_target_pairs={{0,4},{2,6},{4,0},{6,2},{1,5},{3,7},{5,1},{7,3},{8,12},{10,14},{12... | collective-permute-start | bytes 786440 | tf_op jit(solution)/shard_map/ppermute | solution.py:642
  87.4 17.2 %collective-permute-start.11 = (bf16[512,256]{1,0:T(8,128)(2,1)S(1)}, bf16[512,256]{1,0:T(8,128)(2,1)S(1)}, u32[]{:S(2)}, u32[]{:S(2)}) collective-permute-start(bf16[512,256]{1,0:T(8,128)(2,1)S(1)} %own.2.m0), channel_id=1, source_target_pairs={{0,6},{2,0},{4,2},{6,4},{1,7},{3,1},{5,3},{7,5},{8,14},{10,8},{12,... | collective-permute-start | bytes 786440 | tf_op jit(solution)/shard_map/ppermute | solution.py:642
  92.6 12.5 %collective-permute-start.26 = (bf16[512,256]{1,0:T(8,128)(2,1)S(1)}, bf16[512,256]{1,0:T(8,128)(2,1)S(1)}, u32[]{:S(2)}, u32[]{:S(2)}) collective-permute-start(bf16[512,256]{1,0:T(8,128)(2,1)S(1)} %own.3.m0), channel_id=1, source_target_pairs={{0,6},{2,0},{4,2},{6,4},{1,7},{3,1},{5,3},{7,5},{8,14},{10,8},{12,... | collective-permute-start | bytes 786440 | tf_op jit(solution)/shard_map/ppermute | solution.py:642
  94.4 10.9 %collective-permute-start.14 = (bf16[512,256]{1,0:T(8,128)(2,1)S(1)}, bf16[512,256]{1,0:T(8,128)(2,1)S(1)}, u32[]{:S(2)}, u32[]{:S(2)}) collective-permute-start(bf16[512,256]{1,0:T(8,128)(2,1)S(1)} %own.2.m0), channel_id=1, source_target_pairs={{0,1},{1,0},{2,3},{3,2},{4,5},{5,4},{6,7},{7,6},{8,9},{9,8},{10,11... | collective-permute-start | bytes 786440 | tf_op jit(solution)/shard_map/ppermute | solution.py:646
  105.2 10.9 %collective-permute-start.29 = (bf16[512,256]{1,0:T(8,128)(2,1)S(1)}, bf16[512,256]{1,0:T(8,128)(2,1)S(1)}, u32[]{:S(2)}, u32[]{:S(2)}) collective-permute-start(bf16[512,256]{1,0:T(8,128)(2,1)S(1)} %own.3.m0), channel_id=1, source_target_pairs={{0,1},{1,0},{2,3},{3,2},{4,5},{5,4},{6,7},{7,6},{8,9},{9,8},{10,11... | collective-permute-start | bytes 786440 | tf_op jit(solution)/shard_map/ppermute | solution.py:646
  124.8 10.9 %collective-permute-start.19 = (bf16[512,256]{1,0:T(8,128)(2,1)S(1)}, bf16[512,256]{1,0:T(8,128)(2,1)S(1)}, u32[]{:S(2)}, u32[]{:S(2)}) collective-permute-start(bf16[512,256]{1,0:T(8,128)(2,1)S(1)} %get-tuple-element.94), channel_id=1, source_target_pairs={{0,4},{2,6},{4,0},{6,2},{1,5},{3,7},{5,1},{7,3},{8,12},{10,14},{12... | collective-permute-start | bytes 786440 | tf_op jit(solution)/shard_map/ppermute | solution.py:642
  129.7 16.5 %collective-permute-start.34 = (bf16[512,256]{1,0:T(8,128)(2,1)S(1)}, bf16[512,256]{1,0:T(8,128)(2,1)S(1)}, u32[]{:S(2)}, u32[]{:S(2)}) collective-permute-start(bf16[512,256]{1,0:T(8,128)(2,1)S(1)} %get-tuple-element.106), channel_id=1, source_target_pairs={{0,4},{2,6},{4,0},{6,2},{1,5},{3,7},{5,1},{7,3},{8,12},{10,14},{12... | collective-permute-start | bytes 786440 | tf_op jit(solution)/shard_map/ppermute | solution.py:642
  130.2 15.8 %collective-permute-start.20 = (bf16[512,256]{1,0:T(8,128)(2,1)S(1)}, bf16[512,256]{1,0:T(8,128)(2,1)S(1)}, u32[]{:S(2)}, u32[]{:S(2)}) collective-permute-start(bf16[512,256]{1,0:T(8,128)(2,1)S(1)} %get-tuple-element.95), channel_id=1, source_target_pairs={{0,2},{2,4},{4,6},{6,0},{1,3},{3,5},{5,7},{7,1},{8,10},{10,12},{12... | collective-permute-start | bytes 786440 | tf_op jit(solution)/shard_map/ppermute | solution.py:642
  130.9 15.1 %collective-permute-start.21 = (bf16[512,256]{1,0:T(8,128)(2,1)S(1)}, bf16[512,256]{1,0:T(8,128)(2,1)S(1)}, u32[]{:S(2)}, u32[]{:S(2)}) collective-permute-start(bf16[512,256]{1,0:T(8,128)(2,1)S(1)} %get-tuple-element.96), channel_id=1, source_target_pairs={{0,6},{2,0},{4,2},{6,4},{1,7},{3,1},{5,3},{7,5},{8,14},{10,8},{12,... | collective-permute-start | bytes 786440 | tf_op jit(solution)/shard_map/ppermute | solution.py:642
  133.5 18.1 %collective-permute-start.35 = (bf16[512,256]{1,0:T(8,128)(2,1)S(1)}, bf16[512,256]{1,0:T(8,128)(2,1)S(1)}, u32[]{:S(2)}, u32[]{:S(2)}) collective-permute-start(bf16[512,256]{1,0:T(8,128)(2,1)S(1)} %get-tuple-element.107), channel_id=1, source_target_pairs={{0,2},{2,4},{4,6},{6,0},{1,3},{3,5},{5,7},{7,1},{8,10},{10,12},{12... | collective-permute-start | bytes 786440 | tf_op jit(solution)/shard_map/ppermute | solution.py:642
  135.6 15.9 %collective-permute-start.36 = (bf16[512,256]{1,0:T(8,128)(2,1)S(1)}, bf16[512,256]{1,0:T(8,128)(2,1)S(1)}, u32[]{:S(2)}, u32[]{:S(2)}) collective-permute-start(bf16[512,256]{1,0:T(8,128)(2,1)S(1)} %get-tuple-element.108), channel_id=1, source_target_pairs={{0,6},{2,0},{4,2},{6,4},{1,7},{3,1},{5,3},{7,5},{8,14},{10,8},{12,... | collective-permute-start | bytes 786440 | tf_op jit(solution)/shard_map/ppermute | solution.py:642
  (21 other events, 196.9 us)
Sparse Core Ops, SparseCore 0:
  9.5 80.9 all-gather.1

commit v4 on v3

--- a/solution.py
+++ b/solution.py
@@ -20,7 +20,7 @@
 ST = 128
 PAIR = 128
 HALO = 16
-LOGROWS = 16
+LOGROWS = 8
 D = 2048
 COL = 256
 FF = 704
@@ -222,7 +222,7 @@
     payload[0:ST, :] = carry[...].astype(BF)
     high = total[...].astype(BF)
     low = (total[...] - high.astype(F32)).astype(BF)
-    payload[ST : ST + LOGROWS, :] = jnp.concatenate([high, low], axis=0)
+    payload[ST : ST + LOGROWS, :] = jnp.concatenate([high[0:4], low[0:4]], axis=0)
 
 
 def state_kernel(*args):
@@ -304,7 +304,7 @@
 
 
 def log_row(ref):
-    return ref[ST : ST + 1, :].astype(F32) + ref[ST + 8 : ST + 9, :].astype(F32)
+    return ref[ST : ST + 1, :].astype(F32) + ref[ST + 4 : ST + 5, :].astype(F32)
 
 
 def scan_line(place, refs, state, prefix):
@@ -334,8 +334,9 @@
     payload[0:ST, :] = state[...].astype(BF)
     high = whole.astype(BF)
     low = (whole - high.astype(F32)).astype(BF)
-    payload[ST : ST + 8, :] = jnp.broadcast_to(high, (8, CH))
-    payload[ST + 8 : ST + 16, :] = jnp.broadcast_to(low, (8, CH))
+    payload[ST : ST + LOGROWS, :] = jnp.concatenate(
+        [jnp.broadcast_to(high, (4, CH)), jnp.broadcast_to(low, (4, CH))], axis=0
+    )
     ahead_out[...] = jnp.broadcast_to(ahead, (8, CH))
 
 
@@ -541,7 +542,7 @@
             rows_x[rows, cols] = (r[rows, :].astype(F32) * scale * gain[:, cols]).astype(BF)
         return 0
 
-    lax.fori_loop(0, rows_x.shape[0] // NORM_ROWS, norm, 0)
+    lax.fori_loop(0, rows_x.shape[0] // NORM_ROWS, norm, 0, unroll=2)
 
 
 def ffn_hidden(weights, rows_x, hid, at, width):

time: 161 us -> 160 us (level)
  no operation moved by 1% of the time
where the time goes in v4:
time: 160 us; the launch traced here: 159 us
  waiting for transfers between devices  57.4 us (36%)
  starting transfers between devices  45.7 us (29%)
  Pallas kernels  37.8 us (24%)
  between operations  13.6 us (8%)
  local copies, waits for them, and re-layouts  4.02 us (3%)
    ppermute x24, waiting for transfers between devices, turn(): lax.ppermute(array, axis, [(i, (i + distance) % count) for i in range(cou...  56.3 us
    ppermute x24, starting transfers between devices, turn(): lax.ppermute(array, axis, [(i, (i + distance) % count) for i in range(cou...  39.3 us
    pallas_call x2, Pallas kernels, ffn_kernel(): pl.pallas_call(ffn_first_body if first else ffn_next_body, out_shape=shap...  13.7 us
    pallas_call x1, Pallas kernels, state_kernel(): pl.pallas_call(state_body, out_shape=(sds((T, CH), BF), sds((T, 256), BF)...  4.41 us
    pallas_call x1, Pallas kernels, local_kernel(): pl.pallas_call(local_body, out_shape=(sds((T, CH), F32), sds((T, CH), F32...  4.38 us
    unnamed x15, local copies, waits for them, and re-layouts  4.02 us
    ppermute x1, starting transfers between devices, shards(): halo = lax.ppermute(tail, SP, [(i, i + 1) for i in range(15)])  3.59 us
    pallas_call x2, Pallas kernels, mix_kernel(): pl.pallas_call(functools.partial(mix_body, start, count), out_shape=(sds(...  3.48 us
  transfers between devices with their start and end apart: 38, of which 19 were waited for; matrix products, arithmetic and copies ran while one was open for 1% of the time, Pallas kernels for 22%

profile of v4, /device:TPU:0, one launch (start us, length us, event | category | flops | bytes accessed | tf_op | source)
XLA Modules:
  0.0 158.6 jit_solution(9878370875667081331)
XLA Ops:
  6.6 2.1 %head.1 = (bf16[2112,128]{1,0:T(8,128)(2,1)}, bf16[16,768]{1,0:T(8,128)(2,1)S(1)}, f32[8,1024]{1,0:T(8,128)S(1)}, f32[8,1024]{1,0:T(8,128)S(1)}, f32[8,1024]{1,0...) custom-call(bf16[704,128]{1,0:T(8,128)(2,1)} %bitcast.27, ...), custom_call_target="tpu_custom_call" | custom-call | tf_op jit(solution)/shard_map/head/pallas_call | solution.py:162
  8.7 3.6 %collective-permute-start = (bf16[16,768]{1,0:T(8,128)(2,1)S(1)}, bf16[16,768]{1,0:T(8,128)(2,1)S(1)}, u32[]{:S(2)}, u32[]{:S(2)}) collective-permute-start(bf16[16,768]{1,0:T(8,128)(2,1)S(1)} %get-tuple-element.63), channel_id=1, source_target_pairs={{0,8},{8,16},{16,24},{24,32},{32,40},{40,48},{48,56},{56,64},{64,7... | collective-permute-start | bytes 73736 | tf_op jit(solution)/shard_map/ppermute | solution.py:686
  13.9 4.4 %state.1 = (bf16[1024,512]{1,0:T(8,128)(2,1)S(1)}, bf16[1024,256]{1,0:T(8,128)(2,1)S(1)}, bf16[8,128,512]{2,1,0:T(8,128)(2,1)S(1)}, bf16[136,512]{1,0:T(8,128)(2,1)S(1)}) custom-call(bf16[1024,512]{1,0:T(8,128)(2,1)S(1)} %copy-done, bf16[1024,256]{1,0:T(8,128)(2,1)S(1)} %bitcast.20, bf16[16,768]{1,0:T(8,128)(2,1)S(1)} %collective-permute-done.halo, ...), custom_call_target="tpu_custom_call" | custom-call | tf_op jit(solution)/shard_map/state/pallas_call | solution.py:229
  18.3 3.8 %collective-permute-start.3 = (bf16[136,512]{1,0:T(8,128)(2,1)S(1)}, bf16[136,512]{1,0:T(8,128)(2,1)S(1)}, u32[]{:S(2)}, u32[]{:S(2)}) collective-permute-start(bf16[136,512]{1,0:T(8,128)(2,1)S(1)} %get-tuple-element.69.r0), channel_id=1, source_target_pairs={{0,24},{8,0},{16,8},{24,16},{1,25},{9,1},{17,9},{25,17},{2,26},{10... | collective-permute-start | bytes 417800 | tf_op jit(solution)/shard_map/ppermute | solution.py:643
  23.7 5.8 %collective-permute-done.3.r3 = bf16[136,512]{1,0:T(8,128)(2,1)S(1)} collective-permute-done((bf16[136,512]{1,0:T(8,128)(2,1)S(1)}, bf16[136,512]{1,0:T(8,128)(2,1)S(1)}, u32[]{:S(2)}, u32[]{:S(2)}) %collective-permute-start.3) | collective-permute-done | bytes 139296 | tf_op jit(solution)/shard_map/ppermute | solution.py:643
  29.5 2.9 %collective-permute-done.2.r2 = bf16[136,512]{1,0:T(8,128)(2,1)S(1)} collective-permute-done((bf16[136,512]{1,0:T(8,128)(2,1)S(1)}, bf16[136,512]{1,0:T(8,128)(2,1)S(1)}, u32[]{:S(2)}, u32[]{:S(2)}) %collective-permute-start.2) | collective-permute-done | bytes 139296 | tf_op jit(solution)/shard_map/ppermute | solution.py:643
  34.6 4.3 %collective-permute-start.6 = (bf16[136,512]{1,0:T(8,128)(2,1)S(1)}, bf16[136,512]{1,0:T(8,128)(2,1)S(1)}, u32[]{:S(2)}, u32[]{:S(2)}) collective-permute-start(bf16[136,512]{1,0:T(8,128)(2,1)S(1)} %get-tuple-element.70.q0), channel_id=1, source_target_pairs={{0,96},{32,0},{64,32},{96,64},{1,97},{33,1},{65,33},{97,65},{2,98}... | collective-permute-start | bytes 417800 | tf_op jit(solution)/shard_map/ppermute | solution.py:643
  41.3 4.4 %local.1 = (f32[1024,512]{1,0:T(8,128)S(1)}, f32[1024,512]{1,0:T(8,128)S(1)}) custom-call(bf16[1024,512]{1,0:T(8,128)(2,1)S(1)} %get-tuple-element.73.values, bf16[1024,256]{1,0:T(8,128)(2,1)S(1)} %get-tuple-element.74.maps, f32[8,1024]{1,0:T(8,128)S(1)} %get-tuple-element.75.cum_in, f32[8,1024]{1,0:T(8,128)S(1)} %get-tuple-element.76.step_in, ...), custom_call_target="tpu_custom_call" | custom-call | flops 6000000000 | bytes 6000000 | tf_op jit(solution)/shard_map/local/pallas_call | solution.py:295
  54.6 3.3 %collective-permute-start.23 = (bf16[512,256]{1,0:T(8,128)(2,1)S(1)}, bf16[512,256]{1,0:T(8,128)(2,1)S(1)}, u32[]{:S(2)}, u32[]{:S(2)}) collective-permute-start(bf16[512,256]{1,0:T(8,128)(2,1)S(1)} %get-tuple-element.100), channel_id=1, source_target_pairs={{0,4},{2,6},{4,0},{6,2},{1,5},{3,7},{5,1},{7,3},{8,12},{10,14},{12... | collective-permute-start | bytes 786440 | tf_op jit(solution)/shard_map/ppermute | solution.py:643
  59.7 2.6 %collective-permute-start.25 = (bf16[512,256]{1,0:T(8,128)(2,1)S(1)}, bf16[512,256]{1,0:T(8,128)(2,1)S(1)}, u32[]{:S(2)}, u32[]{:S(2)}) collective-permute-start(bf16[512,256]{1,0:T(8,128)(2,1)S(1)} %get-tuple-element.102), channel_id=1, source_target_pairs={{0,6},{2,0},{4,2},{6,4},{1,7},{3,1},{5,3},{7,5},{8,14},{10,8},{12,... | collective-permute-start | bytes 786440 | tf_op jit(solution)/shard_map/ppermute | solution.py:643
  65.5 2.7 %collective-permute-start.10 = (bf16[512,256]{1,0:T(8,128)(2,1)S(1)}, bf16[512,256]{1,0:T(8,128)(2,1)S(1)}, u32[]{:S(2)}, u32[]{:S(2)}) collective-permute-start(bf16[512,256]{1,0:T(8,128)(2,1)S(1)} %get-tuple-element.87), channel_id=1, source_target_pairs={{0,6},{2,0},{4,2},{6,4},{1,7},{3,1},{5,3},{7,5},{8,14},{10,8},{12,... | collective-permute-start | bytes 786440 | tf_op jit(solution)/shard_map/ppermute | solution.py:643
  69.3 5.8 %collective-permute-done.24.f2 = bf16[512,256]{1,0:T(8,128)(2,1)S(1)} collective-permute-done((bf16[512,256]{1,0:T(8,128)(2,1)S(1)}, bf16[512,256]{1,0:T(8,128)(2,1)S(1)}, u32[]{:S(2)}, u32[]{:S(2)}) %collective-permute-start.24) | collective-permute-done | bytes 262176 | tf_op jit(solution)/shard_map/ppermute | solution.py:643
  75.4 4.7 %collective-permute-start.27 = (bf16[512,256]{1,0:T(8,128)(2,1)S(1)}, bf16[512,256]{1,0:T(8,128)(2,1)S(1)}, u32[]{:S(2)}, u32[]{:S(2)}) collective-permute-start(bf16[512,256]{1,0:T(8,128)(2,1)S(1)} %own.3.m0), channel_id=1, source_target_pairs={{0,4},{2,6},{4,0},{6,2},{1,5},{3,7},{5,1},{7,3},{8,12},{10,14},{12... | collective-permute-start | bytes 786440 | tf_op jit(solution)/shard_map/ppermute | solution.py:643
  84.2 2.6 %collective-permute-start.12 = (bf16[512,256]{1,0:T(8,128)(2,1)S(1)}, bf16[512,256]{1,0:T(8,128)(2,1)S(1)}, u32[]{:S(2)}, u32[]{:S(2)}) collective-permute-start(bf16[512,256]{1,0:T(8,128)(2,1)S(1)} %own.2.m0), channel_id=1, source_target_pairs={{0,4},{2,6},{4,0},{6,2},{1,5},{3,7},{5,1},{7,3},{8,12},{10,14},{12... | collective-permute-start | bytes 786440 | tf_op jit(solution)/shard_map/ppermute | solution.py:643
  87.4 4.5 %collective-permute-done.28.m3 = bf16[512,256]{1,0:T(8,128)(2,1)S(1)} collective-permute-done((bf16[512,256]{1,0:T(8,128)(2,1)S(1)}, bf16[512,256]{1,0:T(8,128)(2,1)S(1)}, u32[]{:S(2)}, u32[]{:S(2)}) %collective-permute-start.28) | collective-permute-done | bytes 262176 | tf_op jit(solution)/shard_map/ppermute | solution.py:643
  93.7 5.4 %collective-permute-done.13.m3 = bf16[512,256]{1,0:T(8,128)(2,1)S(1)} collective-permute-done((bf16[512,256]{1,0:T(8,128)(2,1)S(1)}, bf16[512,256]{1,0:T(8,128)(2,1)S(1)}, u32[]{:S(2)}, u32[]{:S(2)}) %collective-permute-start.13) | collective-permute-done | bytes 262176 | tf_op jit(solution)/shard_map/ppermute | solution.py:643
  99.1 4.8 %collective-permute-done.12.m2 = bf16[512,256]{1,0:T(8,128)(2,1)S(1)} collective-permute-done((bf16[512,256]{1,0:T(8,128)(2,1)S(1)}, bf16[512,256]{1,0:T(8,128)(2,1)S(1)}, u32[]{:S(2)}, u32[]{:S(2)}) %collective-permute-start.12) | collective-permute-done | bytes 262176 | tf_op jit(solution)/shard_map/ppermute | solution.py:643
  107.5 7.4 %ffn.2 = (bf16[4,512,256]{2,1,0:T(8,128)(2,1)S(1)}, bf16[512,704]{1,0:T(8,128)(2,1)S(1)}, bf16[16,2112,128]{2,1,0:T(8,128)(2,1)S(1)}) custom-call(s32[8]{0:T(128)S(1)} %pad_add_fusion.order, bf16[16,2112,128]{2,1,0:T(8,128)(2,1)} %bitcast.35, f32[1,2048]{1,0:T(1,128)S(1)} %bitcast.21, bf16[512,256]{1,0:T(8,128)(2,1)S(1)} %own.2.m0, ...), custom_call_target="tpu_custom_call" | custom-call | flops 8999999488 | bytes 12000000 | tf_op jit(solution)/shard_map/ffn/pallas_call | solution.py:613
  115.4 6.3 %ffn.3 = (bf16[4,512,256]{2,1,0:T(8,128)(2,1)S(1)}, bf16[512,704]{1,0:T(8,128)(2,1)S(1)}) custom-call(s32[8]{0:T(128)S(1)} %pad_add_fusion.order, bf16[16,2112,128]{2,1,0:T(8,128)(2,1)S(1)} %get-tuple-element.91.weights, f32[1,2048]{1,0:T(1,128)S(1)} %bitcast.22, bf16[512,256]{1,0:T(8,128)(2,1)S(1)} %own.3.m0, ...), custom_call_target="tpu_custom_call" | custom-call | flops 8999999488 | bytes 12000000 | tf_op jit(solution)/shard_map/ffn/pallas_call | solution.py:613
  124.0 3.1 %collective-permute-start.19 = (bf16[512,256]{1,0:T(8,128)(2,1)S(1)}, bf16[512,256]{1,0:T(8,128)(2,1)S(1)}, u32[]{:S(2)}, u32[]{:S(2)}) collective-permute-start(bf16[512,256]{1,0:T(8,128)(2,1)S(1)} %get-tuple-element.94), channel_id=1, source_target_pairs={{0,4},{2,6},{4,0},{6,2},{1,5},{3,7},{5,1},{7,3},{8,12},{10,14},{12... | collective-permute-start | bytes 786440 | tf_op jit(solution)/shard_map/ppermute | solution.py:643
  130.0 2.7 %collective-permute-start.21 = (bf16[512,256]{1,0:T(8,128)(2,1)S(1)}, bf16[512,256]{1,0:T(8,128)(2,1)S(1)}, u32[]{:S(2)}, u32[]{:S(2)}) collective-permute-start(bf16[512,256]{1,0:T(8,128)(2,1)S(1)} %get-tuple-element.96), channel_id=1, source_target_pairs={{0,6},{2,0},{4,2},{6,4},{1,7},{3,1},{5,3},{7,5},{8,14},{10,8},{12,... | collective-permute-start | bytes 786440 | tf_op jit(solution)/shard_map/ppermute | solution.py:643
  132.7 2.1 %collective-permute-done.19.f1 = bf16[512,256]{1,0:T(8,128)(2,1)S(1)} collective-permute-done((bf16[512,256]{1,0:T(8,128)(2,1)S(1)}, bf16[512,256]{1,0:T(8,128)(2,1)S(1)}, u32[]{:S(2)}, u32[]{:S(2)}) %collective-permute-start.19) | collective-permute-done | bytes 262176 | tf_op jit(solution)/shard_map/ppermute | solution.py:643
  136.6 8.6 %collective-permute-done.20.f2 = bf16[512,256]{1,0:T(8,128)(2,1)S(1)} collective-permute-done((bf16[512,256]{1,0:T(8,128)(2,1)S(1)}, bf16[512,256]{1,0:T(8,128)(2,1)S(1)}, u32[]{:S(2)}, u32[]{:S(2)}) %collective-permute-start.20) | collective-permute-done | bytes 262176 | tf_op jit(solution)/shard_map/ppermute | solution.py:643
  145.5 5.3 %collective-permute-done.35.f2 = bf16[512,256]{1,0:T(8,128)(2,1)S(1)} collective-permute-done((bf16[512,256]{1,0:T(8,128)(2,1)S(1)}, bf16[512,256]{1,0:T(8,128)(2,1)S(1)}, u32[]{:S(2)}, u32[]{:S(2)}) %collective-permute-start.35) | collective-permute-done | bytes 262176 | tf_op jit(solution)/shard_map/ppermute | solution.py:643
  (92 shorter events, 41.5 us)
Async XLA Ops:
  6.5 100.0 %all-gather.2.cloned.1.call-start = ((), (), s32[]{:S(2)}) async-start(), calls=%async_computation | async-start | bytes 9191424 | tf_op jit(solution)/shard_map/all_gather | solution.py:684
  18.3 11.2 %collective-permute-start.3 = (bf16[136,512]{1,0:T(8,128)(2,1)S(1)}, bf16[136,512]{1,0:T(8,128)(2,1)S(1)}, u32[]{:S(2)}, u32[]{:S(2)}) collective-permute-start(bf16[136,512]{1,0:T(8,128)(2,1)S(1)} %get-tuple-element.69.r0), channel_id=1, source_target_pairs={{0,24},{8,0},{16,8},{24,16},{1,25},{9,1},{17,9},{25,17},{2,26},{10... | collective-permute-start | bytes 417800 | tf_op jit(solution)/shard_map/ppermute | solution.py:643
  22.7 11.6 %collective-permute-start.1 = (bf16[136,512]{1,0:T(8,128)(2,1)S(1)}, bf16[136,512]{1,0:T(8,128)(2,1)S(1)}, u32[]{:S(2)}, u32[]{:S(2)}) collective-permute-start(bf16[136,512]{1,0:T(8,128)(2,1)S(1)} %get-tuple-element.69.r0), channel_id=1, source_target_pairs={{0,8},{8,16},{16,24},{24,0},{1,9},{9,17},{17,25},{25,1},{2,10},{10... | collective-permute-start | bytes 417800 | tf_op jit(solution)/shard_map/ppermute | solution.py:643
  34.6 11.1 %collective-permute-start.6 = (bf16[136,512]{1,0:T(8,128)(2,1)S(1)}, bf16[136,512]{1,0:T(8,128)(2,1)S(1)}, u32[]{:S(2)}, u32[]{:S(2)}) collective-permute-start(bf16[136,512]{1,0:T(8,128)(2,1)S(1)} %get-tuple-element.70.q0), channel_id=1, source_target_pairs={{0,96},{32,0},{64,32},{96,64},{1,97},{33,1},{65,33},{97,65},{2,98}... | collective-permute-start | bytes 417800 | tf_op jit(solution)/shard_map/ppermute | solution.py:643
  54.6 10.9 %collective-permute-start.23 = (bf16[512,256]{1,0:T(8,128)(2,1)S(1)}, bf16[512,256]{1,0:T(8,128)(2,1)S(1)}, u32[]{:S(2)}, u32[]{:S(2)}) collective-permute-start(bf16[512,256]{1,0:T(8,128)(2,1)S(1)} %get-tuple-element.100), channel_id=1, source_target_pairs={{0,4},{2,6},{4,0},{6,2},{1,5},{3,7},{5,1},{7,3},{8,12},{10,14},{12... | collective-permute-start | bytes 786440 | tf_op jit(solution)/shard_map/ppermute | solution.py:643
  59.1 16.0 %collective-permute-start.24 = (bf16[512,256]{1,0:T(8,128)(2,1)S(1)}, bf16[512,256]{1,0:T(8,128)(2,1)S(1)}, u32[]{:S(2)}, u32[]{:S(2)}) collective-permute-start(bf16[512,256]{1,0:T(8,128)(2,1)S(1)} %get-tuple-element.101), channel_id=1, source_target_pairs={{0,2},{2,4},{4,6},{6,0},{1,3},{3,5},{5,7},{7,1},{8,10},{10,12},{12... | collective-permute-start | bytes 786440 | tf_op jit(solution)/shard_map/ppermute | solution.py:643
  59.7 15.4 %collective-permute-start.25 = (bf16[512,256]{1,0:T(8,128)(2,1)S(1)}, bf16[512,256]{1,0:T(8,128)(2,1)S(1)}, u32[]{:S(2)}, u32[]{:S(2)}) collective-permute-start(bf16[512,256]{1,0:T(8,128)(2,1)S(1)} %get-tuple-element.102), channel_id=1, source_target_pairs={{0,6},{2,0},{4,2},{6,4},{1,7},{3,1},{5,3},{7,5},{8,14},{10,8},{12,... | collective-permute-start | bytes 786440 | tf_op jit(solution)/shard_map/ppermute | solution.py:643
  62.6 17.4 %collective-permute-start.8 = (bf16[512,256]{1,0:T(8,128)(2,1)S(1)}, bf16[512,256]{1,0:T(8,128)(2,1)S(1)}, u32[]{:S(2)}, u32[]{:S(2)}) collective-permute-start(bf16[512,256]{1,0:T(8,128)(2,1)S(1)} %get-tuple-element.85), channel_id=1, source_target_pairs={{0,4},{2,6},{4,0},{6,2},{1,5},{3,7},{5,1},{7,3},{8,12},{10,14},{12... | collective-permute-start | bytes 786440 | tf_op jit(solution)/shard_map/ppermute | solution.py:643
  62.7 18.8 %collective-permute-start.9 = (bf16[512,256]{1,0:T(8,128)(2,1)S(1)}, bf16[512,256]{1,0:T(8,128)(2,1)S(1)}, u32[]{:S(2)}, u32[]{:S(2)}) collective-permute-start(bf16[512,256]{1,0:T(8,128)(2,1)S(1)} %get-tuple-element.86), channel_id=1, source_target_pairs={{0,2},{2,4},{4,6},{6,0},{1,3},{3,5},{5,7},{7,1},{8,10},{10,12},{12... | collective-permute-start | bytes 786440 | tf_op jit(solution)/shard_map/ppermute | solution.py:643
  65.5 17.0 %collective-permute-start.10 = (bf16[512,256]{1,0:T(8,128)(2,1)S(1)}, bf16[512,256]{1,0:T(8,128)(2,1)S(1)}, u32[]{:S(2)}, u32[]{:S(2)}) collective-permute-start(bf16[512,256]{1,0:T(8,128)(2,1)S(1)} %get-tuple-element.87), channel_id=1, source_target_pairs={{0,6},{2,0},{4,2},{6,4},{1,7},{3,1},{5,3},{7,5},{8,14},{10,8},{12,... | collective-permute-start | bytes 786440 | tf_op jit(solution)/shard_map/ppermute | solution.py:643
  75.3 16.6 %collective-permute-start.28 = (bf16[512,256]{1,0:T(8,128)(2,1)S(1)}, bf16[512,256]{1,0:T(8,128)(2,1)S(1)}, u32[]{:S(2)}, u32[]{:S(2)}) collective-permute-start(bf16[512,256]{1,0:T(8,128)(2,1)S(1)} %own.3.m0), channel_id=1, source_target_pairs={{0,2},{2,4},{4,6},{6,0},{1,3},{3,5},{5,7},{7,1},{8,10},{10,12},{12... | collective-permute-start | bytes 786440 | tf_op jit(solution)/shard_map/ppermute | solution.py:643
  75.4 18.3 %collective-permute-start.27 = (bf16[512,256]{1,0:T(8,128)(2,1)S(1)}, bf16[512,256]{1,0:T(8,128)(2,1)S(1)}, u32[]{:S(2)}, u32[]{:S(2)}) collective-permute-start(bf16[512,256]{1,0:T(8,128)(2,1)S(1)} %own.3.m0), channel_id=1, source_target_pairs={{0,4},{2,6},{4,0},{6,2},{1,5},{3,7},{5,1},{7,3},{8,12},{10,14},{12... | collective-permute-start | bytes 786440 | tf_op jit(solution)/shard_map/ppermute | solution.py:643
  82.6 16.5 %collective-permute-start.13 = (bf16[512,256]{1,0:T(8,128)(2,1)S(1)}, bf16[512,256]{1,0:T(8,128)(2,1)S(1)}, u32[]{:S(2)}, u32[]{:S(2)}) collective-permute-start(bf16[512,256]{1,0:T(8,128)(2,1)S(1)} %own.2.m0), channel_id=1, source_target_pairs={{0,2},{2,4},{4,6},{6,0},{1,3},{3,5},{5,7},{7,1},{8,10},{10,12},{12... | collective-permute-start | bytes 786440 | tf_op jit(solution)/shard_map/ppermute | solution.py:643
  84.2 19.8 %collective-permute-start.12 = (bf16[512,256]{1,0:T(8,128)(2,1)S(1)}, bf16[512,256]{1,0:T(8,128)(2,1)S(1)}, u32[]{:S(2)}, u32[]{:S(2)}) collective-permute-start(bf16[512,256]{1,0:T(8,128)(2,1)S(1)} %own.2.m0), channel_id=1, source_target_pairs={{0,4},{2,6},{4,0},{6,2},{1,5},{3,7},{5,1},{7,3},{8,12},{10,14},{12... | collective-permute-start | bytes 786440 | tf_op jit(solution)/shard_map/ppermute | solution.py:643
  86.7 17.2 %collective-permute-start.11 = (bf16[512,256]{1,0:T(8,128)(2,1)S(1)}, bf16[512,256]{1,0:T(8,128)(2,1)S(1)}, u32[]{:S(2)}, u32[]{:S(2)}) collective-permute-start(bf16[512,256]{1,0:T(8,128)(2,1)S(1)} %own.2.m0), channel_id=1, source_target_pairs={{0,6},{2,0},{4,2},{6,4},{1,7},{3,1},{5,3},{7,5},{8,14},{10,8},{12,... | collective-permute-start | bytes 786440 | tf_op jit(solution)/shard_map/ppermute | solution.py:643
  91.9 12.6 %collective-permute-start.26 = (bf16[512,256]{1,0:T(8,128)(2,1)S(1)}, bf16[512,256]{1,0:T(8,128)(2,1)S(1)}, u32[]{:S(2)}, u32[]{:S(2)}) collective-permute-start(bf16[512,256]{1,0:T(8,128)(2,1)S(1)} %own.3.m0), channel_id=1, source_target_pairs={{0,6},{2,0},{4,2},{6,4},{1,7},{3,1},{5,3},{7,5},{8,14},{10,8},{12,... | collective-permute-start | bytes 786440 | tf_op jit(solution)/shard_map/ppermute | solution.py:643
  93.7 10.9 %collective-permute-start.14 = (bf16[512,256]{1,0:T(8,128)(2,1)S(1)}, bf16[512,256]{1,0:T(8,128)(2,1)S(1)}, u32[]{:S(2)}, u32[]{:S(2)}) collective-permute-start(bf16[512,256]{1,0:T(8,128)(2,1)S(1)} %own.2.m0), channel_id=1, source_target_pairs={{0,1},{1,0},{2,3},{3,2},{4,5},{5,4},{6,7},{7,6},{8,9},{9,8},{10,11... | collective-permute-start | bytes 786440 | tf_op jit(solution)/shard_map/ppermute | solution.py:647
  104.5 10.9 %collective-permute-start.29 = (bf16[512,256]{1,0:T(8,128)(2,1)S(1)}, bf16[512,256]{1,0:T(8,128)(2,1)S(1)}, u32[]{:S(2)}, u32[]{:S(2)}) collective-permute-start(bf16[512,256]{1,0:T(8,128)(2,1)S(1)} %own.3.m0), channel_id=1, source_target_pairs={{0,1},{1,0},{2,3},{3,2},{4,5},{5,4},{6,7},{7,6},{8,9},{9,8},{10,11... | collective-permute-start | bytes 786440 | tf_op jit(solution)/shard_map/ppermute | solution.py:647
  124.0 10.9 %collective-permute-start.19 = (bf16[512,256]{1,0:T(8,128)(2,1)S(1)}, bf16[512,256]{1,0:T(8,128)(2,1)S(1)}, u32[]{:S(2)}, u32[]{:S(2)}) collective-permute-start(bf16[512,256]{1,0:T(8,128)(2,1)S(1)} %get-tuple-element.94), channel_id=1, source_target_pairs={{0,4},{2,6},{4,0},{6,2},{1,5},{3,7},{5,1},{7,3},{8,12},{10,14},{12... | collective-permute-start | bytes 786440 | tf_op jit(solution)/shard_map/ppermute | solution.py:643
  128.9 16.6 %collective-permute-start.34 = (bf16[512,256]{1,0:T(8,128)(2,1)S(1)}, bf16[512,256]{1,0:T(8,128)(2,1)S(1)}, u32[]{:S(2)}, u32[]{:S(2)}) collective-permute-start(bf16[512,256]{1,0:T(8,128)(2,1)S(1)} %get-tuple-element.106), channel_id=1, source_target_pairs={{0,4},{2,6},{4,0},{6,2},{1,5},{3,7},{5,1},{7,3},{8,12},{10,14},{12... | collective-permute-start | bytes 786440 | tf_op jit(solution)/shard_map/ppermute | solution.py:643
  129.5 15.8 %collective-permute-start.20 = (bf16[512,256]{1,0:T(8,128)(2,1)S(1)}, bf16[512,256]{1,0:T(8,128)(2,1)S(1)}, u32[]{:S(2)}, u32[]{:S(2)}) collective-permute-start(bf16[512,256]{1,0:T(8,128)(2,1)S(1)} %get-tuple-element.95), channel_id=1, source_target_pairs={{0,2},{2,4},{4,6},{6,0},{1,3},{3,5},{5,7},{7,1},{8,10},{10,12},{12... | collective-permute-start | bytes 786440 | tf_op jit(solution)/shard_map/ppermute | solution.py:643
  130.0 15.2 %collective-permute-start.21 = (bf16[512,256]{1,0:T(8,128)(2,1)S(1)}, bf16[512,256]{1,0:T(8,128)(2,1)S(1)}, u32[]{:S(2)}, u32[]{:S(2)}) collective-permute-start(bf16[512,256]{1,0:T(8,128)(2,1)S(1)} %get-tuple-element.96), channel_id=1, source_target_pairs={{0,6},{2,0},{4,2},{6,4},{1,7},{3,1},{5,3},{7,5},{8,14},{10,8},{12,... | collective-permute-start | bytes 786440 | tf_op jit(solution)/shard_map/ppermute | solution.py:643
  132.7 18.1 %collective-permute-start.35 = (bf16[512,256]{1,0:T(8,128)(2,1)S(1)}, bf16[512,256]{1,0:T(8,128)(2,1)S(1)}, u32[]{:S(2)}, u32[]{:S(2)}) collective-permute-start(bf16[512,256]{1,0:T(8,128)(2,1)S(1)} %get-tuple-element.107), channel_id=1, source_target_pairs={{0,2},{2,4},{4,6},{6,0},{1,3},{3,5},{5,7},{7,1},{8,10},{10,12},{12... | collective-permute-start | bytes 786440 | tf_op jit(solution)/shard_map/ppermute | solution.py:643
  134.8 15.9 %collective-permute-start.36 = (bf16[512,256]{1,0:T(8,128)(2,1)S(1)}, bf16[512,256]{1,0:T(8,128)(2,1)S(1)}, u32[]{:S(2)}, u32[]{:S(2)}) collective-permute-start(bf16[512,256]{1,0:T(8,128)(2,1)S(1)} %get-tuple-element.108), channel_id=1, source_target_pairs={{0,6},{2,0},{4,2},{6,4},{1,7},{3,1},{5,3},{7,5},{8,14},{10,8},{12,... | collective-permute-start | bytes 786440 | tf_op jit(solution)/shard_map/ppermute | solution.py:643
  (21 other events, 195.3 us)
Sparse Core Ops, SparseCore 0:
  9.5 80.8 all-gather.1
